TPU v7x, 32 devices: a whole 2x2x4 slice. The times are simulated.
32 devices in a mesh: grp: 2 (over x), tp: 16 (over z, y, core).
Axes of the slice: x: 2, y: 2, z: 4, core: 2. Of those that a mesh axis runs over, the one named last changes fastest.
Arguments:
- tokens: bfloat16 [160, 2048], P('grp', 'tp'), parts along dimension 0, may hold values from -6 to 6
- lengths: int32 [160], P('grp'), parts along dimension 0, may hold values from 1 to 4096, 81920 in all
- cell_memory: float32 [2, 160, 2048, 256], P(None, 'grp', 'tp'), parts along dimension 1, may hold values from -0.6 to 0.6
- key_sums: float32 [2, 160, 2048], P(None, 'grp', 'tp'), parts along dimension 1, may hold values from -3 to 3
- stabilizer: float32 [2, 160, 8], P(None, 'grp'), parts along dimension 1, may hold values from -3 to 1
- norm_gain: bfloat16 [2, 2048], replicated, may hold values from 0.099609375 to 1.8984375
- query_weight: bfloat16 [2, 2048, 2048], P(None, None, 'tp'), may hold values from -0.125 to 0.125
- key_weight: bfloat16 [2, 2048, 2048], P(None, None, 'tp'), may hold values from -0.125 to 0.125
- value_weight: bfloat16 [2, 2048, 2048], P(None, None, 'tp'), may hold values from -0.125 to 0.125
- outgate_weight: bfloat16 [2, 2048, 2048], P(None, None, 'tp'), may hold values from -0.125 to 0.125
- ingate_weight: bfloat16 [2, 2048, 8], replicated, may hold values from -0.125 to 0.125
- forget_weight: bfloat16 [2, 2048, 8], replicated, may hold values from -0.125 to 0.125
- ingate_bias: float32 [2, 8], replicated, may hold values from -3 to 3
- forget_bias: float32 [2, 8], replicated, may hold values from -1 to 4
- forget_slope: float32 [2, 8], replicated, may hold values from -3 to 3
- head_gain: bfloat16 [2, 2048], P(None, 'tp'), may hold values from 0.099609375 to 1.8984375
- output_weight: bfloat16 [2, 2048, 2048], P(None, None, 'tp'), may hold values from -0.125 to 0.125
Outputs:
- new_tokens: bfloat16 [160, 2048], P('grp', 'tp'), parts along dimension 0
- new_memory: float32 [2, 160, 2048, 256], P(None, 'grp', 'tp'), parts along dimension 1
- new_key_sums: float32 [2, 160, 2048], P(None, 'grp', 'tp'), parts along dimension 1
- new_stabilizer: float32 [2, 160, 8], P(None, 'grp'), parts along dimension 1
There are 2 independent parts, one for each index of `grp`. A program takes and returns all parts, laid end to end along the dimension named above; an argument that names none is the same for every part. Nothing has to cross between parts.
Inputs may be any that keep to these rules, and one draw needn't show every extreme that they name: Each part's 80 lengths sum to 81920, and the largest is exactly 4096.
All inputs are finite; a program needn't handle non-finite values.
Results may differ from a plain program's by a relative error of at most 0.018.
Values may be sent and summed in bfloat16 or wider, within the bound.
No kernel may reach another device: no remote copies, remote signals or barrier semaphores. Data moves between devices by JAX's collectives and lax.ppermute only.
A program may use at most 128 MiB of HBM per device.

v0:
```python
import jax
import jax.numpy as jnp
from jax import lax
from jax.sharding import PartitionSpec as P

HEADS = 8
HEAD = 256
MAXLEN = 4096


EPS = 1e-05


def from_partner(value, axis, stride):
    mask = 2**stride
    pairs = [(source, source ^ mask) for source in range(lax.axis_size(axis))]
    return lax.ppermute(value, axis, pairs)


def body(
    tokens,
    lengths,
    cell_memory,
    key_sums,
    stabilizer,
    norm_gain,
    query_weight,
    key_weight,
    value_weight,
    outgate_weight,
    ingate_weight,
    forget_weight,
    ingate_bias,
    forget_bias,
    forget_slope,
    head_gain,
    output_weight,
):
    devices = lax.axis_size("tp")
    split_count = devices // HEADS
    own_index = lax.axis_index("tp")
    head_id = own_index // split_count
    onehot = (jnp.arange(HEADS) == head_id).astype(jnp.float32)
    position = lengths.astype(jnp.float32) / MAXLEN
    current = tokens
    memories, sums_list, stabs = ([], [], [])
    for block_id in range(cell_memory.shape[0]):
        gathered_rows = lax.all_gather(current, "tp", axis=1, tiled=True)
        row_float = gathered_rows.astype(jnp.float32)
        normed = (
            row_float
            * lax.rsqrt(jnp.mean(row_float * row_float, axis=-1, keepdims=True) + EPS)
            * norm_gain[block_id].astype(jnp.float32)
        ).astype(jnp.bfloat16)
        queries = jnp.dot(
            normed, query_weight[block_id], preferred_element_type=jnp.float32
        ).astype(jnp.bfloat16)
        key_rows = (
            jnp.dot(normed, key_weight[block_id], preferred_element_type=jnp.float32)
            * HEAD ** (-0.5)
        ).astype(jnp.bfloat16)
        values = jnp.dot(normed, value_weight[block_id], preferred_element_type=jnp.float32).astype(
            jnp.bfloat16
        )
        outgate = jnp.dot(
            normed, outgate_weight[block_id], preferred_element_type=jnp.float32
        ).astype(jnp.bfloat16)
        ingate = (
            jnp.dot(normed, ingate_weight[block_id], preferred_element_type=jnp.float32)
            + ingate_bias[block_id]
        )
        forget = jax.nn.log_sigmoid(
            jnp.dot(normed, forget_weight[block_id], preferred_element_type=jnp.float32)
            + forget_bias[block_id]
            + forget_slope[block_id] * position[:, None]
        )
        stab_new = jnp.maximum(forget + stabilizer[block_id], ingate)
        decays = jnp.exp(forget + stabilizer[block_id] - stab_new)
        in_weight = jnp.exp(ingate - stab_new)
        decay_own = jnp.sum(decays * onehot, axis=1)
        inweight_own = jnp.sum(in_weight * onehot, axis=1)
        sums_new = decay_own[:, None] * key_sums[block_id] + inweight_own[
            :, None
        ] * key_rows.astype(jnp.float32)
        head_pair = jnp.stack((queries, key_rows))
        head_sums = sums_new
        for level in range(split_count.bit_length() - 1):
            partner = from_partner(head_pair, "tp", level)
            upper = own_index // (1 << level) % 2 == 1
            lower_half = jnp.where(upper, partner, head_pair)
            upper_half = jnp.where(upper, head_pair, partner)
            head_pair = jnp.concatenate((lower_half, upper_half), axis=2)
            sums_mate = from_partner(head_sums, "tp", level)
            sums_low = jnp.where(upper, sums_mate, head_sums)
            sums_high = jnp.where(upper, head_sums, sums_mate)
            head_sums = jnp.concatenate((sums_low, sums_high), axis=1)
        head_query = head_pair[0].astype(jnp.float32)
        head_keys = head_pair[1].astype(jnp.float32)
        mem_new = (
            decay_own[:, None, None] * cell_memory[block_id]
            + inweight_own[:, None, None]
            * values.astype(jnp.float32)[:, :, None]
            * head_keys[:, None, :]
        )
        numerator = jnp.einsum("bvk,bk->bv", mem_new, head_query, precision=lax.Precision.HIGHEST)
        denominator = jnp.maximum(jnp.abs(jnp.sum(head_sums * head_query, axis=1)), 1.0)
        hidden = numerator / denominator[:, None]
        gated_out = (
            hidden
            * head_gain[block_id].astype(jnp.float32)
            * jax.nn.sigmoid(outgate.astype(jnp.float32))
        ).astype(jnp.bfloat16)
        out_weight = output_weight[block_id]
        projected = jnp.dot(
            lax.all_gather(gated_out, "tp", axis=1, tiled=True),
            out_weight,
            preferred_element_type=jnp.float32,
        )
        current = (current.astype(jnp.float32) + projected).astype(jnp.bfloat16)
        memories.append(mem_new)
        sums_list.append(sums_new)
        stabs.append(stab_new)
    return (current, jnp.stack(memories), jnp.stack(sums_list), jnp.stack(stabs))


def solution(mesh):
    in_specs = (
        P("grp", "tp"),
        P("grp"),
        P(None, "grp", "tp", None),
        P(None, "grp", "tp"),
        P(None, "grp", None),
        P(),
        P(None, None, "tp"),
        P(None, None, "tp"),
        P(None, None, "tp"),
        P(None, None, "tp"),
        P(),
        P(),
        P(),
        P(),
        P(),
        P(None, "tp"),
        P(None, None, "tp"),
    )
    out_specs = (
        P("grp", "tp"),
        P(None, "grp", "tp", None),
        P(None, "grp", "tp"),
        P(None, "grp", None),
    )
    return jax.shard_map(body, mesh=mesh, in_specs=in_specs, out_specs=out_specs, check_vma=False)
```

profile of v0, /device:TPU:0, one launch (start us, length us, event | category | flops | bytes accessed | tf_op | source)
XLA Modules:
  0.0 133.5 jit_solution(18110746305476406706)
XLA Ops:
  0.7 0.7 convert_multiply_fusion.4
  1.3 0.8 slice_bitcast_fusion
  2.1 0.8 slice_convert_fusion
  2.9 24.3 %all_gather.12 = bf16[80,2048]{1,0:T(8,128)(2,1)S(1)} all-gather(bf16[80,128]{1,0:T(8,128)(2,1)} %param.17), channel_id=1, replica_groups=mesh['grp'=2,'tp'=16] {'tp'}, dimensions={1}, use_global_device_ids=true | all-gather | bytes 348160 | tf_op jit(solution)/shard_map/all_gather | solution.py:48
  27.1 0.0 copy-start
  27.1 0.2 fusion.44
  27.3 0.8 slice_bitcast_fusion.1
  28.1 1.3 %fusion.38 = bf16[1,80,128]{2,1,0:T(8,128)(2,1)S(1)} fusion(bf16[2,2048,128]{2,1,0:T(8,128)(2,1)} %param.23, bf16[80,2048]{1,0:T(8,128)(2,1)S(1)} %all_gather.12, f32[2048]{0:T(1024)S(1)} %bitcast.144, f32[80]{0:T(128)S(1)} %add_rsqrt_fusion.1), kind=kOutput, calls=%fused_computation.51 | convolution fusion | flops 42608640 | bytes 880960 | tf_op jit(solution)/shard_map/dot_general | solution.py:55
  29.4 0.0 copy-start.1
  29.4 1.1 fusion.93
  30.6 1.1 multiply_reduce_fusion.3
  31.6 0.0 copy-start.7
  31.6 0.0 copy-start.9
  31.7 0.0 copy-start.8
  31.7 1.4 %fusion.81 = (f32[80,128]{1,0:T(8,128)S(1)}, bf16[80,128]{1,0:T(8,128)(2,1)S(1)}) fusion(f32[2,80,128]{2,1,0:T(8,128)} %param.20, f32[80]{0:T(128)S(1)} %get-tuple-element.6, f32[80]{0:T(128)S(1)} %get-tuple-element.7, bf16[2,2048,128]{2,1,0:T(8,128)(2,1)} %param.24, bf16[80,2048]{1,0:T(8,128)(2,1)S(1)} %all_gather.12, f32[2048]{0:T(1024)S(1)} %bitcast.147, ...), kind=kOutput, calls=%fused_computation.115 | convolution fusion | flops 42659840 | bytes 963520 | tf_op jit(solution)/shard_map/dot_general | solution.py:59
  33.1 0.0 copy-start.2
  33.1 0.4 collective-permute-start
  33.5 0.2 collective-permute-start.1
  33.7 1.3 %fusion.37 = f32[80,128]{1,0:T(8,128)S(1)} fusion(bf16[2,2048,128]{2,1,0:T(8,128)(2,1)} %param.25, f32[80]{0:T(128)S(1)} %get-tuple-element.7, bf16[80,2048]{1,0:T(8,128)(2,1)S(1)} %all_gather.12, f32[2048]{0:T(1024)S(1)} %bitcast.148, f32[80]{0:T(128)S(1)} %add_rsqrt_fusion.1), kind=kOutput, calls=%fused_computation.50 | convolution fusion | flops 42629120 | bytes 901760 | tf_op jit(solution)/shard_map/dot_general | solution.py:62
  35.0 0.0 copy-start.6
  35.0 0.7 bitcast_convert_fusion
  35.8 0.0 copy-start.4
  35.8 0.0 copy-start.5
  35.8 0.0 copy-start.3
  35.8 0.0 collective-permute-done
  35.8 0.0 collective-permute-done.1
  35.8 0.1 fusion.70
  36.0 8.7 %fusion.4 = f32[80,1,128]{2,1,0:T(1,128)S(1)} fusion(f32[2,80,128,256]{3,2,1,0:T(8,128)} %param.19, f32[80,256]{1,0:T(8,128)S(1)} %get-tuple-element.19, f32[80,128]{1,0:T(8,128)S(1)} %fusion.37, f32[80]{0:T(128)S(1)} %get-tuple-element.6, bf16[80,256,1]{1,0,2:T(8,128)(2,1)S(1)} %get-tuple-element.18), kind=kOutput, calls=%fused_computation.6 | convolution fusion | flops 39321600 | bytes 10690880 | tf_op jit(solution)/shard_map/bvk,bk->bv/dot_general | solution.py:105
  44.7 0.0 copy-done.4
  44.7 0.3 fusion.35
  45.0 18.3 %all_gather.13 = bf16[80,2048]{1,0:T(8,128)(2,1)S(1)} all-gather(bf16[80,128]{1,0:T(8,128)(2,1)S(1)} %fusion.35), channel_id=1, replica_groups=mesh['grp'=2,'tp'=16] {'tp'}, dimensions={1}, use_global_device_ids=true | all-gather | bytes 348160 | tf_op jit(solution)/shard_map/all_gather | solution.py:115
  63.3 0.0 copy-done
  63.3 0.0 copy-done.5
  63.3 0.2 fusion.17
  63.6 19.7 %all_gather.14 = bf16[80,2048]{1,0:T(8,128)(2,1)S(1)} all-gather(bf16[80,128]{1,0:T(8,128)(2,1)S(1)} %fusion.17), channel_id=1, replica_groups=mesh['grp'=2,'tp'=16] {'tp'}, dimensions={1}, use_global_device_ids=true | all-gather | bytes 348160 | tf_op jit(solution)/shard_map/all_gather | solution.py:48
  83.3 0.2 fusion.47
  83.4 0.0 copy-done.1
  83.4 0.3 fusion.39
  83.8 0.0 copy-done.7
  83.8 0.0 copy-done.9
  83.8 0.3 fusion.95
  84.1 0.0 copy-done.8
  84.1 0.3 multiply_reduce_fusion.1
  84.4 0.0 copy-done.2
  84.4 0.3 fusion.28
  84.7 0.0 copy-done.6
  84.7 0.0 copy-done.3
  84.7 0.3 fusion.80
  85.0 0.4 collective-permute-start.2
  85.5 0.2 collective-permute-start.3
  85.6 0.6 pad_maximum_fusion.1
  86.3 0.6 pad_maximum_fusion.6
  86.9 0.0 collective-permute-done.2
  86.9 0.0 collective-permute-done.3
  86.9 0.1 fusion.71
  87.1 10.3 %multiply_add_fusion.1 = (f32[1,80,128,256]{3,2,1,0:T(8,128)S(1)}, f32[1,80,128,256]{3,2,1,0:T(8,128)S(1)}) fusion(f32[2,80,128,256]{3,2,1,0:T(8,128)} %param.19, f32[80,256]{1,0:T(8,128)S(1)} %get-tuple-element.19, f32[80,128]{1,0:T(8,128)S(1)} %fusion.37, f32[80]{0:T(128)S(1)} %get-tuple-element.6, f32[80,256]{1,0:T(8,128)S(1)} %get-tuple-element.13, ...), kind=kLoop, calls=%fused_computation.8 | loop fusion | flops 15728640 | bytes 42189440 | tf_op jit(solution)/shard_map/add | solution.py:100
  97.4 8.6 %fusion.1 = f32[80,1,128]{2,1,0:T(1,128)S(1)} fusion(f32[2,80,128,256]{3,2,1,0:T(8,128)} %param.19, f32[80,256]{1,0:T(8,128)S(1)} %get-tuple-element.13, f32[80,128]{1,0:T(8,128)S(1)} %fusion.28, f32[80]{0:T(128)S(1)} %get-tuple-element.4, bf16[80,256,1]{1,0,2:T(8,128)(2,1)S(1)} %get-tuple-element.12), kind=kOutput, calls=%fused_computation.3 | convolution fusion | flops 39321600 | bytes 10690880 | tf_op jit(solution)/shard_map/bvk,bk->bv/dot_general | solution.py:105
  106.0 0.3 fusion.26
  106.3 18.3 %all_gather.15 = bf16[80,2048]{1,0:T(8,128)(2,1)S(1)} all-gather(bf16[80,128]{1,0:T(8,128)(2,1)S(1)} %fusion.26), channel_id=1, replica_groups=mesh['grp'=2,'tp'=16] {'tp'}, dimensions={1}, use_global_device_ids=true | all-gather | bytes 348160 | tf_op jit(solution)/shard_map/all_gather | solution.py:115
  124.6 0.9 fusion.19
  125.5 8.0 %pad_maximum_fusion = f32[2,80,128,256]{3,2,1,0:T(8,128)} fusion(f32[1,80,128,256]{3,2,1,0:T(8,128)S(1)} %get-tuple-element.9, f32[1,80,128,256]{3,2,1,0:T(8,128)S(1)} %get-tuple-element.8), kind=kLoop, calls=%fused_computation | loop fusion | flops 5242880 | bytes 41943040 | tf_op jit(solution)/shard_map/stack | solution.py:123
  (13 shorter events, 0.1 us)
Async XLA Ops:
  27.1 36.2 %copy-start = (bf16[80,128]{1,0:T(8,128)(2,1)S(1)}, bf16[80,128]{1,0:T(8,128)(2,1)}, u32[]{:S(2)}) copy-start(bf16[80,128]{1,0:T(8,128)(2,1)} %param.17) | copy-start | bytes 61444
  29.4 54.0 %copy-start.1 = (bf16[2,2048,128]{2,1,0:T(8,128)(2,1)S(1)}, bf16[2,2048,128]{2,1,0:T(8,128)(2,1)}, u32[]{:S(2)}) copy-start(bf16[2,2048,128]{2,1,0:T(8,128)(2,1)} %param.23) | copy-start | bytes 3145732
  31.6 52.1 %copy-start.7 = (bf16[2,2048,8]{1,2,0:T(8,128)(2,1)S(1)}, bf16[2,2048,8]{1,2,0:T(8,128)(2,1)}, u32[]{:S(2)}) copy-start(bf16[2,2048,8]{1,2,0:T(8,128)(2,1)} %param.28) | copy-start | bytes 196612
  31.6 52.1 %copy-start.9 = (f32[2,80,8]{1,2,0:T(8,128)S(1)}, f32[2,80,8]{1,2,0:T(8,128)}, u32[]{:S(2)}) copy-start(f32[2,80,8]{1,2,0:T(8,128)} %param.21) | copy-start | bytes 15364
  31.7 52.4 %copy-start.8 = (bf16[2,2048,8]{1,2,0:T(8,128)(2,1)S(1)}, bf16[2,2048,8]{1,2,0:T(8,128)(2,1)}, u32[]{:S(2)}) copy-start(bf16[2,2048,8]{1,2,0:T(8,128)(2,1)} %param.27) | copy-start | bytes 196612
  33.1 51.3 %copy-start.2 = (bf16[2,2048,128]{2,1,0:T(8,128)(2,1)S(1)}, bf16[2,2048,128]{2,1,0:T(8,128)(2,1)}, u32[]{:S(2)}) copy-start(bf16[2,2048,128]{2,1,0:T(8,128)(2,1)} %param.25) | copy-start | bytes 3145732
  33.1 2.7 %collective-permute-start = (bf16[2,80,128]{2,1,0:T(8,128)(2,1)S(1)}, bf16[2,80,128]{2,1,0:T(8,128)(2,1)S(1)}, u32[]{:S(2)}, u32[]{:S(2)}) collective-permute-start(bf16[2,80,128]{2,1,0:T(8,128)(2,1)S(1)} %pad_maximum_fusion.4), channel_id=1, source_target_pairs={{0,1},{1,0},{2,3},{3,2},{4,5},{5,4},{6,7},{7,6},{8,9},{9,8},{10,11... | collective-permute-start | bytes 122888 | tf_op jit(solution)/shard_map/ppermute | solution.py:17
  33.5 2.3 %collective-permute-start.1 = (f32[80,128]{1,0:T(8,128)S(1)}, f32[80,128]{1,0:T(8,128)S(1)}, u32[]{:S(2)}, u32[]{:S(2)}) collective-permute-start(f32[80,128]{1,0:T(8,128)S(1)} %get-tuple-element.34), channel_id=1, source_target_pairs={{0,1},{1,0},{2,3},{3,2},{4,5},{5,4},{6,7},{7,6},{8,9},{9,8},{10,11... | collective-permute-start | bytes 122888 | tf_op jit(solution)/shard_map/ppermute | solution.py:17
  35.0 49.7 %copy-start.6 = (f32[2,80,128]{2,1,0:T(8,128)S(1)}, f32[2,80,128]{2,1,0:T(8,128)}, u32[]{:S(2)}) copy-start(f32[2,80,128]{2,1,0:T(8,128)} %param.20) | copy-start | bytes 245764
  35.8 8.9 %copy-start.4 = (bf16[2,2048,128]{2,1,0:T(8,128)(2,1)S(1)}, bf16[2,2048,128]{2,1,0:T(8,128)(2,1)}, u32[]{:S(2)}) copy-start(bf16[2,2048,128]{2,1,0:T(8,128)(2,1)} %param.26) | copy-start | bytes 3145732
  35.8 27.6 %copy-start.5 = (bf16[2,2048,128]{2,1,0:T(8,128)(2,1)S(1)}, bf16[2,2048,128]{2,1,0:T(8,128)(2,1)}, u32[]{:S(2)}) copy-start(bf16[2,2048,128]{2,1,0:T(8,128)(2,1)} %param.33) | copy-start | bytes 3145732
  35.8 48.9 %copy-start.3 = (bf16[2,2048,128]{2,1,0:T(8,128)(2,1)S(1)}, bf16[2,2048,128]{2,1,0:T(8,128)(2,1)}, u32[]{:S(2)}) copy-start(bf16[2,2048,128]{2,1,0:T(8,128)(2,1)} %param.24) | copy-start | bytes 3145732
  85.0 1.8 %collective-permute-start.2 = (bf16[2,80,128]{2,1,0:T(8,128)(2,1)S(1)}, bf16[2,80,128]{2,1,0:T(8,128)(2,1)S(1)}, u32[]{:S(2)}, u32[]{:S(2)}) collective-permute-start(bf16[2,80,128]{2,1,0:T(8,128)(2,1)S(1)} %pad_maximum_fusion.5), channel_id=1, source_target_pairs={{0,1},{1,0},{2,3},{3,2},{4,5},{5,4},{6,7},{7,6},{8,9},{9,8},{10,11... | collective-permute-start | bytes 122888 | tf_op jit(solution)/shard_map/ppermute | solution.py:17
  85.5 1.4 %collective-permute-start.3 = (f32[80,128]{1,0:T(8,128)S(1)}, f32[80,128]{1,0:T(8,128)S(1)}, u32[]{:S(2)}, u32[]{:S(2)}) collective-permute-start(f32[80,128]{1,0:T(8,128)S(1)} %get-tuple-element.36), channel_id=1, source_target_pairs={{0,1},{1,0},{2,3},{3,2},{4,5},{5,4},{6,7},{7,6},{8,9},{9,8},{10,11... | collective-permute-start | bytes 122888 | tf_op jit(solution)/shard_map/ppermute | solution.py:17
where the time goes:
time: 134 us; the launch traced here: 133 us
  blocking collectives  80.6 us (60%)
  matrix products  26.8 us (20%)
  other arithmetic  22.4 us (17%)
  local copies, waits for them, and re-layouts  1.58 us (1%)
    all_gather x2, blocking collectives, body(): gathered_rows = lax.all_gather(current, 'tp', axis=1, tiled=True)  43.9 us
    all_gather x2, blocking collectives, body(): lax.all_gather(gated_out, 'tp', axis=1, tiled=True)  36.7 us
    dot_general x2, matrix products, body(): jnp.einsum('bvk,bk->bv', mem_new, head_query, precision=lax.Precision.HIG...  17.2 us
    add x1, other arithmetic, body(): decay_own[:, None, None] * cell_memory[block_id]  10.3 us
    another operation x1, other arithmetic, body(): jnp.stack(memories)  8 us
  transfers between devices with their start and end apart: 4, of which 0 were waited for; matrix products, arithmetic and copies ran while one was open for 3% of the time, Pallas kernels for 0%

commit v1 on v0

v1 whole, which is shorter than its diff:
```python
import functools

import jax
import jax.numpy as jnp
from jax import lax
from jax.experimental import pallas as pl
from jax.experimental.pallas import tpu as pltpu
from jax.sharding import PartitionSpec as P


MAXLEN = 4096
EPS = 1e-05
MIB = 1 << 20
PARTS = 3


VM = pl.BlockSpec(memory_space=pltpu.VMEM)
SM = pl.BlockSpec(memory_space=pltpu.SMEM)
HBM = pl.BlockSpec(memory_space=pltpu.HBM)
F32 = jnp.float32
BF16 = jnp.bfloat16


def gather_phases(count):
    bits = [1 << i for i in range(count.bit_length() - 1)][::-1]
    if len(bits) < 2:
        return [tuple(bits)] if bits else []
    low = bits[-1]
    rounds = [(bits[0] | low,)] if len(bits) > 1 else []
    middle = bits[1:-1]
    for at in range(0, len(middle), 2):
        pair = middle[at : at + 2]
        if len(pair) == 2:
            rounds.append((pair[0] | pair[1], pair[1] | low, pair[0] | low))
        else:
            rounds.append((pair[0] | low,))
    return rounds + [(low,)]


def swap(value, mask):
    return lax.ppermute(value, "tp", [(s, s ^ mask) for s in range(lax.axis_size("tp"))])


def gather(value):
    *rounds, last = gather_phases(lax.axis_size("tp"))
    blocks, masks = value[None], [0]
    for group in rounds:
        parts, held = [blocks], list(masks)
        for mask in group:
            parts.append(swap(blocks, mask))
            masks = masks + [m ^ mask for m in held]
        blocks = jnp.concatenate(parts, axis=0)
    far = swap(blocks, last[0])
    return blocks, far, masks, last[0]


def shares(steps):
    sizes = [steps // PARTS + (i < steps % PARTS) for i in range(PARTS)]
    return sizes[1:2] + sizes[0:1] + sizes[2:]


def call(kernel, out_shape, in_specs, out_specs, scratch=(), aliases=None, limit=4, flops=1 << 20):
    return pl.pallas_call(
        kernel,
        out_shape=out_shape,
        in_specs=in_specs,
        out_specs=out_specs,
        scratch_shapes=scratch,
        input_output_aliases=aliases or {},
        compiler_params=pltpu.CompilerParams(vmem_limit_bytes=limit * MIB),
        cost_estimate=pl.CostEstimate(flops=flops, bytes_accessed=1 << 20, transcendentals=0),
    )


def place(own, near, far, rows, masks, low):
    for j, mask in enumerate(masks):
        rows[own ^ mask] = near[j]
        rows[own ^ mask ^ low] = far[j]


def joined(rows):
    return jnp.concatenate([rows[i] for i in range(rows.shape[0])], axis=1)


def dot(a, b):
    return jnp.dot(a, b, preferred_element_type=F32)


def heads_kernel(layer, masks, low, scale, ids, near, far, gain, wq, wk, pair, normed, rows):
    place(ids[0], near, far, rows, masks, low)
    x = joined(rows).astype(F32)
    inv = lax.rsqrt(jnp.mean(x * x, axis=1, keepdims=True) + EPS)
    n = (x * inv * gain[layer : layer + 1].astype(F32)).astype(BF16)
    normed[...] = n
    width = wq.shape[2]
    both = dot(n, jnp.concatenate([wq[layer], wk[layer]], axis=1))
    pair[0] = both[:, :width].astype(BF16)
    pair[1] = (both[:, width:] * scale).astype(BF16)


def as_column(row):
    n = row.shape[1]
    same = lax.broadcasted_iota(jnp.int32, (n, n), 0) == lax.broadcasted_iota(jnp.int32, (n, n), 1)
    return jnp.sum(jnp.where(same, row, 0.0), axis=1, keepdims=True)


def gates_kernel(
    layer, ids, normed, wv, wo, wi, wf, ibias, fbias, slope, lengths, stab, old,
    values, outgate, factors, stab_new, columns, decays,
):
    n = normed[...]
    width = wv.shape[2]
    both = dot(n, jnp.concatenate([wv[layer], wo[layer]], axis=1))
    values[...] = both[:, :width].astype(BF16)
    outgate[...] = both[:, width:].astype(BF16)

    def logits(w):
        return lax.dot_general(w[layer], n, (((1,), (1,)), ((), ())), preferred_element_type=F32)

    row = slice(layer, layer + 1)
    position = lengths[...].astype(F32) / MAXLEN
    ingate = logits(wi) + as_column(ibias[row])
    forget = jax.nn.log_sigmoid(logits(wf) + as_column(fbias[row]) + as_column(slope[row]) * position)
    held = forget + stab[layer]
    top = jnp.maximum(held, ingate)
    for other in range(layer):
        stab_new[other] = old[other]
    stab_new[layer] = top
    index = lax.broadcasted_iota(jnp.int32, top.shape, 0)
    mine = index == ids[1]
    decay = jnp.sum(jnp.where(mine, jnp.exp(held - top), 0.0), axis=0, keepdims=True)
    weight = jnp.sum(jnp.where(mine, jnp.exp(ingate - top), 0.0), axis=0, keepdims=True)
    factors[...] = jnp.where(index == 0, decay, weight).T
    batch, lanes = n.shape[0], columns.shape[1]
    v = both[:, :width].astype(BF16).astype(F32) * factors[:, 1:2]
    if lanes > batch:
        v = jnp.concatenate([v, jnp.zeros((lanes - batch, width), F32)], axis=0)
    columns[...] = v.T.astype(BF16)
    decays[...] = jnp.broadcast_to(factors[:, 0:1], decays.shape)


def read_kernel(
    layer,
    rows,
    memory,
    head_pair,
    pair,
    values,
    outgate,
    factors,
    all_sums,
    sums,
    gain,
    old,
    gated,
    sums_new,
    kept,
    query,
    arrived,
):
    batch, width, _ = kept.shape
    chunks = batch // rows

    def fetch(i):
        part = pl.ds(i * rows, rows)
        return pltpu.make_async_copy(memory.at[layer, part], kept.at[part], arrived.at[i])

    for i in range(chunks):
        fetch(i).start()
    q = head_pair[0].astype(F32)
    query[...] = q
    lanes = -(-batch // 128) * 128
    lane = lax.broadcasted_iota(jnp.int32, (width, lanes), 1)
    total = jnp.zeros((width, lanes), F32)

    def some(i, total):
        fetch(i).wait()
        for r in range(rows):
            b = i * rows + r
            product = kept[b] * query[pl.ds(b, 1), :]
            column = jnp.sum(product, axis=1, keepdims=True)
            total = jnp.where(lane == b, column, total)
        return total

    read = lax.fori_loop(0, chunks, some, total).T[:batch]
    decay, weight = factors[:, 0:1], factors[:, 1:2]
    match = weight * jnp.sum(head_pair[1].astype(F32) * q, axis=1, keepdims=True)
    v = values[...].astype(F32)
    numerator = decay * read + match * v
    below = decay * jnp.sum(all_sums[layer] * q, axis=1, keepdims=True) + match
    hidden = numerator / jnp.maximum(jnp.abs(below), 1.0)
    gate = jax.nn.sigmoid(outgate[...].astype(F32))
    gated[...] = (hidden * gain[layer : layer + 1].astype(F32) * gate).astype(BF16)
    for other in range(layer):
        sums_new[other] = old[other]
    sums_new[layer] = decay * sums[layer] + weight * pair[1].astype(F32)


def out_kernel(layer, masks, low, ids, near, far, current, wo, after, rows):
    place(ids[0], near, far, rows, masks, low)
    total = current[...].astype(F32) + dot(joined(rows), wo[layer])
    after[...] = total.astype(BF16)


def update_kernel(first, rows, kept, columns, decays, head_pair, _old, new):
    batch, width, depth = kept.shape
    lanes = columns.shape[1]
    keys = head_pair[1]
    if lanes > batch:
        keys = jnp.concatenate([keys, jnp.zeros((lanes - batch, depth), BF16)], axis=0)
    lane = lax.broadcasted_iota(jnp.int32, columns.shape, 1)
    at = first + pl.program_id(0) * rows
    all_columns = columns[...]
    chosen = [jnp.where(lane == at + r, all_columns, jnp.zeros_like(all_columns)) for r in range(rows)]
    outer = dot(jnp.concatenate(chosen, axis=0), keys)
    for r in range(rows):
        new[0, r] = decays[pl.ds(at + r, 1), :] * kept[at + r] + outer[r * width : (r + 1) * width]


def in_hbm(x):
    return pltpu.with_memory_space_constraint(x, pltpu.HBM)


def load_kernel(count, *refs):
    arrived = refs[-1]
    copies = [pltpu.make_async_copy(refs[i], refs[count + i], arrived.at[i]) for i in range(count)]
    for copy in copies:
        copy.start()
    for copy in copies:
        copy.wait()


def load(*arrays):
    return pl.pallas_call(
        functools.partial(load_kernel, len(arrays)),
        out_shape=tuple(pltpu.VMEM(a.shape, a.dtype) for a in arrays),
        in_specs=[HBM] * len(arrays),
        out_specs=(VM,) * len(arrays),
        scratch_shapes=[pltpu.SemaphoreType.DMA((len(arrays),))],
        compiler_params=pltpu.CompilerParams(vmem_limit_bytes=MIB),
        cost_estimate=pl.CostEstimate(flops=1 << 20, bytes_accessed=1 << 20, transcendentals=0),
    )(*(in_hbm(a) for a in arrays))


def body(
    tokens,
    lengths,
    cell_memory,
    key_sums,
    stabilizer,
    norm_gain,
    query_weight,
    key_weight,
    value_weight,
    outgate_weight,
    ingate_weight,
    forget_weight,
    ingate_bias,
    forget_bias,
    forget_slope,
    head_gain,
    output_weight,
):
    count = lax.axis_size("tp")
    blocks, batch, width, depth = cell_memory.shape
    heads = stabilizer.shape[2]
    split_count = count // heads
    own = lax.axis_index("tp")
    ids = jnp.stack([own, own // split_count]).astype(jnp.int32)

    def whole_head(value):
        axis = value.ndim - 1
        for level in range(split_count.bit_length() - 1):
            partner = swap(value, 1 << level)
            upper = own // (1 << level) % 2 == 1
            value = jnp.concatenate(
                (jnp.where(upper, partner, value), jnp.where(upper, value, partner)), axis=axis
            )
        return value

    near, far, masks, low = gather(tokens)
    (sums, wq, wk, wv, wg, wo, wi, wf, ibias, fbias, slope, at, stab, norm_gain, head_gain, current) = load(
        key_sums,
        query_weight,
        key_weight,
        value_weight,
        outgate_weight,
        output_weight,
        jnp.swapaxes(ingate_weight, 1, 2),
        jnp.swapaxes(forget_weight, 1, 2),
        ingate_bias,
        forget_bias,
        forget_slope,
        lengths[None],
        jnp.swapaxes(stabilizer, 1, 2),
        norm_gain,
        head_gain,
        tokens,
    )
    all_sums = whole_head(sums)
    shape = jax.ShapeDtypeStruct
    rows = 8 if batch % 8 == 0 else 1
    lanes = -(-batch // 128) * 128
    new_memory, new_sums, new_stab = ids, sums, stab
    for layer in range(blocks):
        if layer:
            near, far, masks, low = gather(current)
        pair, normed = call(
            functools.partial(heads_kernel, layer, masks, low, depth ** (-0.5)),
            (shape((2, batch, width), BF16), pltpu.VMEM((batch, count * width), BF16)),
            [SM] + [VM] * 5,
            (VM, VM),
            [pltpu.VMEM((count, batch, width), BF16)],
        )(ids, near, far, norm_gain, wq, wk)
        head_pair = whole_head(pair)
        values, outgate, factors, new_stab, columns, decays = call(
            functools.partial(gates_kernel, layer),
            (
                shape((batch, width), BF16),
                shape((batch, width), BF16),
                shape((batch, heads), F32),
                shape(stab.shape, F32),
                pltpu.VMEM((width, lanes), BF16),
                pltpu.VMEM((batch, depth), F32),
            ),
            [SM] + [VM] * 11,
            (VM,) * 6,
        )(ids, normed, wv, wg, wi, wf, ibias, fbias, slope, at, stab, new_stab)
        gated, new_sums, kept = call(
            functools.partial(read_kernel, layer, rows),
            (
                shape((batch, width), BF16),
                shape(sums.shape, F32),
                pltpu.VMEM((batch, width, depth), F32),
            ),
            [HBM] + [VM] * 9,
            (VM, VM, VM),
            [pltpu.VMEM((batch, depth), F32), pltpu.SemaphoreType.DMA((batch // rows,))],
        )(in_hbm(cell_memory), head_pair, pair, values, outgate, factors, all_sums, sums, head_gain, new_sums)

        near, far, masks, low = gather(gated)
        first = 0
        for part, size in enumerate(shares(batch // rows)):
            if not size:
                continue
            new_memory = pl.pallas_call(
                functools.partial(update_kernel, first * rows, rows),
                out_shape=shape(cell_memory.shape, F32),
                grid=(size,),
                in_specs=[VM] * 4 + [pl.BlockSpec(memory_space=pl.ANY)],
                out_specs=pl.BlockSpec(
                    (1, rows, width, depth),
                    lambda i, layer=layer, first=first: (layer, first + i, 0, 0),
                ),
                input_output_aliases={} if layer == part == 0 else {4: 0},
                compiler_params=pltpu.CompilerParams(vmem_limit_bytes=8 * MIB),
                cost_estimate=pl.CostEstimate(flops=1 << 22, bytes_accessed=1 << 20, transcendentals=0),
            )(kept, columns, decays, head_pair, new_memory)
            first += size

        current = call(
            functools.partial(out_kernel, layer, masks, low),
            shape((batch, width), BF16),
            [SM] + [VM] * 4,
            VM,
            [pltpu.VMEM((count, batch, width), BF16)],
        )(ids, near, far, current, wo)
    return current, new_memory, new_sums, jnp.swapaxes(new_stab, 1, 2)


def solution(mesh):
    in_specs = (
        P("grp", "tp"),
        P("grp"),
        P(None, "grp", "tp", None),
        P(None, "grp", "tp"),
        P(None, "grp", None),
        P(),
        P(None, None, "tp"),
        P(None, None, "tp"),
        P(None, None, "tp"),
        P(None, None, "tp"),
        P(),
        P(),
        P(),
        P(),
        P(),
        P(None, "tp"),
        P(None, None, "tp"),
    )
    out_specs = (
        P("grp", "tp"),
        P(None, "grp", "tp", None),
        P(None, "grp", "tp"),
        P(None, "grp", None),
    )

    return jax.shard_map(body, mesh=mesh, in_specs=in_specs, out_specs=out_specs, check_vma=False)
```

time: 134 us -> 91.5 us (0.68)
  blocking collectives: 80.6 us -> 0 us
  Pallas kernels: 0 us -> 35.3 us
  matrix products: 26.8 us -> 0 us
  starting transfers between devices: 1.15 us -> 27 us
  other arithmetic: 22.4 us -> 1.81 us
  waiting for transfers between devices: 0.01 us -> 17.9 us
  local copies, waits for them, and re-layouts: 1.58 us -> 8.32 us
    all_gather x4 -> x0, blocking collectives: 80.6 us -> none  [the longest x2 43.9 us: body(): gathered_rows = lax.all_gather(current, 'tp', axis=1, tiled=True)]
    pallas_call x0 -> x15, Pallas kernels: none -> 35.3 us  [the longest x6 15.6 us: body(): pl.pallas_call(functools.partial(update_kernel, first * rows, rows), out_...]
    dot_general x16 -> x0, matrix products: 26.8 us -> none  [the longest x2 17.2 us: body(): jnp.einsum('bvk,bk->bv', mem_new, head_query, precision=lax.Precision.HIG...]
    ppermute x4 -> x23, starting transfers between devices: 1.15 us -> 27 us  [swap(): lax.ppermute(value, 'tp', [(s, s ^ mask) for s in range(lax.axis_size('tp...]
    ppermute x4 -> x23, waiting for transfers between devices: 0.01 us -> 17.9 us  [swap(): lax.ppermute(value, 'tp', [(s, s ^ mask) for s in range(lax.axis_size('tp...]
    add x1 -> x0, other arithmetic: 10.3 us -> none  [body(): decay_own[:, None, None] * cell_memory[block_id]]
    another operation x5 -> x1, other arithmetic: 9.26 us -> 0.07 us  [body(): ids = jnp.stack([own, own // split_count]).astype(jnp.int32)]
    unnamed x20 -> x42, local copies, waits for them, and re-layouts: 0.05 us -> 8.28 us
  transfers between devices with their start and end apart: 4 -> 23, of which waited for: 0 -> 16; matrix products, arithmetic and copies ran while one was open for 3% -> 4% of each run, Pallas kernels for 0% -> 20%
where the time goes in v1:
time: 91.5 us; the launch traced here: 91.1 us
  Pallas kernels  35.3 us (39%)
  starting transfers between devices  27 us (30%)
  waiting for transfers between devices  17.9 us (20%)
  local copies, waits for them, and re-layouts  8.32 us (9%)
  other arithmetic  1.81 us (2%)
    ppermute x23, starting transfers between devices, swap(): lax.ppermute(value, 'tp', [(s, s ^ mask) for s in range(lax.axis_size('tp...  27 us
    ppermute x23, waiting for transfers between devices, swap(): lax.ppermute(value, 'tp', [(s, s ^ mask) for s in range(lax.axis_size('tp...  17.9 us
    pallas_call x6, Pallas kernels, body(): pl.pallas_call(functools.partial(update_kernel, first * rows, rows), out_...  15.6 us
    pallas_call x2, Pallas kernels, body(): call(functools.partial(read_kernel, layer, rows), (shape((batch, width),...  9.81 us
    unnamed x42, local copies, waits for them, and re-layouts  8.28 us
    pallas_call x2, Pallas kernels, body(): call(functools.partial(gates_kernel, layer), (shape((batch, width), BF16)...  2.93 us
    pallas_call x1, Pallas kernels, load(): pl.pallas_call(functools.partial(load_kernel, len(arrays)), out_shape=tup...  2.72 us
    pallas_call x2, Pallas kernels, body(): call(functools.partial(out_kernel, layer, masks, low), shape((batch, widt...  2.21 us
  transfers between devices with their start and end apart: 23, of which 16 were waited for; matrix products, arithmetic and copies ran while one was open for 4% of the time, Pallas kernels for 20%

profile of v1, /device:TPU:0, one launch (start us, length us, event | category | flops | bytes accessed | tf_op | source)
XLA Modules:
  0.0 91.1 jit_solution(9825908725435852410)
XLA Ops:
  0.6 2.7 %shard_map.192 = (f32[2,80,128]{2,1,0:T(8,128)S(1)}, bf16[2,2048,128]{2,1,0:T(8,128)(2,1)S(1)}, bf16[2,2048,128]{2,1,0:T(8,128)(2,1)S(1)}, bf16[2,2048,128]{2,1,...) custom-call(f32[2,80,128]{2,1,0:T(8,128)} %refs_0_.1, ...), custom_call_target="tpu_custom_call" | custom-call | flops 1048576 | bytes 1048576 | tf_op jit(solution)/shard_map/pallas_call | solution.py:234
  3.4 1.0 %copy-done = bf16[2,2048,128]{2,1,0:T(8,128)(2,1)} copy-done((bf16[2,2048,128]{2,1,0:T(8,128)(2,1)}, bf16[2,2048,128]{2,1,0:T(8,128)(2,1)S(1)}, u32[]{:S(2)}) %copy-start) | copy-done | bytes 1048600
  4.3 1.0 %copy-done.3 = bf16[2,2048,128]{2,1,0:T(8,128)(2,1)} copy-done((bf16[2,2048,128]{2,1,0:T(8,128)(2,1)}, bf16[2,2048,128]{2,1,0:T(8,128)(2,1)S(1)}, u32[]{:S(2)}) %copy-start.3) | copy-done | bytes 1048600
  5.3 0.6 copy-done.6
  5.9 0.5 copy-done.10
  6.4 0.5 collective-permute-start.6
  6.9 3.7 %collective-permute-start = (bf16[1,80,128]{2,1,0:T(8,128)(2,1)}, bf16[1,80,128]{2,1,0:T(8,128)(2,1)}, u32[]{:S(2)}, u32[]{:S(2)}) collective-permute-start(bf16[1,80,128]{2,1,0:T(8,128)(2,1)} %bitcast.21), channel_id=1, source_target_pairs={{0,9},{1,8},{2,11},{3,10},{4,13},{5,12},{6,15},{7,14},{8,1},{9,0},... | collective-permute-start | bytes 61448 | tf_op jit(solution)/shard_map/ppermute | solution.py:41
  10.6 0.8 constant_dynamic-update-slice_fusion.4
  11.4 1.0 %collective-permute-done = bf16[1,80,128]{2,1,0:T(8,128)(2,1)} collective-permute-done((bf16[1,80,128]{2,1,0:T(8,128)(2,1)}, bf16[1,80,128]{2,1,0:T(8,128)(2,1)}, u32[]{:S(2)}, u32[]{:S(2)}) %collective-permute-start) | collective-permute-done | bytes 20512 | tf_op jit(solution)/shard_map/ppermute | solution.py:41
  12.4 0.8 pad_maximum_fusion.3
  13.2 2.5 %collective-permute-start.1 = (bf16[2,80,128]{2,1,0:T(8,128)(2,1)S(1)}, bf16[2,80,128]{2,1,0:T(8,128)(2,1)S(1)}, u32[]{:S(2)}, u32[]{:S(2)}) collective-permute-start(bf16[2,80,128]{2,1,0:T(8,128)(2,1)S(1)} %pad_maximum_fusion.3), channel_id=1, source_target_pairs={{0,6},{1,7},{2,4},{3,5},{4,2},{5,3},{6,0},{7,1},{8,14},{9,15},{10,... | collective-permute-start | bytes 122888 | tf_op jit(solution)/shard_map/ppermute | solution.py:41
  15.7 0.3 collective-permute-start.2
  15.9 0.4 collective-permute-start.3
  16.4 0.7 constant_dynamic-update-slice_fusion.3
  17.1 1.0 %collective-permute-done.1 = bf16[2,80,128]{2,1,0:T(8,128)(2,1)S(1)} collective-permute-done((bf16[2,80,128]{2,1,0:T(8,128)(2,1)S(1)}, bf16[2,80,128]{2,1,0:T(8,128)(2,1)S(1)}, u32[]{:S(2)}, u32[]{:S(2)}) %collective-permute-start.1) | collective-permute-done | bytes 40992 | tf_op jit(solution)/shard_map/ppermute | solution.py:41
  18.1 1.1 %collective-permute-done.2 = bf16[2,80,128]{2,1,0:T(8,128)(2,1)S(1)} collective-permute-done((bf16[2,80,128]{2,1,0:T(8,128)(2,1)S(1)}, bf16[2,80,128]{2,1,0:T(8,128)(2,1)S(1)}, u32[]{:S(2)}, u32[]{:S(2)}) %collective-permute-start.2) | collective-permute-done | bytes 40992 | tf_op jit(solution)/shard_map/ppermute | solution.py:41
  19.2 0.2 collective-permute-done.3
  19.4 0.4 collective-permute-start.4
  19.8 0.9 broadcast_select_fusion.3
  20.8 1.2 %copy-done.1 = bf16[2,2048,128]{2,1,0:T(8,128)(2,1)S(1)} copy-done((bf16[2,2048,128]{2,1,0:T(8,128)(2,1)S(1)}, bf16[2,2048,128]{2,1,0:T(8,128)(2,1)}, u32[]{:S(2)}) %copy-start.1) | copy-done | bytes 1048600
  22.1 1.2 %copy-done.4 = bf16[2,2048,128]{2,1,0:T(8,128)(2,1)S(1)} copy-done((bf16[2,2048,128]{2,1,0:T(8,128)(2,1)S(1)}, bf16[2,2048,128]{2,1,0:T(8,128)(2,1)}, u32[]{:S(2)}) %copy-start.4) | copy-done | bytes 1048600
  23.3 1.0 %shard_map.193 = (bf16[2,80,128]{2,1,0:T(8,128)(2,1)S(1)}, bf16[80,2048]{1,0:T(8,128)(2,1)S(1)}) custom-call(s32[2]{0:T(128)S(1)} %pad_add_fusion.ids._old, bf16[8,80,128]{2,1,0:T(8,128)(2,1)S(1)} %constant_dynamic-update-slice_fusion.near, bf16[8,80,128]{2,1,0:T(8,128)(2,1)S(1)} %collective-permute-done.4.far, bf16[2,2048]{1,0:T(2,128)(2,1)S(1)} %get-tuple-element.42.gain, ...), custom_call_target="tpu_custom_call" | custom-call | flops 1048576 | bytes 1048576 | tf_op jit(solution)/shard_map/pallas_call | solution.py:308
  24.3 0.4 collective-permute-start.5
  24.7 0.6 copy-done.11
  25.3 1.3 %shard_map.194 = (bf16[80,128]{1,0:T(8,128)(2,1)S(1)}, bf16[80,128]{1,0:T(8,128)(2,1)S(1)}, f32[80,8]{1,0:T(8,128)S(1)}, f32[2,8,80]{2,1,0:T(8,128)S(1)}, bf16[1...) custom-call(s32[2]{0:T(128)S(1)} %pad_add_fusion.ids._old, bf16[80,2048]{1,0:T(8,128)(2,1)S(1)} %get-tuple-element.46.normed, ...), custom_call_target="tpu_custom_call" | custom-call | flops 1048576 | bytes 1048576 | tf_op jit(solution)/shard_map/pallas_call | solution.py:316
  26.6 0.6 copy-done.9
  27.2 4.6 %shard_map.195 = (bf16[80,128]{1,0:T(8,128)(2,1)S(1)}, f32[2,80,128]{2,1,0:T(8,128)S(1)}, f32[80,128,256]{2,1,0:T(8,128)S(1)}) custom-call(f32[2,80,128,256]{3,2,1,0:T(8,128)} %memory.3, bf16[2,80,256]{2,1,0:T(8,128)(2,1)S(1)} %pad_maximum_fusion.1.head_pair, bf16[2,80,128]{2,1,0:T(8,128)(2,1)S(1)} %get-tuple-element.45.pair, ...), custom_call_target="tpu_custom_call" | custom-call | flops 1048576 | bytes 1048576 | tf_op jit(solution)/shard_map/pallas_call | solution.py:329
  31.8 2.5 %collective-permute-start.7 = (bf16[1,80,128]{2,1,0:T(8,128)(2,1)S(1)}, bf16[1,80,128]{2,1,0:T(8,128)(2,1)S(1)}, u32[]{:S(2)}, u32[]{:S(2)}) collective-permute-start(bf16[1,80,128]{2,1,0:T(8,128)(2,1)S(1)} %bitcast.19), channel_id=1, source_target_pairs={{0,9},{1,8},{2,11},{3,10},{4,13},{5,12},{6,15},{7,14},{8,1},{9,0},... | collective-permute-start | bytes 61448 | tf_op jit(solution)/shard_map/ppermute | solution.py:41
  34.3 1.6 %collective-permute-done.7 = bf16[1,80,128]{2,1,0:T(8,128)(2,1)S(1)} collective-permute-done((bf16[1,80,128]{2,1,0:T(8,128)(2,1)S(1)}, bf16[1,80,128]{2,1,0:T(8,128)(2,1)S(1)}, u32[]{:S(2)}, u32[]{:S(2)}) %collective-permute-start.7) | collective-permute-done | bytes 20512 | tf_op jit(solution)/shard_map/ppermute | solution.py:41
  36.0 1.4 %collective-permute-start.8 = (bf16[2,80,128]{2,1,0:T(8,128)(2,1)S(1)}, bf16[2,80,128]{2,1,0:T(8,128)(2,1)S(1)}, u32[]{:S(2)}, u32[]{:S(2)}) collective-permute-start(bf16[2,80,128]{2,1,0:T(8,128)(2,1)S(1)} %pad_maximum_fusion.4), channel_id=1, source_target_pairs={{0,6},{1,7},{2,4},{3,5},{4,2},{5,3},{6,0},{7,1},{8,14},{9,15},{10,... | collective-permute-start | bytes 122888 | tf_op jit(solution)/shard_map/ppermute | solution.py:41
  37.4 0.5 collective-permute-start.9
  37.8 1.3 %collective-permute-start.10 = (bf16[2,80,128]{2,1,0:T(8,128)(2,1)S(1)}, bf16[2,80,128]{2,1,0:T(8,128)(2,1)S(1)}, u32[]{:S(2)}, u32[]{:S(2)}) collective-permute-start(bf16[2,80,128]{2,1,0:T(8,128)(2,1)S(1)} %pad_maximum_fusion.4), channel_id=1, source_target_pairs={{0,5},{1,4},{2,7},{3,6},{4,1},{5,0},{6,3},{7,2},{8,13},{9,12},{10,... | collective-permute-start | bytes 122888 | tf_op jit(solution)/shard_map/ppermute | solution.py:41
  39.2 1.7 %collective-permute-done.8 = bf16[2,80,128]{2,1,0:T(8,128)(2,1)S(1)} collective-permute-done((bf16[2,80,128]{2,1,0:T(8,128)(2,1)S(1)}, bf16[2,80,128]{2,1,0:T(8,128)(2,1)S(1)}, u32[]{:S(2)}, u32[]{:S(2)}) %collective-permute-start.8) | collective-permute-done | bytes 40992 | tf_op jit(solution)/shard_map/ppermute | solution.py:41
  40.9 0.8 collective-permute-done.9
  41.8 0.2 collective-permute-start.11
  42.0 1.3 %collective-permute-done.11.far = bf16[8,80,128]{2,1,0:T(8,128)(2,1)S(1)} collective-permute-done((bf16[8,80,128]{2,1,0:T(8,128)(2,1)S(1)}, bf16[8,80,128]{2,1,0:T(8,128)(2,1)S(1)}, u32[]{:S(2)}, u32[]{:S(2)}) %collective-permute-start.11) | collective-permute-done | bytes 163872 | tf_op jit(solution)/shard_map/ppermute | solution.py:41
  43.2 0.8 shard_map.196.current
  44.0 2.5 %collective-permute-start.12 = (bf16[1,80,128]{2,1,0:T(8,128)(2,1)S(1)}, bf16[1,80,128]{2,1,0:T(8,128)(2,1)S(1)}, u32[]{:S(2)}, u32[]{:S(2)}) collective-permute-start(bf16[1,80,128]{2,1,0:T(8,128)(2,1)S(1)} %bitcast.15), channel_id=1, source_target_pairs={{0,9},{1,8},{2,11},{3,10},{4,13},{5,12},{6,15},{7,14},{8,1},{9,0},... | collective-permute-start | bytes 61448 | tf_op jit(solution)/shard_map/ppermute | solution.py:41
  46.5 1.7 %collective-permute-done.12 = bf16[1,80,128]{2,1,0:T(8,128)(2,1)S(1)} collective-permute-done((bf16[1,80,128]{2,1,0:T(8,128)(2,1)S(1)}, bf16[1,80,128]{2,1,0:T(8,128)(2,1)S(1)}, u32[]{:S(2)}, u32[]{:S(2)}) %collective-permute-start.12) | collective-permute-done | bytes 20512 | tf_op jit(solution)/shard_map/ppermute | solution.py:41
  48.2 1.9 %collective-permute-start.13 = (bf16[2,80,128]{2,1,0:T(8,128)(2,1)S(1)}, bf16[2,80,128]{2,1,0:T(8,128)(2,1)S(1)}, u32[]{:S(2)}, u32[]{:S(2)}) collective-permute-start(bf16[2,80,128]{2,1,0:T(8,128)(2,1)S(1)} %pad_maximum_fusion.5), channel_id=1, source_target_pairs={{0,6},{1,7},{2,4},{3,5},{4,2},{5,3},{6,0},{7,1},{8,14},{9,15},{10,... | collective-permute-start | bytes 122888 | tf_op jit(solution)/shard_map/ppermute | solution.py:41
  50.3 1.2 %collective-permute-start.15 = (bf16[2,80,128]{2,1,0:T(8,128)(2,1)S(1)}, bf16[2,80,128]{2,1,0:T(8,128)(2,1)S(1)}, u32[]{:S(2)}, u32[]{:S(2)}) collective-permute-start(bf16[2,80,128]{2,1,0:T(8,128)(2,1)S(1)} %pad_maximum_fusion.5), channel_id=1, source_target_pairs={{0,5},{1,4},{2,7},{3,6},{4,1},{5,0},{6,3},{7,2},{8,13},{9,12},{10,... | collective-permute-start | bytes 122888 | tf_op jit(solution)/shard_map/ppermute | solution.py:41
  51.4 1.7 %collective-permute-done.13 = bf16[2,80,128]{2,1,0:T(8,128)(2,1)S(1)} collective-permute-done((bf16[2,80,128]{2,1,0:T(8,128)(2,1)S(1)}, bf16[2,80,128]{2,1,0:T(8,128)(2,1)S(1)}, u32[]{:S(2)}, u32[]{:S(2)}) %collective-permute-start.13) | collective-permute-done | bytes 40992 | tf_op jit(solution)/shard_map/ppermute | solution.py:41
  53.1 0.6 collective-permute-done.14
  53.8 0.6 collective-permute-start.16
  54.4 1.0 %collective-permute-done.16.far = bf16[8,80,128]{2,1,0:T(8,128)(2,1)S(1)} collective-permute-done((bf16[8,80,128]{2,1,0:T(8,128)(2,1)S(1)}, bf16[8,80,128]{2,1,0:T(8,128)(2,1)S(1)}, u32[]{:S(2)}, u32[]{:S(2)}) %collective-permute-start.16) | collective-permute-done | bytes 163872 | tf_op jit(solution)/shard_map/ppermute | solution.py:41
  55.4 1.0 %shard_map.197 = (bf16[2,80,128]{2,1,0:T(8,128)(2,1)S(1)}, bf16[80,2048]{1,0:T(8,128)(2,1)S(1)}) custom-call(s32[2]{0:T(128)S(1)} %pad_add_fusion.ids._old, bf16[8,80,128]{2,1,0:T(8,128)(2,1)S(1)} %constant_dynamic-update-slice_fusion.10.near, bf16[8,80,128]{2,1,0:T(8,128)(2,1)S(1)} %collective-permute-done.16.far, ...), custom_call_target="tpu_custom_call" | custom-call | flops 1048576 | bytes 1048576 | tf_op jit(solution)/shard_map/pallas_call | solution.py:308
  56.4 0.4 collective-permute-start.17
  56.9 1.6 %shard_map.198 = (bf16[80,128]{1,0:T(8,128)(2,1)S(1)}, bf16[80,128]{1,0:T(8,128)(2,1)S(1)}, f32[80,8]{1,0:T(8,128)S(1)}, f32[2,8,80]{2,1,0:T(8,128)}, bf16[128,1...) custom-call(s32[2]{0:T(128)S(1)} %pad_add_fusion.ids._old, bf16[80,2048]{1,0:T(8,128)(2,1)S(1)} %get-tuple-element.65.normed, ...), custom_call_target="tpu_custom_call" | custom-call | flops 1048576 | bytes 1048576 | tf_op jit(solution)/shard_map/pallas_call | solution.py:316
  58.5 5.2 %shard_map.199 = (bf16[80,128]{1,0:T(8,128)(2,1)S(1)}, f32[2,80,128]{2,1,0:T(8,128)}, f32[80,128,256]{2,1,0:T(8,128)S(1)}) custom-call(f32[2,80,128,256]{3,2,1,0:T(8,128)} %memory.3, bf16[2,80,256]{2,1,0:T(8,128)(2,1)S(1)} %pad_maximum_fusion.2.head_pair, bf16[2,80,128]{2,1,0:T(8,128)(2,1)S(1)} %get-tuple-element.64.pair, ...), custom_call_target="tpu_custom_call" | custom-call | flops 1048576 | bytes 1048576 | tf_op jit(solution)/shard_map/pallas_call | solution.py:329
  63.8 2.7 %collective-permute-start.18 = (bf16[1,80,128]{2,1,0:T(8,128)(2,1)S(1)}, bf16[1,80,128]{2,1,0:T(8,128)(2,1)S(1)}, u32[]{:S(2)}, u32[]{:S(2)}) collective-permute-start(bf16[1,80,128]{2,1,0:T(8,128)(2,1)S(1)} %bitcast.17), channel_id=1, source_target_pairs={{0,9},{1,8},{2,11},{3,10},{4,13},{5,12},{6,15},{7,14},{8,1},{9,0},... | collective-permute-start | bytes 61448 | tf_op jit(solution)/shard_map/ppermute | solution.py:41
  66.5 1.5 %collective-permute-done.18 = bf16[1,80,128]{2,1,0:T(8,128)(2,1)S(1)} collective-permute-done((bf16[1,80,128]{2,1,0:T(8,128)(2,1)S(1)}, bf16[1,80,128]{2,1,0:T(8,128)(2,1)S(1)}, u32[]{:S(2)}, u32[]{:S(2)}) %collective-permute-start.18) | collective-permute-done | bytes 20512 | tf_op jit(solution)/shard_map/ppermute | solution.py:41
  68.0 1.7 %collective-permute-start.19 = (bf16[2,80,128]{2,1,0:T(8,128)(2,1)S(1)}, bf16[2,80,128]{2,1,0:T(8,128)(2,1)S(1)}, u32[]{:S(2)}, u32[]{:S(2)}) collective-permute-start(bf16[2,80,128]{2,1,0:T(8,128)(2,1)S(1)} %pad_maximum_fusion.6), channel_id=1, source_target_pairs={{0,6},{1,7},{2,4},{3,5},{4,2},{5,3},{6,0},{7,1},{8,14},{9,15},{10,... | collective-permute-start | bytes 122888 | tf_op jit(solution)/shard_map/ppermute | solution.py:41
  69.7 0.4 collective-permute-start.20
  70.0 1.1 %collective-permute-start.21 = (bf16[2,80,128]{2,1,0:T(8,128)(2,1)S(1)}, bf16[2,80,128]{2,1,0:T(8,128)(2,1)S(1)}, u32[]{:S(2)}, u32[]{:S(2)}) collective-permute-start(bf16[2,80,128]{2,1,0:T(8,128)(2,1)S(1)} %pad_maximum_fusion.6), channel_id=1, source_target_pairs={{0,5},{1,4},{2,7},{3,6},{4,1},{5,0},{6,3},{7,2},{8,13},{9,12},{10,... | collective-permute-start | bytes 122888 | tf_op jit(solution)/shard_map/ppermute | solution.py:41
  71.2 1.7 %collective-permute-done.19 = bf16[2,80,128]{2,1,0:T(8,128)(2,1)S(1)} collective-permute-done((bf16[2,80,128]{2,1,0:T(8,128)(2,1)S(1)}, bf16[2,80,128]{2,1,0:T(8,128)(2,1)S(1)}, u32[]{:S(2)}, u32[]{:S(2)}) %collective-permute-start.19) | collective-permute-done | bytes 40992 | tf_op jit(solution)/shard_map/ppermute | solution.py:41
  72.9 0.8 collective-permute-done.20
  73.8 0.3 collective-permute-start.22
  74.1 2.5 %shard_map.201._old = f32[2,80,128,256]{3,2,1,0:T(8,128)} custom-call(f32[80,128,256]{2,1,0:T(8,128)S(1)} %get-tuple-element.75.kept, bf16[128,128]{1,0:T(8,128)(2,1)S(1)} %get-tuple-element.76.columns, f32[80,256]{1,0:T(8,128)S(1)} %get-tuple-element.77.decays, bf16[2,80,256]{2,1,0:T(8,128)(2,1)S(1)} %pad_maximum_fusion.1.head_pair, s32[2]{0:T(128)S(1)} %pad_add_fusion.ids._old), custom_call_target="tpu_custom_call" | custom-call | flops 4194304 | bytes 1048576 | tf_op jit(solution)/shard_map/pallas_call | solution.py:346
  76.6 2.8 %shard_map.202._old = f32[2,80,128,256]{3,2,1,0:T(8,128)} custom-call(f32[80,128,256]{2,1,0:T(8,128)S(1)} %get-tuple-element.75.kept, bf16[128,128]{1,0:T(8,128)(2,1)S(1)} %get-tuple-element.76.columns, f32[80,256]{1,0:T(8,128)S(1)} %get-tuple-element.77.decays, bf16[2,80,256]{2,1,0:T(8,128)(2,1)S(1)} %pad_maximum_fusion.1.head_pair, ...), custom_call_target="tpu_custom_call", output_to_operand_aliasing={{}: (4, {})} | custom-call | flops 4194304 | bytes 1048576 | tf_op jit(solution)/shard_map/pallas_call | solution.py:346
  79.4 2.5 %shard_map.203._old = f32[2,80,128,256]{3,2,1,0:T(8,128)} custom-call(f32[80,128,256]{2,1,0:T(8,128)S(1)} %get-tuple-element.75.kept, bf16[128,128]{1,0:T(8,128)(2,1)S(1)} %get-tuple-element.76.columns, f32[80,256]{1,0:T(8,128)S(1)} %get-tuple-element.77.decays, bf16[2,80,256]{2,1,0:T(8,128)(2,1)S(1)} %pad_maximum_fusion.1.head_pair, ...), custom_call_target="tpu_custom_call", output_to_operand_aliasing={{}: (4, {})} | custom-call | flops 4194304 | bytes 1048576 | tf_op jit(solution)/shard_map/pallas_call | solution.py:346
  81.9 2.5 %shard_map.204._old = f32[2,80,128,256]{3,2,1,0:T(8,128)} custom-call(f32[80,128,256]{2,1,0:T(8,128)S(1)} %get-tuple-element.72.kept, bf16[128,128]{1,0:T(8,128)(2,1)S(1)} %get-tuple-element.73.columns, f32[80,256]{1,0:T(8,128)S(1)} %get-tuple-element.74.decays, bf16[2,80,256]{2,1,0:T(8,128)(2,1)S(1)} %pad_maximum_fusion.2.head_pair, ...), custom_call_target="tpu_custom_call", output_to_operand_aliasing={{}: (4, {})} | custom-call | flops 4194304 | bytes 1048576 | tf_op jit(solution)/shard_map/pallas_call | solution.py:346
  84.4 2.8 %shard_map.205._old = f32[2,80,128,256]{3,2,1,0:T(8,128)} custom-call(f32[80,128,256]{2,1,0:T(8,128)S(1)} %get-tuple-element.72.kept, bf16[128,128]{1,0:T(8,128)(2,1)S(1)} %get-tuple-element.73.columns, f32[80,256]{1,0:T(8,128)S(1)} %get-tuple-element.74.decays, bf16[2,80,256]{2,1,0:T(8,128)(2,1)S(1)} %pad_maximum_fusion.2.head_pair, ...), custom_call_target="tpu_custom_call", output_to_operand_aliasing={{}: (4, {})} | custom-call | flops 4194304 | bytes 1048576 | tf_op jit(solution)/shard_map/pallas_call | solution.py:346
  87.2 2.5 %shard_map.206 = f32[2,80,128,256]{3,2,1,0:T(8,128)} custom-call(f32[80,128,256]{2,1,0:T(8,128)S(1)} %get-tuple-element.72.kept, bf16[128,128]{1,0:T(8,128)(2,1)S(1)} %get-tuple-element.73.columns, f32[80,256]{1,0:T(8,128)S(1)} %get-tuple-element.74.decays, bf16[2,80,256]{2,1,0:T(8,128)(2,1)S(1)} %pad_maximum_fusion.2.head_pair, ...), custom_call_target="tpu_custom_call", output_to_operand_aliasing={{}: (4, {})} | custom-call | flops 4194304 | bytes 1048576 | tf_op jit(solution)/shard_map/pallas_call | solution.py:346
  89.7 1.4 %shard_map.200 = bf16[80,128]{1,0:T(8,128)(2,1)} custom-call(s32[2]{0:T(128)S(1)} %pad_add_fusion.ids._old, bf16[8,80,128]{2,1,0:T(8,128)(2,1)S(1)} %constant_dynamic-update-slice_fusion.15.near, bf16[8,80,128]{2,1,0:T(8,128)(2,1)S(1)} %collective-permute-done.22.far, bf16[80,128]{1,0:T(8,128)(2,1)S(1)} %shard_map.196.current, ...), custom_call_target="tpu_custom_call" | custom-call | flops 1048576 | bytes 1048576 | tf_op jit(solution)/shard_map/pallas_call | solution.py:361
  (54 shorter events, 0.6 us)
Async XLA Ops:
  3.4 1.0 %copy-start = (bf16[2,2048,128]{2,1,0:T(8,128)(2,1)}, bf16[2,2048,128]{2,1,0:T(8,128)(2,1)S(1)}, u32[]{:S(2)}) copy-start(bf16[2,2048,128]{2,1,0:T(8,128)(2,1)S(1)} %get-tuple-element.43.wq) | copy-start | bytes 3145732
  4.3 1.0 %copy-start.3 = (bf16[2,2048,128]{2,1,0:T(8,128)(2,1)}, bf16[2,2048,128]{2,1,0:T(8,128)(2,1)S(1)}, u32[]{:S(2)}) copy-start(bf16[2,2048,128]{2,1,0:T(8,128)(2,1)S(1)} %get-tuple-element.44.wk) | copy-start | bytes 3145732
  5.3 0.6 copy-start.6
  5.9 0.5 copy-start.10
  6.4 4.9 %copy-start.8 = (bf16[2,128]{1,0:T(2,128)(2,1)}, bf16[2,128]{1,0:T(2,128)(2,1)S(1)}, u32[]{:S(2)}) copy-start(bf16[2,128]{1,0:T(2,128)(2,1)S(1)} %get-tuple-element.60.gain) | copy-start | bytes 1540
  6.4 13.4 %collective-permute-start.6 = (f32[2,80,128]{2,1,0:T(8,128)S(1)}, f32[2,80,128]{2,1,0:T(8,128)}, u32[]{:S(2)}, u32[]{:S(2)}) collective-permute-start(f32[2,80,128]{2,1,0:T(8,128)S(1)} %get-tuple-element.59.sums.old), channel_id=1, source_target_pairs={{0,1},{1,0},{2,3},{3,2},{4,5},{5,4},{6,7},{7,6},{8,9},{9,8},{10,11... | collective-permute-start | bytes 245768 | tf_op jit(solution)/shard_map/ppermute | solution.py:41
  6.9 5.5 %collective-permute-start = (bf16[1,80,128]{2,1,0:T(8,128)(2,1)}, bf16[1,80,128]{2,1,0:T(8,128)(2,1)}, u32[]{:S(2)}, u32[]{:S(2)}) collective-permute-start(bf16[1,80,128]{2,1,0:T(8,128)(2,1)} %bitcast.21), channel_id=1, source_target_pairs={{0,9},{1,8},{2,11},{3,10},{4,13},{5,12},{6,15},{7,14},{8,1},{9,0},... | collective-permute-start | bytes 61448 | tf_op jit(solution)/shard_map/ppermute | solution.py:41
  11.4 31.8 %copy-start.7 = (bf16[80,128]{1,0:T(8,128)(2,1)S(1)}, bf16[80,128]{1,0:T(8,128)(2,1)}, u32[]{:S(2)}) copy-start(bf16[80,128]{1,0:T(8,128)(2,1)} %copy-done.6) | copy-start | bytes 61444
  11.4 45.4 %copy-start.12 = (s32[1,80]{1,0:T(1,128)S(1)}, s32[1,80]{1,0:T(1,128)}, u32[]{:S(2)}) copy-start(s32[1,80]{1,0:T(1,128)} %copy-done.10) | copy-start | bytes 964
  13.2 4.9 %collective-permute-start.1 = (bf16[2,80,128]{2,1,0:T(8,128)(2,1)S(1)}, bf16[2,80,128]{2,1,0:T(8,128)(2,1)S(1)}, u32[]{:S(2)}, u32[]{:S(2)}) collective-permute-start(bf16[2,80,128]{2,1,0:T(8,128)(2,1)S(1)} %pad_maximum_fusion.3), channel_id=1, source_target_pairs={{0,6},{1,7},{2,4},{3,5},{4,2},{5,3},{6,0},{7,1},{8,14},{9,15},{10,... | collective-permute-start | bytes 122888 | tf_op jit(solution)/shard_map/ppermute | solution.py:41
  15.7 3.5 %collective-permute-start.2 = (bf16[2,80,128]{2,1,0:T(8,128)(2,1)S(1)}, bf16[2,80,128]{2,1,0:T(8,128)(2,1)S(1)}, u32[]{:S(2)}, u32[]{:S(2)}) collective-permute-start(bf16[2,80,128]{2,1,0:T(8,128)(2,1)S(1)} %pad_maximum_fusion.3), channel_id=1, source_target_pairs={{0,3},{1,2},{2,1},{3,0},{4,7},{5,6},{6,5},{7,4},{8,11},{9,10},{10,... | collective-permute-start | bytes 122888 | tf_op jit(solution)/shard_map/ppermute | solution.py:41
  15.9 3.4 %collective-permute-start.3 = (bf16[2,80,128]{2,1,0:T(8,128)(2,1)S(1)}, bf16[2,80,128]{2,1,0:T(8,128)(2,1)S(1)}, u32[]{:S(2)}, u32[]{:S(2)}) collective-permute-start(bf16[2,80,128]{2,1,0:T(8,128)(2,1)S(1)} %pad_maximum_fusion.3), channel_id=1, source_target_pairs={{0,5},{1,4},{2,7},{3,6},{4,1},{5,0},{6,3},{7,2},{8,13},{9,12},{10,... | collective-permute-start | bytes 122888 | tf_op jit(solution)/shard_map/ppermute | solution.py:41
  19.4 1.5 %collective-permute-start.4 = (bf16[8,80,128]{2,1,0:T(8,128)(2,1)S(1)}, bf16[8,80,128]{2,1,0:T(8,128)(2,1)S(1)}, u32[]{:S(2)}, u32[]{:S(2)}) collective-permute-start(bf16[8,80,128]{2,1,0:T(8,128)(2,1)S(1)} %constant_dynamic-update-slice_fusion.near), channel_id=1, source_target_pairs={{0,1},{1,0},{2,3},{3,2},{4,5},{5,4},{6,7},{7,6},{8,9},{9,8},{10,11... | collective-permute-start | bytes 491528 | tf_op jit(solution)/shard_map/ppermute | solution.py:41
  20.8 1.2 %copy-start.1 = (bf16[2,2048,128]{2,1,0:T(8,128)(2,1)S(1)}, bf16[2,2048,128]{2,1,0:T(8,128)(2,1)}, u32[]{:S(2)}) copy-start(bf16[2,2048,128]{2,1,0:T(8,128)(2,1)} %copy-done) | copy-start | bytes 3145732
  22.1 1.2 %copy-start.4 = (bf16[2,2048,128]{2,1,0:T(8,128)(2,1)S(1)}, bf16[2,2048,128]{2,1,0:T(8,128)(2,1)}, u32[]{:S(2)}) copy-start(bf16[2,2048,128]{2,1,0:T(8,128)(2,1)} %copy-done.3) | copy-start | bytes 3145732
  23.3 32.1 %copy-start.2 = (bf16[2,2048,128]{2,1,0:T(8,128)(2,1)S(1)}, bf16[2,2048,128]{2,1,0:T(8,128)(2,1)}, u32[]{:S(2)}) copy-start(bf16[2,2048,128]{2,1,0:T(8,128)(2,1)} %copy-done) | copy-start | bytes 3145732
  23.3 32.1 %copy-start.5 = (bf16[2,2048,128]{2,1,0:T(8,128)(2,1)S(1)}, bf16[2,2048,128]{2,1,0:T(8,128)(2,1)}, u32[]{:S(2)}) copy-start(bf16[2,2048,128]{2,1,0:T(8,128)(2,1)} %copy-done.3) | copy-start | bytes 3145732
  24.3 2.3 %collective-permute-start.5 = (bf16[2,80,128]{2,1,0:T(8,128)(2,1)S(1)}, bf16[2,80,128]{2,1,0:T(8,128)(2,1)S(1)}, u32[]{:S(2)}, u32[]{:S(2)}) collective-permute-start(bf16[2,80,128]{2,1,0:T(8,128)(2,1)S(1)} %get-tuple-element.45.pair), channel_id=1, source_target_pairs={{0,1},{1,0},{2,3},{3,2},{4,5},{5,4},{6,7},{7,6},{8,9},{9,8},{10,11... | collective-permute-start | bytes 122888 | tf_op jit(solution)/shard_map/ppermute | solution.py:41
  24.7 0.6 copy-start.11
  26.6 0.6 copy-start.9
  31.8 4.2 %collective-permute-start.7 = (bf16[1,80,128]{2,1,0:T(8,128)(2,1)S(1)}, bf16[1,80,128]{2,1,0:T(8,128)(2,1)S(1)}, u32[]{:S(2)}, u32[]{:S(2)}) collective-permute-start(bf16[1,80,128]{2,1,0:T(8,128)(2,1)S(1)} %bitcast.19), channel_id=1, source_target_pairs={{0,9},{1,8},{2,11},{3,10},{4,13},{5,12},{6,15},{7,14},{8,1},{9,0},... | collective-permute-start | bytes 61448 | tf_op jit(solution)/shard_map/ppermute | solution.py:41
  36.0 5.0 %collective-permute-start.8 = (bf16[2,80,128]{2,1,0:T(8,128)(2,1)S(1)}, bf16[2,80,128]{2,1,0:T(8,128)(2,1)S(1)}, u32[]{:S(2)}, u32[]{:S(2)}) collective-permute-start(bf16[2,80,128]{2,1,0:T(8,128)(2,1)S(1)} %pad_maximum_fusion.4), channel_id=1, source_target_pairs={{0,6},{1,7},{2,4},{3,5},{4,2},{5,3},{6,0},{7,1},{8,14},{9,15},{10,... | collective-permute-start | bytes 122888 | tf_op jit(solution)/shard_map/ppermute | solution.py:41
  37.4 4.3 %collective-permute-start.9 = (bf16[2,80,128]{2,1,0:T(8,128)(2,1)S(1)}, bf16[2,80,128]{2,1,0:T(8,128)(2,1)S(1)}, u32[]{:S(2)}, u32[]{:S(2)}) collective-permute-start(bf16[2,80,128]{2,1,0:T(8,128)(2,1)S(1)} %pad_maximum_fusion.4), channel_id=1, source_target_pairs={{0,3},{1,2},{2,1},{3,0},{4,7},{5,6},{6,5},{7,4},{8,11},{9,10},{10,... | collective-permute-start | bytes 122888 | tf_op jit(solution)/shard_map/ppermute | solution.py:41
  37.8 3.9 %collective-permute-start.10 = (bf16[2,80,128]{2,1,0:T(8,128)(2,1)S(1)}, bf16[2,80,128]{2,1,0:T(8,128)(2,1)S(1)}, u32[]{:S(2)}, u32[]{:S(2)}) collective-permute-start(bf16[2,80,128]{2,1,0:T(8,128)(2,1)S(1)} %pad_maximum_fusion.4), channel_id=1, source_target_pairs={{0,5},{1,4},{2,7},{3,6},{4,1},{5,0},{6,3},{7,2},{8,13},{9,12},{10,... | collective-permute-start | bytes 122888 | tf_op jit(solution)/shard_map/ppermute | solution.py:41
  41.8 1.5 %collective-permute-start.11 = (bf16[8,80,128]{2,1,0:T(8,128)(2,1)S(1)}, bf16[8,80,128]{2,1,0:T(8,128)(2,1)S(1)}, u32[]{:S(2)}, u32[]{:S(2)}) collective-permute-start(bf16[8,80,128]{2,1,0:T(8,128)(2,1)S(1)} %constant_dynamic-update-slice_fusion.5.near), channel_id=1, source_target_pairs={{0,1},{1,0},{2,3},{3,2},{4,5},{5,4},{6,7},{7,6},{8,9},{9,8},{10,11... | collective-permute-start | bytes 491528 | tf_op jit(solution)/shard_map/ppermute | solution.py:41
  44.0 4.2 %collective-permute-start.12 = (bf16[1,80,128]{2,1,0:T(8,128)(2,1)S(1)}, bf16[1,80,128]{2,1,0:T(8,128)(2,1)S(1)}, u32[]{:S(2)}, u32[]{:S(2)}) collective-permute-start(bf16[1,80,128]{2,1,0:T(8,128)(2,1)S(1)} %bitcast.15), channel_id=1, source_target_pairs={{0,9},{1,8},{2,11},{3,10},{4,13},{5,12},{6,15},{7,14},{8,1},{9,0},... | collective-permute-start | bytes 61448 | tf_op jit(solution)/shard_map/ppermute | solution.py:41
  48.2 4.9 %collective-permute-start.13 = (bf16[2,80,128]{2,1,0:T(8,128)(2,1)S(1)}, bf16[2,80,128]{2,1,0:T(8,128)(2,1)S(1)}, u32[]{:S(2)}, u32[]{:S(2)}) collective-permute-start(bf16[2,80,128]{2,1,0:T(8,128)(2,1)S(1)} %pad_maximum_fusion.5), channel_id=1, source_target_pairs={{0,6},{1,7},{2,4},{3,5},{4,2},{5,3},{6,0},{7,1},{8,14},{9,15},{10,... | collective-permute-start | bytes 122888 | tf_op jit(solution)/shard_map/ppermute | solution.py:41
  50.2 3.6 %collective-permute-start.14 = (bf16[2,80,128]{2,1,0:T(8,128)(2,1)S(1)}, bf16[2,80,128]{2,1,0:T(8,128)(2,1)S(1)}, u32[]{:S(2)}, u32[]{:S(2)}) collective-permute-start(bf16[2,80,128]{2,1,0:T(8,128)(2,1)S(1)} %pad_maximum_fusion.5), channel_id=1, source_target_pairs={{0,3},{1,2},{2,1},{3,0},{4,7},{5,6},{6,5},{7,4},{8,11},{9,10},{10,... | collective-permute-start | bytes 122888 | tf_op jit(solution)/shard_map/ppermute | solution.py:41
  50.3 3.5 %collective-permute-start.15 = (bf16[2,80,128]{2,1,0:T(8,128)(2,1)S(1)}, bf16[2,80,128]{2,1,0:T(8,128)(2,1)S(1)}, u32[]{:S(2)}, u32[]{:S(2)}) collective-permute-start(bf16[2,80,128]{2,1,0:T(8,128)(2,1)S(1)} %pad_maximum_fusion.5), channel_id=1, source_target_pairs={{0,5},{1,4},{2,7},{3,6},{4,1},{5,0},{6,3},{7,2},{8,13},{9,12},{10,... | collective-permute-start | bytes 122888 | tf_op jit(solution)/shard_map/ppermute | solution.py:41
  53.8 1.6 %collective-permute-start.16 = (bf16[8,80,128]{2,1,0:T(8,128)(2,1)S(1)}, bf16[8,80,128]{2,1,0:T(8,128)(2,1)S(1)}, u32[]{:S(2)}, u32[]{:S(2)}) collective-permute-start(bf16[8,80,128]{2,1,0:T(8,128)(2,1)S(1)} %constant_dynamic-update-slice_fusion.10.near), channel_id=1, source_target_pairs={{0,1},{1,0},{2,3},{3,2},{4,5},{5,4},{6,7},{7,6},{8,9},{9,8},{10,11... | collective-permute-start | bytes 491528 | tf_op jit(solution)/shard_map/ppermute | solution.py:41
  56.4 2.1 %collective-permute-start.17 = (bf16[2,80,128]{2,1,0:T(8,128)(2,1)S(1)}, bf16[2,80,128]{2,1,0:T(8,128)(2,1)S(1)}, u32[]{:S(2)}, u32[]{:S(2)}) collective-permute-start(bf16[2,80,128]{2,1,0:T(8,128)(2,1)S(1)} %get-tuple-element.64.pair), channel_id=1, source_target_pairs={{0,1},{1,0},{2,3},{3,2},{4,5},{5,4},{6,7},{7,6},{8,9},{9,8},{10,11... | collective-permute-start | bytes 122888 | tf_op jit(solution)/shard_map/ppermute | solution.py:41
  63.8 4.2 %collective-permute-start.18 = (bf16[1,80,128]{2,1,0:T(8,128)(2,1)S(1)}, bf16[1,80,128]{2,1,0:T(8,128)(2,1)S(1)}, u32[]{:S(2)}, u32[]{:S(2)}) collective-permute-start(bf16[1,80,128]{2,1,0:T(8,128)(2,1)S(1)} %bitcast.17), channel_id=1, source_target_pairs={{0,9},{1,8},{2,11},{3,10},{4,13},{5,12},{6,15},{7,14},{8,1},{9,0},... | collective-permute-start | bytes 61448 | tf_op jit(solution)/shard_map/ppermute | solution.py:41
  68.0 4.9 %collective-permute-start.19 = (bf16[2,80,128]{2,1,0:T(8,128)(2,1)S(1)}, bf16[2,80,128]{2,1,0:T(8,128)(2,1)S(1)}, u32[]{:S(2)}, u32[]{:S(2)}) collective-permute-start(bf16[2,80,128]{2,1,0:T(8,128)(2,1)S(1)} %pad_maximum_fusion.6), channel_id=1, source_target_pairs={{0,6},{1,7},{2,4},{3,5},{4,2},{5,3},{6,0},{7,1},{8,14},{9,15},{10,... | collective-permute-start | bytes 122888 | tf_op jit(solution)/shard_map/ppermute | solution.py:41
  69.7 4.1 %collective-permute-start.20 = (bf16[2,80,128]{2,1,0:T(8,128)(2,1)S(1)}, bf16[2,80,128]{2,1,0:T(8,128)(2,1)S(1)}, u32[]{:S(2)}, u32[]{:S(2)}) collective-permute-start(bf16[2,80,128]{2,1,0:T(8,128)(2,1)S(1)} %pad_maximum_fusion.6), channel_id=1, source_target_pairs={{0,3},{1,2},{2,1},{3,0},{4,7},{5,6},{6,5},{7,4},{8,11},{9,10},{10,... | collective-permute-start | bytes 122888 | tf_op jit(solution)/shard_map/ppermute | solution.py:41
  70.0 3.7 %collective-permute-start.21 = (bf16[2,80,128]{2,1,0:T(8,128)(2,1)S(1)}, bf16[2,80,128]{2,1,0:T(8,128)(2,1)S(1)}, u32[]{:S(2)}, u32[]{:S(2)}) collective-permute-start(bf16[2,80,128]{2,1,0:T(8,128)(2,1)S(1)} %pad_maximum_fusion.6), channel_id=1, source_target_pairs={{0,5},{1,4},{2,7},{3,6},{4,1},{5,0},{6,3},{7,2},{8,13},{9,12},{10,... | collective-permute-start | bytes 122888 | tf_op jit(solution)/shard_map/ppermute | solution.py:41
  73.8 15.9 %collective-permute-start.22 = (bf16[8,80,128]{2,1,0:T(8,128)(2,1)S(1)}, bf16[8,80,128]{2,1,0:T(8,128)(2,1)S(1)}, u32[]{:S(2)}, u32[]{:S(2)}) collective-permute-start(bf16[8,80,128]{2,1,0:T(8,128)(2,1)S(1)} %constant_dynamic-update-slice_fusion.15.near), channel_id=1, source_target_pairs={{0,1},{1,0},{2,3},{3,2},{4,5},{5,4},{6,7},{7,6},{8,9},{9,8},{10,11... | collective-permute-start | bytes 491528 | tf_op jit(solution)/shard_map/ppermute | solution.py:41

commit v2 on v1

v2 whole, which is shorter than its diff:
```python
import functools

import jax
import jax.numpy as jnp
from jax import lax
from jax.experimental import pallas as pl
from jax.experimental.pallas import tpu as pltpu
from jax.sharding import PartitionSpec as P


MAXLEN = 4096
EPS = 1e-05
MIB = 1 << 20
BYTES = 1 << 26


VM = pl.BlockSpec(memory_space=pltpu.VMEM)
SM = pl.BlockSpec(memory_space=pltpu.SMEM)
HBM = pl.BlockSpec(memory_space=pltpu.HBM)
F32 = jnp.float32
BF16 = jnp.bfloat16


def gather_phases(count):
    bits = [1 << i for i in range(count.bit_length() - 1)][::-1]
    if len(bits) < 2:
        return [tuple(bits)] if bits else []
    low = bits[-1]
    rounds = [(bits[0] | low,)] if len(bits) > 1 else []
    middle = bits[1:-1]
    for at in range(0, len(middle), 2):
        pair = middle[at : at + 2]
        if len(pair) == 2:
            rounds.append((pair[0] | pair[1], pair[1] | low, pair[0] | low))
        else:
            rounds.append((pair[0] | low,))
    return rounds + [(low,)]


def swap(value, mask):
    return lax.ppermute(value, "tp", [(s, s ^ mask) for s in range(lax.axis_size("tp"))])


def gather(value, held):
    *rounds, last = gather_phases(lax.axis_size("tp"))
    blocks, masks = value[None], [0]
    first = held[None]
    for number, group in enumerate(rounds):
        parts, before = [first if number == 0 else blocks], list(masks)
        for mask in group:
            parts.append(swap(blocks, mask))
            masks = masks + [m ^ mask for m in before]
        blocks = jnp.concatenate(parts, axis=0)
    far = swap(blocks, last[0])
    return blocks, far, masks, last[0]


def call(kernel, out_shape, in_specs, out_specs, scratch=(), aliases=None, limit=4, flops=1 << 20):
    return pl.pallas_call(
        kernel,
        out_shape=out_shape,
        in_specs=in_specs,
        out_specs=out_specs,
        scratch_shapes=scratch,
        input_output_aliases=aliases or {},
        compiler_params=pltpu.CompilerParams(vmem_limit_bytes=limit * MIB),
        cost_estimate=pl.CostEstimate(flops=flops, bytes_accessed=BYTES, transcendentals=0),
    )


def place(near, far, rows, masks, low):
    own = lax.axis_index("tp")
    for j, mask in enumerate(masks):
        rows[own ^ mask] = near[j]
        rows[own ^ mask ^ low] = far[j]


def joined(rows):
    return jnp.concatenate([rows[i] for i in range(rows.shape[0])], axis=1)


def dot(a, b):
    return jnp.dot(a, b, preferred_element_type=F32)


def heads_kernel(layer, masks, low, scale, near, far, gain, wq, wk, pair, normed, rows):
    place(near, far, rows, masks, low)
    x = joined(rows).astype(F32)
    inv = lax.rsqrt(jnp.mean(x * x, axis=1, keepdims=True) + EPS)
    n = (x * inv * gain[layer : layer + 1].astype(F32)).astype(BF16)
    normed[...] = n
    width = wq.shape[1]
    both = dot(n, jnp.concatenate([wq[...], wk[...]], axis=1))
    pair[0] = both[:, :width].astype(BF16)
    pair[1] = (both[:, width:] * scale).astype(BF16)


def as_column(row):
    n = row.shape[1]
    same = lax.broadcasted_iota(jnp.int32, (n, n), 0) == lax.broadcasted_iota(jnp.int32, (n, n), 1)
    return jnp.sum(jnp.where(same, row, 0.0), axis=1, keepdims=True)


def gates_kernel(
    layer, split, normed, wv, wo, wi, wf, ibias, fbias, slope, lengths, stab, old,
    values, outgate, factors, stab_new, columns, decays,
):
    n = normed[...]
    width = wv.shape[1]
    both = dot(n, jnp.concatenate([wv[...], wo[...]], axis=1))
    values[...] = both[:, :width].astype(BF16)
    outgate[...] = both[:, width:].astype(BF16)

    def logits(w):
        return lax.dot_general(w[layer], n, (((1,), (1,)), ((), ())), preferred_element_type=F32)

    row = slice(layer, layer + 1)
    position = lengths[...].astype(F32) / MAXLEN
    ingate = logits(wi) + as_column(ibias[row])
    forget = jax.nn.log_sigmoid(logits(wf) + as_column(fbias[row]) + as_column(slope[row]) * position)
    held = forget + stab[layer]
    top = jnp.maximum(held, ingate)
    for other in range(layer):
        stab_new[other] = old[other]
    stab_new[layer] = top
    index = lax.broadcasted_iota(jnp.int32, top.shape, 0)
    mine = index == lax.axis_index("tp") // split
    decay = jnp.sum(jnp.where(mine, jnp.exp(held - top), 0.0), axis=0, keepdims=True)
    weight = jnp.sum(jnp.where(mine, jnp.exp(ingate - top), 0.0), axis=0, keepdims=True)
    factors[...] = jnp.where(index == 0, decay, weight).T
    batch, lanes = n.shape[0], columns.shape[1]
    v = both[:, :width].astype(BF16).astype(F32) * factors[:, 1:2]
    if lanes > batch:
        v = jnp.concatenate([v, jnp.zeros((lanes - batch, width), F32)], axis=0)
    columns[...] = v.T
    decays[...] = jnp.broadcast_to(factors[:, 0:1], decays.shape)


def in_order(parts, rows):
    local = lax.rem(lax.axis_index("tp"), len(parts))
    for mask, part in enumerate(parts):
        rows[local ^ mask] = part[...]


def read_kernel(layer, split, rows, memory, kept, *refs):
    pairs, refs = refs[:split], refs[split:]
    sums, refs = refs[:split], refs[split:]
    values, outgate, factors, gain, old, gated, sums_new, keys, rest, query, pieces, arrived = refs
    (first, width, depth), batch = kept.shape, values.shape[0]
    lanes = -(-batch // 128) * 128

    def fetch(i):
        part = pl.ds(i * rows, rows)
        return pltpu.make_async_copy(memory.at[layer, pl.ds(first + i * rows, rows)], rest.at[part], arrived.at[i])

    for i in range((batch - first) // rows):
        fetch(i).start()
    in_order(pairs, pieces)
    q = jnp.concatenate([pieces[i, 0] for i in range(split)], axis=1).astype(F32)
    query[...] = q
    key = jnp.concatenate([pieces[i, 1] for i in range(split)], axis=1).astype(F32)
    keys[...] = key
    lane = lax.broadcasted_iota(jnp.int32, (width, lanes), 1)

    def add(state, i, at, total):
        for r in range(rows):
            b = at + i * rows + r
            product = state[i * rows + r] * query[pl.ds(b, 1), :]
            column = jnp.sum(product, axis=1, keepdims=True)
            total = jnp.where(lane == b, column, total)
        return total

    def late(i, total):
        fetch(i).wait()
        return add(rest, i, first, total)

    total = jnp.zeros((width, lanes), F32)
    total = lax.fori_loop(0, first // rows, lambda i, total: add(kept, i, 0, total), total)
    total = lax.fori_loop(0, (batch - first) // rows, late, total)
    read = total.T[:batch]
    decay, weight = factors[:, 0:1], factors[:, 1:2]
    match = weight * jnp.sum(key * q, axis=1, keepdims=True)
    v = values[...].astype(F32)
    numerator = decay * read + match * v
    held = sum(s[layer] * p[0].astype(F32) for s, p in zip(sums, pairs))
    below = decay * jnp.sum(held, axis=1, keepdims=True) + match
    hidden = numerator / jnp.maximum(jnp.abs(below), 1.0)
    gate = jax.nn.sigmoid(outgate[...].astype(F32))
    gated[...] = (hidden * gain[layer : layer + 1].astype(F32) * gate).astype(BF16)
    for other in range(layer):
        sums_new[other] = old[other]
    sums_new[layer] = decay * sums[0][layer] + weight * pairs[0][1].astype(F32)


def out_kernel(masks, low, near, far, current, wo, after, rows):
    place(near, far, rows, masks, low)
    total = current[...].astype(F32) + dot(joined(rows), wo[...])
    after[...] = total.astype(BF16)


def update_kernel(layer, first, rows, kept, columns, decays, keys, _old, new, staged, sent):
    batch, width, depth = kept.shape
    lanes = columns.shape[1]

    def send(i):
        part = pl.ds(i * rows, rows)
        return pltpu.make_async_copy(staged.at[part], new.at[layer, pl.ds(first + i * rows, rows)], sent.at[i])

    def some(i, carry):
        at = first + i * rows
        turned = pltpu.roll(columns[...], lanes - at, axis=1)
        for r in range(rows):
            column = jnp.broadcast_to(turned[:, r : r + 1], (width, depth))
            key = keys[pl.ds(at + r, 1), :]
            staged[i * rows + r] = decays[pl.ds(at + r, 1), :] * kept[i * rows + r] + column * key
        send(i).start()
        return carry

    lax.fori_loop(0, batch // rows, some, 0)
    for i in range(batch // rows):
        send(i).wait()


def in_hbm(x):
    return pltpu.with_memory_space_constraint(x, pltpu.HBM)


def load_kernel(layer, whole, sliced, *refs):
    arrived, count = refs[-1], whole + sliced
    copies = []
    for i in range(count):
        source = refs[i] if i < whole else refs[i].at[layer]
        copies.append(pltpu.make_async_copy(source, refs[count + i], arrived.at[i]))
    for copy in copies:
        copy.start()
    for copy in copies:
        copy.wait()


def load(layer, whole, sliced):
    count = len(whole) + len(sliced)
    shapes = [a.shape for a in whole] + [a.shape[1:] for a in sliced]
    return call(
        functools.partial(load_kernel, layer, len(whole), len(sliced)),
        tuple(pltpu.VMEM(s, a.dtype) for s, a in zip(shapes, (*whole, *sliced))),
        [HBM] * count,
        (VM,) * count,
        [pltpu.SemaphoreType.DMA((count,))],
    )(*(in_hbm(a) for a in (*whole, *sliced)))


def state_kernel(layer, rows, memory, kept, arrived):
    copies = []
    for i in range(kept.shape[0] // rows):
        part = pl.ds(i * rows, rows)
        copies.append(pltpu.make_async_copy(memory.at[layer, part], kept.at[part], arrived.at[i]))
    for copy in copies:
        copy.start()
    for copy in copies:
        copy.wait()


def body(
    tokens,
    lengths,
    cell_memory,
    key_sums,
    stabilizer,
    norm_gain,
    query_weight,
    key_weight,
    value_weight,
    outgate_weight,
    ingate_weight,
    forget_weight,
    ingate_bias,
    forget_bias,
    forget_slope,
    head_gain,
    output_weight,
):
    count = lax.axis_size("tp")
    blocks, batch, width, depth = cell_memory.shape
    heads = stabilizer.shape[2]
    split = count // heads

    def pieces(value):
        found = [value]
        for mask in range(1, split):
            found.append(swap(value, mask))
        return found

    shape = jax.ShapeDtypeStruct
    rows = 8 if batch % 8 == 0 else 1
    lanes = -(-batch // 128) * 128
    first = batch // rows // 2 * rows
    sizes = (first, batch - first)
    weights = [query_weight, key_weight, value_weight, outgate_weight, output_weight]
    own_sums, wi, wf, ibias, fbias, slope, at, stab, norm_gain, head_gain, current, *loaded = load(
        0,
        [
            key_sums,
            jnp.swapaxes(ingate_weight, 1, 2),
            jnp.swapaxes(forget_weight, 1, 2),
            ingate_bias,
            forget_bias,
            forget_slope,
            lengths[None],
            jnp.swapaxes(stabilizer, 1, 2),
            norm_gain,
            head_gain,
            tokens,
        ],
        weights,
    )
    near, far, masks, low = gather(tokens, current)
    sums = pieces(own_sums)
    memory = in_hbm(cell_memory)
    new_memory, new_sums, new_stab = at, own_sums, stab
    for layer in range(blocks):
        if layer:
            near, far, masks, low = gather(current, current)
            loaded = load(layer, [], weights)
        wq, wk, wv, wg, wo = loaded
        kept = call(
            functools.partial(state_kernel, layer, rows),
            pltpu.VMEM((first, width, depth), F32),
            [HBM],
            VM,
            [pltpu.SemaphoreType.DMA((first // rows,))],
        )(memory)
        pair, normed = call(
            functools.partial(heads_kernel, layer, masks, low, depth ** (-0.5)),
            (shape((2, batch, width), BF16), pltpu.VMEM((batch, count * width), BF16)),
            [VM] * 5,
            (VM, VM),
            [pltpu.VMEM((count, batch, width), BF16)],
        )(near, far, norm_gain, wq, wk)
        pairs = pieces(pair)
        values, outgate, factors, new_stab, columns, decays = call(
            functools.partial(gates_kernel, layer, split),
            (
                shape((batch, width), BF16),
                shape((batch, width), BF16),
                shape((batch, heads), F32),
                shape(stab.shape, F32),
                pltpu.VMEM((width, lanes), F32),
                pltpu.VMEM((batch, depth), F32),
            ),
            [VM] * 11,
            (VM,) * 6,
        )(normed, wv, wg, wi, wf, ibias, fbias, slope, at, stab, new_stab)
        gated, new_sums, keys, rest = call(
            functools.partial(read_kernel, layer, split, rows),
            (
                shape((batch, width), BF16),
                shape(own_sums.shape, F32),
                pltpu.VMEM((batch, depth), F32),
                pltpu.VMEM((batch - first, width, depth), F32),
            ),
            [HBM] + [VM] * (6 + 2 * split),
            (VM,) * 4,
            [
                pltpu.VMEM((batch, depth), F32),
                pltpu.VMEM((split, 2, batch, width), BF16),
                pltpu.SemaphoreType.DMA(((batch - first) // rows,)),
            ],
        )(memory, kept, *pairs, *sums, values, outgate, factors, head_gain, new_sums)

        near, far, masks, low = gather(gated, gated)
        for part, state in enumerate((kept, rest)):
            new_memory = call(
                functools.partial(update_kernel, layer, part * first, rows),
                shape(cell_memory.shape, F32),
                [VM] * 4 + [HBM],
                HBM,
                [
                    pltpu.VMEM((sizes[part], width, depth), F32),
                    pltpu.SemaphoreType.DMA((sizes[part] // rows,)),
                ],
                {} if layer == part == 0 else {4: 0},
                limit=8,
            )(state, columns, decays, keys, in_hbm(new_memory))

        current = call(
            functools.partial(out_kernel, masks, low),
            shape((batch, width), BF16),
            [VM] * 4,
            VM,
            [pltpu.VMEM((count, batch, width), BF16)],
        )(near, far, current, wo)
    return current, new_memory, new_sums, jnp.swapaxes(new_stab, 1, 2)


def solution(mesh):
    in_specs = (
        P("grp", "tp"),
        P("grp"),
        P(None, "grp", "tp", None),
        P(None, "grp", "tp"),
        P(None, "grp", None),
        P(),
        P(None, None, "tp"),
        P(None, None, "tp"),
        P(None, None, "tp"),
        P(None, None, "tp"),
        P(),
        P(),
        P(),
        P(),
        P(),
        P(None, "tp"),
        P(None, None, "tp"),
    )
    out_specs = (
        P("grp", "tp"),
        P(None, "grp", "tp", None),
        P(None, "grp", "tp"),
        P(None, "grp", None),
    )

    return jax.shard_map(body, mesh=mesh, in_specs=in_specs, out_specs=out_specs, check_vma=False)
```

time: 91.5 us -> 76.1 us (0.83)
  local copies, waits for them, and re-layouts: 8.32 us -> 0.17 us
  Pallas kernels: 35.3 us -> 30.1 us
  other arithmetic: 1.81 us -> 0.02 us
    unnamed x42 -> x18, local copies, waits for them, and re-layouts: 8.28 us -> 0.13 us
    pallas_call x13 -> x14, Pallas kernels: 33.3 us -> 29.2 us  [the longest x4 10.7 us: body(): call(functools.partial(update_kernel, layer, part * first, rows), shape(c...]
    pallas_call x2, Pallas kernels: 1.98 us -> 0.91 us  [body(): call(functools.partial(heads_kernel, layer, masks, low, depth ** (-0.5)),...]
    ppermute x23, starting transfers between devices: 27 us -> 26.1 us  [swap(): lax.ppermute(value, 'tp', [(s, s ^ mask) for s in range(lax.axis_size('tp...]
    select_n x3 -> x0, other arithmetic: 0.93 us -> none  [whole_head(): jnp.where(upper, partner, value)]
  transfers between devices with their start and end apart: 23 -> 23, of which waited for: 16 -> 15; matrix products, arithmetic and copies ran while one was open for 4% -> 0% of each run, Pallas kernels for 20% -> 29%
where the time goes in v2:
time: 76.1 us; the launch traced here: 75.9 us
  Pallas kernels  30.1 us (40%)
  starting transfers between devices  26.1 us (34%)
  waiting for transfers between devices  18.6 us (24%)
  between operations  0.82 us (1%)
    ppermute x23, starting transfers between devices, swap(): lax.ppermute(value, 'tp', [(s, s ^ mask) for s in range(lax.axis_size('tp...  26.1 us
    ppermute x23, waiting for transfers between devices, swap(): lax.ppermute(value, 'tp', [(s, s ^ mask) for s in range(lax.axis_size('tp...  18.6 us
    pallas_call x4, Pallas kernels, body(): call(functools.partial(update_kernel, layer, part * first, rows), shape(c...  10.7 us
    pallas_call x2, Pallas kernels, body(): call(functools.partial(read_kernel, layer, split, rows), (shape((batch, w...  6.7 us
    pallas_call x2, Pallas kernels, body(): call(functools.partial(state_kernel, layer, rows), pltpu.VMEM((first, wid...  5.06 us
    pallas_call x2, Pallas kernels, load(): call(functools.partial(load_kernel, layer, len(whole), len(sliced)), tupl...  3.74 us
    pallas_call x2, Pallas kernels, body(): call(functools.partial(gates_kernel, layer, split), (shape((batch, width)...  1.87 us
  transfers between devices with their start and end apart: 23, of which 15 were waited for; matrix products, arithmetic and copies ran while one was open for 0% of the time, Pallas kernels for 29%

profile of v2, /device:TPU:0, one launch (start us, length us, event | category | flops | bytes accessed | tf_op | source)
XLA Modules:
  0.0 75.9 jit_solution(9277069080897439547)
XLA Ops:
  0.6 3.6 %collective-permute-start = (bf16[1,80,128]{2,1,0:T(8,128)(2,1)}, bf16[1,80,128]{2,1,0:T(8,128)(2,1)S(1)}, u32[]{:S(2)}, u32[]{:S(2)}) collective-permute-start(bf16[1,80,128]{2,1,0:T(8,128)(2,1)} %bitcast.23), channel_id=1, source_target_pairs={{0,9},{1,8},{2,11},{3,10},{4,13},{5,12},{6,15},{7,14},{8,1},{9,0},... | collective-permute-start | bytes 61448 | tf_op jit(solution)/shard_map/ppermute | solution.py:41
  4.2 2.0 %shard_map.194 = (f32[2,80,128]{2,1,0:T(8,128)S(1)}, bf16[2,8,2048]{2,1,0:T(8,128)(2,1)S(1)}, bf16[2,8,2048]{2,1,0:T(8,128)(2,1)S(1)}, f32[2,8]{1,0:T(2,128)S(1)...) custom-call(f32[2,80,128]{2,1,0:T(8,128)} %refs_0_.2, ...), custom_call_target="tpu_custom_call" | custom-call | flops 1048576 | bytes 67108864 | tf_op jit(solution)/shard_map/pallas_call | solution.py:243
  6.2 0.0 copy-start
  6.3 0.0 collective-permute-done
  6.3 2.7 %collective-permute-start.1 = (bf16[2,80,128]{2,1,0:T(8,128)(2,1)S(1)}, bf16[2,80,128]{2,1,0:T(8,128)(2,1)S(1)}, u32[]{:S(2)}, u32[]{:S(2)}) collective-permute-start(bf16[2,80,128]{2,1,0:T(8,128)(2,1)S(1)} %pad_maximum_fusion), channel_id=1, source_target_pairs={{0,6},{1,7},{2,4},{3,5},{4,2},{5,3},{6,0},{7,1},{8,14},{9,15},{10,... | collective-permute-start | bytes 122888 | tf_op jit(solution)/shard_map/ppermute | solution.py:41
  9.0 0.4 collective-permute-start.2
  9.4 0.2 collective-permute-start.3
  9.6 1.8 %collective-permute-done.1 = bf16[2,80,128]{2,1,0:T(8,128)(2,1)S(1)} collective-permute-done((bf16[2,80,128]{2,1,0:T(8,128)(2,1)S(1)}, bf16[2,80,128]{2,1,0:T(8,128)(2,1)S(1)}, u32[]{:S(2)}, u32[]{:S(2)}) %collective-permute-start.1) | collective-permute-done | bytes 40992 | tf_op jit(solution)/shard_map/ppermute | solution.py:41
  11.4 1.1 %collective-permute-done.2 = bf16[2,80,128]{2,1,0:T(8,128)(2,1)S(1)} collective-permute-done((bf16[2,80,128]{2,1,0:T(8,128)(2,1)S(1)}, bf16[2,80,128]{2,1,0:T(8,128)(2,1)S(1)}, u32[]{:S(2)}, u32[]{:S(2)}) %collective-permute-start.2) | collective-permute-done | bytes 40992 | tf_op jit(solution)/shard_map/ppermute | solution.py:41
  12.5 0.3 collective-permute-done.3
  12.8 0.3 collective-permute-start.4
  13.2 0.2 collective-permute-start.6
  13.4 0.9 %collective-permute-done.4.far = bf16[8,80,128]{2,1,0:T(8,128)(2,1)S(1)} collective-permute-done((bf16[8,80,128]{2,1,0:T(8,128)(2,1)S(1)}, bf16[8,80,128]{2,1,0:T(8,128)(2,1)S(1)}, u32[]{:S(2)}, u32[]{:S(2)}) %collective-permute-start.4) | collective-permute-done | bytes 163872 | tf_op jit(solution)/shard_map/ppermute | solution.py:41
  14.3 0.5 shard_map.195
  14.7 0.3 collective-permute-start.5
  15.1 2.5 %shard_map.193.kept = f32[40,128,256]{2,1,0:T(8,128)S(1)} custom-call(f32[2,80,128,256]{3,2,1,0:T(8,128)} %memory.7), custom_call_target="tpu_custom_call" | custom-call | flops 1048576 | bytes 67108864 | tf_op jit(solution)/shard_map/pallas_call | solution.py:325
  17.6 0.8 %shard_map.196 = (bf16[80,128]{1,0:T(8,128)(2,1)S(1)}, bf16[80,128]{1,0:T(8,128)(2,1)S(1)}, f32[80,8]{1,0:T(8,128)S(1)}, f32[2,8,80]{2,1,0:T(8,128)S(1)}, f32[128,128]{1,0:T(8,128)S(1)}, /*index=5*/f32[80,256]{1,0:T(8,128)S(1)}) custom-call(bf16[80,2048]{1,0:T(8,128)(2,1)S(1)} %get-tuple-element.55.normed, bf16[2048,128]{1,0:T(8,128)(2,1)S(1)} %get-tuple-element.56.wv, ...), custom_call_target="tpu_custom_call" | custom-call | flops 1048576 | bytes 67108864 | tf_op jit(solution)/shard_map/pallas_call | solution.py:340
  18.4 0.0 collective-permute-done.6.refs_3_
  18.4 0.0 collective-permute-done.5.refs_1_
  18.4 3.0 %shard_map.197 = (bf16[80,128]{1,0:T(8,128)(2,1)S(1)}, f32[2,80,128]{2,1,0:T(8,128)S(1)}, f32[80,256]{1,0:T(8,128)S(1)}, f32[40,128,256]{2,1,0:T(8,128)S(1)}) custom-call(f32[2,80,128,256]{3,2,1,0:T(8,128)} %memory.7, f32[40,128,256]{2,1,0:T(8,128)S(1)} %shard_map.193.kept, bf16[2,80,128]{2,1,0:T(8,128)(2,1)S(1)} %get-tuple-element.53.refs_0_, ...), custom_call_target="tpu_custom_call" | custom-call | flops 1048576 | bytes 67108864 | tf_op jit(solution)/shard_map/pallas_call | solution.py:353
  21.4 3.1 %collective-permute-start.7 = (bf16[1,80,128]{2,1,0:T(8,128)(2,1)S(1)}, bf16[1,80,128]{2,1,0:T(8,128)(2,1)S(1)}, u32[]{:S(2)}, u32[]{:S(2)}) collective-permute-start(bf16[1,80,128]{2,1,0:T(8,128)(2,1)S(1)} %bitcast.19), channel_id=1, source_target_pairs={{0,9},{1,8},{2,11},{3,10},{4,13},{5,12},{6,15},{7,14},{8,1},{9,0},... | collective-permute-start | bytes 61448 | tf_op jit(solution)/shard_map/ppermute | solution.py:41
  24.6 2.0 %collective-permute-done.7 = bf16[1,80,128]{2,1,0:T(8,128)(2,1)S(1)} collective-permute-done((bf16[1,80,128]{2,1,0:T(8,128)(2,1)S(1)}, bf16[1,80,128]{2,1,0:T(8,128)(2,1)S(1)}, u32[]{:S(2)}, u32[]{:S(2)}) %collective-permute-start.7) | collective-permute-done | bytes 20512 | tf_op jit(solution)/shard_map/ppermute | solution.py:41
  26.6 1.0 %collective-permute-start.8 = (bf16[2,80,128]{2,1,0:T(8,128)(2,1)S(1)}, bf16[2,80,128]{2,1,0:T(8,128)(2,1)S(1)}, u32[]{:S(2)}, u32[]{:S(2)}) collective-permute-start(bf16[2,80,128]{2,1,0:T(8,128)(2,1)S(1)} %pad_maximum_fusion.1), channel_id=1, source_target_pairs={{0,6},{1,7},{2,4},{3,5},{4,2},{5,3},{6,0},{7,1},{8,14},{9,15},{10,... | collective-permute-start | bytes 122888 | tf_op jit(solution)/shard_map/ppermute | solution.py:41
  27.6 0.1 collective-permute-start.9
  27.7 2.1 %collective-permute-start.10 = (bf16[2,80,128]{2,1,0:T(8,128)(2,1)S(1)}, bf16[2,80,128]{2,1,0:T(8,128)(2,1)S(1)}, u32[]{:S(2)}, u32[]{:S(2)}) collective-permute-start(bf16[2,80,128]{2,1,0:T(8,128)(2,1)S(1)} %pad_maximum_fusion.1), channel_id=1, source_target_pairs={{0,5},{1,4},{2,7},{3,6},{4,1},{5,0},{6,3},{7,2},{8,13},{9,12},{10,... | collective-permute-start | bytes 122888 | tf_op jit(solution)/shard_map/ppermute | solution.py:41
  29.8 1.7 %collective-permute-done.8 = bf16[2,80,128]{2,1,0:T(8,128)(2,1)S(1)} collective-permute-done((bf16[2,80,128]{2,1,0:T(8,128)(2,1)S(1)}, bf16[2,80,128]{2,1,0:T(8,128)(2,1)S(1)}, u32[]{:S(2)}, u32[]{:S(2)}) %collective-permute-start.8) | collective-permute-done | bytes 40992 | tf_op jit(solution)/shard_map/ppermute | solution.py:41
  31.5 0.4 collective-permute-done.9
  31.9 0.0 collective-permute-done.10
  32.0 0.2 collective-permute-start.11
  32.1 1.3 %collective-permute-done.11.far = bf16[8,80,128]{2,1,0:T(8,128)(2,1)S(1)} collective-permute-done((bf16[8,80,128]{2,1,0:T(8,128)(2,1)S(1)}, bf16[8,80,128]{2,1,0:T(8,128)(2,1)S(1)}, u32[]{:S(2)}, u32[]{:S(2)}) %collective-permute-start.11) | collective-permute-done | bytes 163872 | tf_op jit(solution)/shard_map/ppermute | solution.py:41
  33.4 0.3 shard_map.198.current
  33.7 2.2 %collective-permute-start.12 = (bf16[1,80,128]{2,1,0:T(8,128)(2,1)S(1)}, bf16[1,80,128]{2,1,0:T(8,128)(2,1)S(1)}, u32[]{:S(2)}, u32[]{:S(2)}) collective-permute-start(bf16[1,80,128]{2,1,0:T(8,128)(2,1)S(1)} %bitcast.14), channel_id=1, source_target_pairs={{0,9},{1,8},{2,11},{3,10},{4,13},{5,12},{6,15},{7,14},{8,1},{9,0},... | collective-permute-start | bytes 61448 | tf_op jit(solution)/shard_map/ppermute | solution.py:41
  35.9 2.0 %collective-permute-done.12 = bf16[1,80,128]{2,1,0:T(8,128)(2,1)S(1)} collective-permute-done((bf16[1,80,128]{2,1,0:T(8,128)(2,1)S(1)}, bf16[1,80,128]{2,1,0:T(8,128)(2,1)S(1)}, u32[]{:S(2)}, u32[]{:S(2)}) %collective-permute-start.12) | collective-permute-done | bytes 20512 | tf_op jit(solution)/shard_map/ppermute | solution.py:41
  37.9 1.7 %collective-permute-start.13 = (bf16[2,80,128]{2,1,0:T(8,128)(2,1)S(1)}, bf16[2,80,128]{2,1,0:T(8,128)(2,1)S(1)}, u32[]{:S(2)}, u32[]{:S(2)}) collective-permute-start(bf16[2,80,128]{2,1,0:T(8,128)(2,1)S(1)} %pad_maximum_fusion.2), channel_id=1, source_target_pairs={{0,6},{1,7},{2,4},{3,5},{4,2},{5,3},{6,0},{7,1},{8,14},{9,15},{10,... | collective-permute-start | bytes 122888 | tf_op jit(solution)/shard_map/ppermute | solution.py:41
  39.6 0.7 collective-permute-start.14
  40.3 0.8 %collective-permute-start.15 = (bf16[2,80,128]{2,1,0:T(8,128)(2,1)S(1)}, bf16[2,80,128]{2,1,0:T(8,128)(2,1)S(1)}, u32[]{:S(2)}, u32[]{:S(2)}) collective-permute-start(bf16[2,80,128]{2,1,0:T(8,128)(2,1)S(1)} %pad_maximum_fusion.2), channel_id=1, source_target_pairs={{0,5},{1,4},{2,7},{3,6},{4,1},{5,0},{6,3},{7,2},{8,13},{9,12},{10,... | collective-permute-start | bytes 122888 | tf_op jit(solution)/shard_map/ppermute | solution.py:41
  41.1 1.7 %collective-permute-done.13 = bf16[2,80,128]{2,1,0:T(8,128)(2,1)S(1)} collective-permute-done((bf16[2,80,128]{2,1,0:T(8,128)(2,1)S(1)}, bf16[2,80,128]{2,1,0:T(8,128)(2,1)S(1)}, u32[]{:S(2)}, u32[]{:S(2)}) %collective-permute-start.13) | collective-permute-done | bytes 40992 | tf_op jit(solution)/shard_map/ppermute | solution.py:41
  42.8 0.9 %collective-permute-done.14 = bf16[2,80,128]{2,1,0:T(8,128)(2,1)S(1)} collective-permute-done((bf16[2,80,128]{2,1,0:T(8,128)(2,1)S(1)}, bf16[2,80,128]{2,1,0:T(8,128)(2,1)S(1)}, u32[]{:S(2)}, u32[]{:S(2)}) %collective-permute-start.14) | collective-permute-done | bytes 40992 | tf_op jit(solution)/shard_map/ppermute | solution.py:41
  43.7 0.1 collective-permute-done.15
  43.7 0.5 collective-permute-start.16
  44.2 1.7 %shard_map.199 = (bf16[2048,128]{1,0:T(8,128)(2,1)S(1)}, bf16[2048,128]{1,0:T(8,128)(2,1)S(1)}, bf16[2048,128]{1,0:T(8,128)(2,1)S(1)}, bf16[2048,128]{1,0:T(8,128)(2,1)S(1)}, bf16[2048,128]{1,0:T(8,128)(2,1)S(1)}) custom-call(bf16[2,2048,128]{2,1,0:T(8,128)(2,1)} %refs_0_.3, bf16[2,2048,128]{2,1,0:T(8,128)(2,1)} %refs_1_.1, bf16[2,2048,128]{2,1,0:T(8,128)(2,1)} %refs_2_.1, ...), custom_call_target="tpu_custom_call" | custom-call | flops 1048576 | bytes 67108864 | tf_op jit(solution)/shard_map/pallas_call | solution.py:243
  45.9 0.0 collective-permute-done.16.far
  46.0 0.5 shard_map.200
  46.4 0.1 collective-permute-start.17
  46.6 2.5 %shard_map.192.kept = f32[40,128,256]{2,1,0:T(8,128)S(1)} custom-call(f32[2,80,128,256]{3,2,1,0:T(8,128)} %memory.7), custom_call_target="tpu_custom_call" | custom-call | flops 1048576 | bytes 67108864 | tf_op jit(solution)/shard_map/pallas_call | solution.py:325
  49.1 0.0 copy-done
  49.1 1.1 %shard_map.201 = (bf16[80,128]{1,0:T(8,128)(2,1)S(1)}, bf16[80,128]{1,0:T(8,128)(2,1)S(1)}, f32[80,8]{1,0:T(8,128)S(1)}, f32[2,8,80]{2,1,0:T(8,128)}, f32[128,128]{1,0:T(8,128)S(1)}, /*index=5*/f32[80,256]{1,0:T(8,128)S(1)}) custom-call(bf16[80,2048]{1,0:T(8,128)(2,1)S(1)} %get-tuple-element.74.normed, bf16[2048,128]{1,0:T(8,128)(2,1)S(1)} %get-tuple-element.75.wv, ...), custom_call_target="tpu_custom_call" | custom-call | flops 1048576 | bytes 67108864 | tf_op jit(solution)/shard_map/pallas_call | solution.py:340
  50.2 0.0 collective-permute-done.17.refs_1_
  50.2 3.7 %shard_map.202 = (bf16[80,128]{1,0:T(8,128)(2,1)S(1)}, f32[2,80,128]{2,1,0:T(8,128)}, f32[80,256]{1,0:T(8,128)S(1)}, f32[40,128,256]{2,1,0:T(8,128)S(1)}) custom-call(f32[2,80,128,256]{3,2,1,0:T(8,128)} %memory.7, f32[40,128,256]{2,1,0:T(8,128)S(1)} %shard_map.192.kept, bf16[2,80,128]{2,1,0:T(8,128)(2,1)S(1)} %get-tuple-element.73.refs_0_, ...), custom_call_target="tpu_custom_call" | custom-call | flops 1048576 | bytes 67108864 | tf_op jit(solution)/shard_map/pallas_call | solution.py:353
  53.9 2.4 %collective-permute-start.18 = (bf16[1,80,128]{2,1,0:T(8,128)(2,1)S(1)}, bf16[1,80,128]{2,1,0:T(8,128)(2,1)S(1)}, u32[]{:S(2)}, u32[]{:S(2)}) collective-permute-start(bf16[1,80,128]{2,1,0:T(8,128)(2,1)S(1)} %bitcast.17), channel_id=1, source_target_pairs={{0,9},{1,8},{2,11},{3,10},{4,13},{5,12},{6,15},{7,14},{8,1},{9,0},... | collective-permute-start | bytes 61448 | tf_op jit(solution)/shard_map/ppermute | solution.py:41
  56.3 1.7 %collective-permute-done.18 = bf16[1,80,128]{2,1,0:T(8,128)(2,1)S(1)} collective-permute-done((bf16[1,80,128]{2,1,0:T(8,128)(2,1)S(1)}, bf16[1,80,128]{2,1,0:T(8,128)(2,1)S(1)}, u32[]{:S(2)}, u32[]{:S(2)}) %collective-permute-start.18) | collective-permute-done | bytes 20512 | tf_op jit(solution)/shard_map/ppermute | solution.py:41
  58.1 1.5 %collective-permute-start.19 = (bf16[2,80,128]{2,1,0:T(8,128)(2,1)S(1)}, bf16[2,80,128]{2,1,0:T(8,128)(2,1)S(1)}, u32[]{:S(2)}, u32[]{:S(2)}) collective-permute-start(bf16[2,80,128]{2,1,0:T(8,128)(2,1)S(1)} %pad_maximum_fusion.3), channel_id=1, source_target_pairs={{0,6},{1,7},{2,4},{3,5},{4,2},{5,3},{6,0},{7,1},{8,14},{9,15},{10,... | collective-permute-start | bytes 122888 | tf_op jit(solution)/shard_map/ppermute | solution.py:41
  59.5 0.5 collective-permute-start.20
  60.0 1.2 %collective-permute-start.21 = (bf16[2,80,128]{2,1,0:T(8,128)(2,1)S(1)}, bf16[2,80,128]{2,1,0:T(8,128)(2,1)S(1)}, u32[]{:S(2)}, u32[]{:S(2)}) collective-permute-start(bf16[2,80,128]{2,1,0:T(8,128)(2,1)S(1)} %pad_maximum_fusion.3), channel_id=1, source_target_pairs={{0,5},{1,4},{2,7},{3,6},{4,1},{5,0},{6,3},{7,2},{8,13},{9,12},{10,... | collective-permute-start | bytes 122888 | tf_op jit(solution)/shard_map/ppermute | solution.py:41
  61.3 2.0 %collective-permute-done.19 = bf16[2,80,128]{2,1,0:T(8,128)(2,1)S(1)} collective-permute-done((bf16[2,80,128]{2,1,0:T(8,128)(2,1)S(1)}, bf16[2,80,128]{2,1,0:T(8,128)(2,1)S(1)}, u32[]{:S(2)}, u32[]{:S(2)}) %collective-permute-start.19) | collective-permute-done | bytes 40992 | tf_op jit(solution)/shard_map/ppermute | solution.py:41
  63.3 0.8 %collective-permute-done.20 = bf16[2,80,128]{2,1,0:T(8,128)(2,1)S(1)} collective-permute-done((bf16[2,80,128]{2,1,0:T(8,128)(2,1)S(1)}, bf16[2,80,128]{2,1,0:T(8,128)(2,1)S(1)}, u32[]{:S(2)}, u32[]{:S(2)}) %collective-permute-start.20) | collective-permute-done | bytes 40992 | tf_op jit(solution)/shard_map/ppermute | solution.py:41
  64.1 0.0 collective-permute-done.21
  64.1 0.2 collective-permute-start.22
  64.3 2.7 %shard_map.204._old = f32[2,80,128,256]{3,2,1,0:T(8,128)} custom-call(f32[40,128,256]{2,1,0:T(8,128)S(1)} %shard_map.193.kept, f32[128,128]{1,0:T(8,128)S(1)} %get-tuple-element.89.columns, f32[80,256]{1,0:T(8,128)S(1)} %get-tuple-element.90.decays, f32[80,256]{1,0:T(8,128)S(1)} %get-tuple-element.91.keys, s32[1,80]{1,0:T(1,128)} %copy-done), custom_call_target="tpu_custom_call" | custom-call | flops 1048576 | bytes 67108864 | tf_op jit(solution)/shard_map/pallas_call | solution.py:372
  67.0 2.7 %shard_map.205._old = f32[2,80,128,256]{3,2,1,0:T(8,128)} custom-call(f32[40,128,256]{2,1,0:T(8,128)S(1)} %get-tuple-element.88.kept, f32[128,128]{1,0:T(8,128)S(1)} %get-tuple-element.89.columns, f32[80,256]{1,0:T(8,128)S(1)} %get-tuple-element.90.decays, f32[80,256]{1,0:T(8,128)S(1)} %get-tuple-element.91.keys, ...), custom_call_target="tpu_custom_call", output_to_operand_aliasing={{}: (4, {})} | custom-call | flops 1048576 | bytes 67108864 | tf_op jit(solution)/shard_map/pallas_call | solution.py:372
  69.6 2.7 %shard_map.206._old = f32[2,80,128,256]{3,2,1,0:T(8,128)} custom-call(f32[40,128,256]{2,1,0:T(8,128)S(1)} %shard_map.192.kept, f32[128,128]{1,0:T(8,128)S(1)} %get-tuple-element.85.columns, f32[80,256]{1,0:T(8,128)S(1)} %get-tuple-element.86.decays, f32[80,256]{1,0:T(8,128)S(1)} %get-tuple-element.87.keys, ...), custom_call_target="tpu_custom_call", output_to_operand_aliasing={{}: (4, {})} | custom-call | flops 1048576 | bytes 67108864 | tf_op jit(solution)/shard_map/pallas_call | solution.py:372
  72.3 2.7 %shard_map.207 = f32[2,80,128,256]{3,2,1,0:T(8,128)} custom-call(f32[40,128,256]{2,1,0:T(8,128)S(1)} %get-tuple-element.84.kept, f32[128,128]{1,0:T(8,128)S(1)} %get-tuple-element.85.columns, f32[80,256]{1,0:T(8,128)S(1)} %get-tuple-element.86.decays, f32[80,256]{1,0:T(8,128)S(1)} %get-tuple-element.87.keys, ...), custom_call_target="tpu_custom_call", output_to_operand_aliasing={{}: (4, {})} | custom-call | flops 1048576 | bytes 67108864 | tf_op jit(solution)/shard_map/pallas_call | solution.py:372
  75.0 0.0 collective-permute-done.22.far
  75.0 0.9 %shard_map.203 = bf16[80,128]{1,0:T(8,128)(2,1)} custom-call(bf16[8,80,128]{2,1,0:T(8,128)(2,1)S(1)} %constant_dynamic-update-slice_fusion.15.near, bf16[8,80,128]{2,1,0:T(8,128)(2,1)S(1)} %collective-permute-done.22.far, bf16[80,128]{1,0:T(8,128)(2,1)S(1)} %shard_map.198.current, bf16[2048,128]{1,0:T(8,128)(2,1)S(1)} %get-tuple-element.83.wo), custom_call_target="tpu_custom_call" | custom-call | flops 1048576 | bytes 67108864 | tf_op jit(solution)/shard_map/pallas_call | solution.py:385
  (24 shorter events, 0.2 us)
Async XLA Ops:
  0.6 5.6 %collective-permute-start = (bf16[1,80,128]{2,1,0:T(8,128)(2,1)}, bf16[1,80,128]{2,1,0:T(8,128)(2,1)S(1)}, u32[]{:S(2)}, u32[]{:S(2)}) collective-permute-start(bf16[1,80,128]{2,1,0:T(8,128)(2,1)} %bitcast.23), channel_id=1, source_target_pairs={{0,9},{1,8},{2,11},{3,10},{4,13},{5,12},{6,15},{7,14},{8,1},{9,0},... | collective-permute-start | bytes 61448 | tf_op jit(solution)/shard_map/ppermute | solution.py:41
  6.2 42.9 %copy-start = (s32[1,80]{1,0:T(1,128)}, s32[1,80]{1,0:T(1,128)S(1)}, u32[]{:S(2)}) copy-start(s32[1,80]{1,0:T(1,128)S(1)} %get-tuple-element.63.lengths._old) | copy-start | bytes 964
  6.3 5.1 %collective-permute-start.1 = (bf16[2,80,128]{2,1,0:T(8,128)(2,1)S(1)}, bf16[2,80,128]{2,1,0:T(8,128)(2,1)S(1)}, u32[]{:S(2)}, u32[]{:S(2)}) collective-permute-start(bf16[2,80,128]{2,1,0:T(8,128)(2,1)S(1)} %pad_maximum_fusion), channel_id=1, source_target_pairs={{0,6},{1,7},{2,4},{3,5},{4,2},{5,3},{6,0},{7,1},{8,14},{9,15},{10,... | collective-permute-start | bytes 122888 | tf_op jit(solution)/shard_map/ppermute | solution.py:41
  9.0 3.4 %collective-permute-start.2 = (bf16[2,80,128]{2,1,0:T(8,128)(2,1)S(1)}, bf16[2,80,128]{2,1,0:T(8,128)(2,1)S(1)}, u32[]{:S(2)}, u32[]{:S(2)}) collective-permute-start(bf16[2,80,128]{2,1,0:T(8,128)(2,1)S(1)} %pad_maximum_fusion), channel_id=1, source_target_pairs={{0,3},{1,2},{2,1},{3,0},{4,7},{5,6},{6,5},{7,4},{8,11},{9,10},{10,... | collective-permute-start | bytes 122888 | tf_op jit(solution)/shard_map/ppermute | solution.py:41
  9.4 3.4 %collective-permute-start.3 = (bf16[2,80,128]{2,1,0:T(8,128)(2,1)S(1)}, bf16[2,80,128]{2,1,0:T(8,128)(2,1)S(1)}, u32[]{:S(2)}, u32[]{:S(2)}) collective-permute-start(bf16[2,80,128]{2,1,0:T(8,128)(2,1)S(1)} %pad_maximum_fusion), channel_id=1, source_target_pairs={{0,5},{1,4},{2,7},{3,6},{4,1},{5,0},{6,3},{7,2},{8,13},{9,12},{10,... | collective-permute-start | bytes 122888 | tf_op jit(solution)/shard_map/ppermute | solution.py:41
  12.8 1.5 %collective-permute-start.4 = (bf16[8,80,128]{2,1,0:T(8,128)(2,1)S(1)}, bf16[8,80,128]{2,1,0:T(8,128)(2,1)S(1)}, u32[]{:S(2)}, u32[]{:S(2)}) collective-permute-start(bf16[8,80,128]{2,1,0:T(8,128)(2,1)S(1)} %constant_dynamic-update-slice_fusion.near), channel_id=1, source_target_pairs={{0,1},{1,0},{2,3},{3,2},{4,5},{5,4},{6,7},{7,6},{8,9},{9,8},{10,11... | collective-permute-start | bytes 491528 | tf_op jit(solution)/shard_map/ppermute | solution.py:41
  13.2 5.2 %collective-permute-start.6 = (f32[2,80,128]{2,1,0:T(8,128)S(1)}, f32[2,80,128]{2,1,0:T(8,128)S(1)}, u32[]{:S(2)}, u32[]{:S(2)}) collective-permute-start(f32[2,80,128]{2,1,0:T(8,128)S(1)} %get-tuple-element.54.refs_2_.refs_8_), channel_id=1, source_target_pairs={{0,1},{1,0},{2,3},{3,2},{4,5},{5,4},{6,7},{7,6},{8,9},{9,8},{10,11... | collective-permute-start | bytes 245768 | tf_op jit(solution)/shard_map/ppermute | solution.py:41
  14.7 3.6 %collective-permute-start.5 = (bf16[2,80,128]{2,1,0:T(8,128)(2,1)S(1)}, bf16[2,80,128]{2,1,0:T(8,128)(2,1)S(1)}, u32[]{:S(2)}, u32[]{:S(2)}) collective-permute-start(bf16[2,80,128]{2,1,0:T(8,128)(2,1)S(1)} %get-tuple-element.53.refs_0_), channel_id=1, source_target_pairs={{0,1},{1,0},{2,3},{3,2},{4,5},{5,4},{6,7},{7,6},{8,9},{9,8},{10,11... | collective-permute-start | bytes 122888 | tf_op jit(solution)/shard_map/ppermute | solution.py:41
  21.4 5.1 %collective-permute-start.7 = (bf16[1,80,128]{2,1,0:T(8,128)(2,1)S(1)}, bf16[1,80,128]{2,1,0:T(8,128)(2,1)S(1)}, u32[]{:S(2)}, u32[]{:S(2)}) collective-permute-start(bf16[1,80,128]{2,1,0:T(8,128)(2,1)S(1)} %bitcast.19), channel_id=1, source_target_pairs={{0,9},{1,8},{2,11},{3,10},{4,13},{5,12},{6,15},{7,14},{8,1},{9,0},... | collective-permute-start | bytes 61448 | tf_op jit(solution)/shard_map/ppermute | solution.py:41
  26.6 5.0 %collective-permute-start.8 = (bf16[2,80,128]{2,1,0:T(8,128)(2,1)S(1)}, bf16[2,80,128]{2,1,0:T(8,128)(2,1)S(1)}, u32[]{:S(2)}, u32[]{:S(2)}) collective-permute-start(bf16[2,80,128]{2,1,0:T(8,128)(2,1)S(1)} %pad_maximum_fusion.1), channel_id=1, source_target_pairs={{0,6},{1,7},{2,4},{3,5},{4,2},{5,3},{6,0},{7,1},{8,14},{9,15},{10,... | collective-permute-start | bytes 122888 | tf_op jit(solution)/shard_map/ppermute | solution.py:41
  27.6 4.3 %collective-permute-start.9 = (bf16[2,80,128]{2,1,0:T(8,128)(2,1)S(1)}, bf16[2,80,128]{2,1,0:T(8,128)(2,1)S(1)}, u32[]{:S(2)}, u32[]{:S(2)}) collective-permute-start(bf16[2,80,128]{2,1,0:T(8,128)(2,1)S(1)} %pad_maximum_fusion.1), channel_id=1, source_target_pairs={{0,3},{1,2},{2,1},{3,0},{4,7},{5,6},{6,5},{7,4},{8,11},{9,10},{10,... | collective-permute-start | bytes 122888 | tf_op jit(solution)/shard_map/ppermute | solution.py:41
  27.7 4.3 %collective-permute-start.10 = (bf16[2,80,128]{2,1,0:T(8,128)(2,1)S(1)}, bf16[2,80,128]{2,1,0:T(8,128)(2,1)S(1)}, u32[]{:S(2)}, u32[]{:S(2)}) collective-permute-start(bf16[2,80,128]{2,1,0:T(8,128)(2,1)S(1)} %pad_maximum_fusion.1), channel_id=1, source_target_pairs={{0,5},{1,4},{2,7},{3,6},{4,1},{5,0},{6,3},{7,2},{8,13},{9,12},{10,... | collective-permute-start | bytes 122888 | tf_op jit(solution)/shard_map/ppermute | solution.py:41
  32.0 1.5 %collective-permute-start.11 = (bf16[8,80,128]{2,1,0:T(8,128)(2,1)S(1)}, bf16[8,80,128]{2,1,0:T(8,128)(2,1)S(1)}, u32[]{:S(2)}, u32[]{:S(2)}) collective-permute-start(bf16[8,80,128]{2,1,0:T(8,128)(2,1)S(1)} %constant_dynamic-update-slice_fusion.5.near), channel_id=1, source_target_pairs={{0,1},{1,0},{2,3},{3,2},{4,5},{5,4},{6,7},{7,6},{8,9},{9,8},{10,11... | collective-permute-start | bytes 491528 | tf_op jit(solution)/shard_map/ppermute | solution.py:41
  33.7 4.2 %collective-permute-start.12 = (bf16[1,80,128]{2,1,0:T(8,128)(2,1)S(1)}, bf16[1,80,128]{2,1,0:T(8,128)(2,1)S(1)}, u32[]{:S(2)}, u32[]{:S(2)}) collective-permute-start(bf16[1,80,128]{2,1,0:T(8,128)(2,1)S(1)} %bitcast.14), channel_id=1, source_target_pairs={{0,9},{1,8},{2,11},{3,10},{4,13},{5,12},{6,15},{7,14},{8,1},{9,0},... | collective-permute-start | bytes 61448 | tf_op jit(solution)/shard_map/ppermute | solution.py:41
  37.9 4.9 %collective-permute-start.13 = (bf16[2,80,128]{2,1,0:T(8,128)(2,1)S(1)}, bf16[2,80,128]{2,1,0:T(8,128)(2,1)S(1)}, u32[]{:S(2)}, u32[]{:S(2)}) collective-permute-start(bf16[2,80,128]{2,1,0:T(8,128)(2,1)S(1)} %pad_maximum_fusion.2), channel_id=1, source_target_pairs={{0,6},{1,7},{2,4},{3,5},{4,2},{5,3},{6,0},{7,1},{8,14},{9,15},{10,... | collective-permute-start | bytes 122888 | tf_op jit(solution)/shard_map/ppermute | solution.py:41
  39.6 4.0 %collective-permute-start.14 = (bf16[2,80,128]{2,1,0:T(8,128)(2,1)S(1)}, bf16[2,80,128]{2,1,0:T(8,128)(2,1)S(1)}, u32[]{:S(2)}, u32[]{:S(2)}) collective-permute-start(bf16[2,80,128]{2,1,0:T(8,128)(2,1)S(1)} %pad_maximum_fusion.2), channel_id=1, source_target_pairs={{0,3},{1,2},{2,1},{3,0},{4,7},{5,6},{6,5},{7,4},{8,11},{9,10},{10,... | collective-permute-start | bytes 122888 | tf_op jit(solution)/shard_map/ppermute | solution.py:41
  40.3 3.4 %collective-permute-start.15 = (bf16[2,80,128]{2,1,0:T(8,128)(2,1)S(1)}, bf16[2,80,128]{2,1,0:T(8,128)(2,1)S(1)}, u32[]{:S(2)}, u32[]{:S(2)}) collective-permute-start(bf16[2,80,128]{2,1,0:T(8,128)(2,1)S(1)} %pad_maximum_fusion.2), channel_id=1, source_target_pairs={{0,5},{1,4},{2,7},{3,6},{4,1},{5,0},{6,3},{7,2},{8,13},{9,12},{10,... | collective-permute-start | bytes 122888 | tf_op jit(solution)/shard_map/ppermute | solution.py:41
  43.7 2.2 %collective-permute-start.16 = (bf16[8,80,128]{2,1,0:T(8,128)(2,1)S(1)}, bf16[8,80,128]{2,1,0:T(8,128)(2,1)S(1)}, u32[]{:S(2)}, u32[]{:S(2)}) collective-permute-start(bf16[8,80,128]{2,1,0:T(8,128)(2,1)S(1)} %constant_dynamic-update-slice_fusion.10.near), channel_id=1, source_target_pairs={{0,1},{1,0},{2,3},{3,2},{4,5},{5,4},{6,7},{7,6},{8,9},{9,8},{10,11... | collective-permute-start | bytes 491528 | tf_op jit(solution)/shard_map/ppermute | solution.py:41
  46.4 3.8 %collective-permute-start.17 = (bf16[2,80,128]{2,1,0:T(8,128)(2,1)S(1)}, bf16[2,80,128]{2,1,0:T(8,128)(2,1)S(1)}, u32[]{:S(2)}, u32[]{:S(2)}) collective-permute-start(bf16[2,80,128]{2,1,0:T(8,128)(2,1)S(1)} %get-tuple-element.73.refs_0_), channel_id=1, source_target_pairs={{0,1},{1,0},{2,3},{3,2},{4,5},{5,4},{6,7},{7,6},{8,9},{9,8},{10,11... | collective-permute-start | bytes 122888 | tf_op jit(solution)/shard_map/ppermute | solution.py:41
  53.9 4.2 %collective-permute-start.18 = (bf16[1,80,128]{2,1,0:T(8,128)(2,1)S(1)}, bf16[1,80,128]{2,1,0:T(8,128)(2,1)S(1)}, u32[]{:S(2)}, u32[]{:S(2)}) collective-permute-start(bf16[1,80,128]{2,1,0:T(8,128)(2,1)S(1)} %bitcast.17), channel_id=1, source_target_pairs={{0,9},{1,8},{2,11},{3,10},{4,13},{5,12},{6,15},{7,14},{8,1},{9,0},... | collective-permute-start | bytes 61448 | tf_op jit(solution)/shard_map/ppermute | solution.py:41
  58.1 5.2 %collective-permute-start.19 = (bf16[2,80,128]{2,1,0:T(8,128)(2,1)S(1)}, bf16[2,80,128]{2,1,0:T(8,128)(2,1)S(1)}, u32[]{:S(2)}, u32[]{:S(2)}) collective-permute-start(bf16[2,80,128]{2,1,0:T(8,128)(2,1)S(1)} %pad_maximum_fusion.3), channel_id=1, source_target_pairs={{0,6},{1,7},{2,4},{3,5},{4,2},{5,3},{6,0},{7,1},{8,14},{9,15},{10,... | collective-permute-start | bytes 122888 | tf_op jit(solution)/shard_map/ppermute | solution.py:41
  59.5 4.5 %collective-permute-start.20 = (bf16[2,80,128]{2,1,0:T(8,128)(2,1)S(1)}, bf16[2,80,128]{2,1,0:T(8,128)(2,1)S(1)}, u32[]{:S(2)}, u32[]{:S(2)}) collective-permute-start(bf16[2,80,128]{2,1,0:T(8,128)(2,1)S(1)} %pad_maximum_fusion.3), channel_id=1, source_target_pairs={{0,3},{1,2},{2,1},{3,0},{4,7},{5,6},{6,5},{7,4},{8,11},{9,10},{10,... | collective-permute-start | bytes 122888 | tf_op jit(solution)/shard_map/ppermute | solution.py:41
  60.0 4.0 %collective-permute-start.21 = (bf16[2,80,128]{2,1,0:T(8,128)(2,1)S(1)}, bf16[2,80,128]{2,1,0:T(8,128)(2,1)S(1)}, u32[]{:S(2)}, u32[]{:S(2)}) collective-permute-start(bf16[2,80,128]{2,1,0:T(8,128)(2,1)S(1)} %pad_maximum_fusion.3), channel_id=1, source_target_pairs={{0,5},{1,4},{2,7},{3,6},{4,1},{5,0},{6,3},{7,2},{8,13},{9,12},{10,... | collective-permute-start | bytes 122888 | tf_op jit(solution)/shard_map/ppermute | solution.py:41
  64.1 10.9 %collective-permute-start.22 = (bf16[8,80,128]{2,1,0:T(8,128)(2,1)S(1)}, bf16[8,80,128]{2,1,0:T(8,128)(2,1)S(1)}, u32[]{:S(2)}, u32[]{:S(2)}) collective-permute-start(bf16[8,80,128]{2,1,0:T(8,128)(2,1)S(1)} %constant_dynamic-update-slice_fusion.15.near), channel_id=1, source_target_pairs={{0,1},{1,0},{2,3},{3,2},{4,5},{5,4},{6,7},{7,6},{8,9},{9,8},{10,11... | collective-permute-start | bytes 491528 | tf_op jit(solution)/shard_map/ppermute | solution.py:41

commit v3 on v2

--- a/solution.py
+++ b/solution.py
@@ -11,6 +11,9 @@
 MAXLEN = 4096
 EPS = 1e-05
 MIB = 1 << 20
+LANES = 128
+EARLY = (6, 5)
+DIRECT = 4
 BYTES = 1 << 26
 
 
@@ -31,7 +34,7 @@
     for at in range(0, len(middle), 2):
         pair = middle[at : at + 2]
         if len(pair) == 2:
-            rounds.append((pair[0] | pair[1], pair[1] | low, pair[0] | low))
+            rounds.append((pair[0] | pair[1] | low, pair[1] | low, pair[0] | low))
         else:
             rounds.append((pair[0] | low,))
     return rounds + [(low,)]
@@ -102,7 +105,7 @@
 
 
 def gates_kernel(
-    layer, split, normed, wv, wo, wi, wf, ibias, fbias, slope, lengths, stab, old,
+    layer, split, normed, wv, wo, wi, wf, ibias, fbias, slope, lengths, stab,
     values, outgate, factors, stab_new, columns, decays,
 ):
     n = normed[...]
@@ -120,9 +123,7 @@
     forget = jax.nn.log_sigmoid(logits(wf) + as_column(fbias[row]) + as_column(slope[row]) * position)
     held = forget + stab[layer]
     top = jnp.maximum(held, ingate)
-    for other in range(layer):
-        stab_new[other] = old[other]
-    stab_new[layer] = top
+    stab_new[...] = top
     index = lax.broadcasted_iota(jnp.int32, top.shape, 0)
     mine = index == lax.axis_index("tp") // split
     decay = jnp.sum(jnp.where(mine, jnp.exp(held - top), 0.0), axis=0, keepdims=True)
@@ -145,9 +146,9 @@
 def read_kernel(layer, split, rows, memory, kept, *refs):
     pairs, refs = refs[:split], refs[split:]
     sums, refs = refs[:split], refs[split:]
-    values, outgate, factors, gain, old, gated, sums_new, keys, rest, query, pieces, arrived = refs
+    values, outgate, factors, gain, gated, sums_new, keys, rest, query, pieces, arrived = refs
     (first, width, depth), batch = kept.shape, values.shape[0]
-    lanes = -(-batch // 128) * 128
+    lanes = -(-batch // LANES) * LANES
 
     def fetch(i):
         part = pl.ds(i * rows, rows)
@@ -162,12 +163,22 @@
     keys[...] = key
     lane = lax.broadcasted_iota(jnp.int32, (width, lanes), 1)
 
+    ones = jnp.ones((LANES, LANES), BF16)
+    direct = rows * DIRECT // 8
+
     def add(state, i, at, total):
+        products = []
         for r in range(rows):
-            b = at + i * rows + r
-            product = state[i * rows + r] * query[pl.ds(b, 1), :]
-            column = jnp.sum(product, axis=1, keepdims=True)
-            total = jnp.where(lane == b, column, total)
+            x = state[i * rows + r] * query[pl.ds(at + i * rows + r, 1), :]
+            products.append(sum(x[:, j : j + LANES] for j in range(0, depth, LANES)))
+        if direct < rows:
+            summed = dot(jnp.concatenate(products[direct:], axis=0).astype(BF16), ones)
+        for r in range(rows):
+            if r < direct:
+                column = jnp.sum(products[r], axis=1, keepdims=True)
+            else:
+                column = summed[(r - direct) * width : (r - direct + 1) * width]
+            total = jnp.where(lane == at + i * rows + r, column, total)
         return total
 
     def late(i, total):
@@ -187,9 +198,7 @@
     hidden = numerator / jnp.maximum(jnp.abs(below), 1.0)
     gate = jax.nn.sigmoid(outgate[...].astype(F32))
     gated[...] = (hidden * gain[layer : layer + 1].astype(F32) * gate).astype(BF16)
-    for other in range(layer):
-        sums_new[other] = old[other]
-    sums_new[layer] = decay * sums[0][layer] + weight * pairs[0][1].astype(F32)
+    sums_new[...] = decay * sums[0][layer] + weight * pairs[0][1].astype(F32)
 
 
 def out_kernel(masks, low, near, far, current, wo, after, rows):
@@ -198,27 +207,54 @@
     after[...] = total.astype(BF16)
 
 
-def update_kernel(layer, first, rows, kept, columns, decays, keys, _old, new, staged, sent):
-    batch, width, depth = kept.shape
+def update_kernel(layer, start, count, rows, kept, rest, columns, decays, keys, _old, new, staged, sent):
+    first, width, depth = kept.shape
     lanes = columns.shape[1]
 
     def send(i):
         part = pl.ds(i * rows, rows)
-        return pltpu.make_async_copy(staged.at[part], new.at[layer, pl.ds(first + i * rows, rows)], sent.at[i])
-
-    def some(i, carry):
-        at = first + i * rows
-        turned = pltpu.roll(columns[...], lanes - at, axis=1)
+        return pltpu.make_async_copy(staged.at[part], new.at[layer, pl.ds(start + i * rows, rows)], sent.at[i])
+
+    lane = lax.broadcasted_iota(jnp.int32, columns.shape, 1)
+    direct = rows * DIRECT // 8
+    operand = keys[...].astype(BF16)
+    if lanes > keys.shape[0]:
+        operand = jnp.concatenate([operand, jnp.zeros((lanes - keys.shape[0], depth), BF16)], axis=0)
+
+    def some(state, skipped, i, carry):
+        at = start + i * rows
+        if direct < rows:
+            chosen = [jnp.where(lane == at + r, columns[...], 0.0).astype(BF16) for r in range(direct, rows)]
+            outer = dot(jnp.concatenate(chosen, axis=0), operand)
+        if direct:
+            turned = pltpu.roll(columns[...], lanes - at, axis=1)
         for r in range(rows):
-            column = jnp.broadcast_to(turned[:, r : r + 1], (width, depth))
-            key = keys[pl.ds(at + r, 1), :]
-            staged[i * rows + r] = decays[pl.ds(at + r, 1), :] * kept[i * rows + r] + column * key
+            if r < direct:
+                added = jnp.broadcast_to(turned[:, r : r + 1], (width, depth)) * keys[pl.ds(at + r, 1), :]
+            else:
+                added = outer[(r - direct) * width : (r - direct + 1) * width]
+            staged[i * rows + r] = decays[pl.ds(at + r, 1), :] * state[at - skipped + r] + added
         send(i).start()
         return carry
 
-    lax.fori_loop(0, batch // rows, some, 0)
-    for i in range(batch // rows):
+    steps = count // rows
+    middle = min(max((first - start) // rows, 0), steps)
+    lax.fori_loop(0, middle, functools.partial(some, kept, 0), 0)
+    lax.fori_loop(middle, steps, functools.partial(some, rest, first), 0)
+    for i in range(steps):
         send(i).wait()
+
+
+def store_kernel(blocks, *refs):
+    parts, (sums, stab, sent) = refs[: 2 * blocks], refs[2 * blocks :]
+    copies = []
+    for i, part in enumerate(parts):
+        target = sums.at[i] if i < blocks else stab.at[i - blocks]
+        copies.append(pltpu.make_async_copy(part, target, sent.at[i]))
+    for copy in copies:
+        copy.start()
+    for copy in copies:
+        copy.wait()
 
 
 def in_hbm(x):
@@ -292,9 +328,8 @@
 
     shape = jax.ShapeDtypeStruct
     rows = 8 if batch % 8 == 0 else 1
-    lanes = -(-batch // 128) * 128
-    first = batch // rows // 2 * rows
-    sizes = (first, batch - first)
+    lanes = -(-batch // LANES) * LANES
+    sizes = (batch // rows // 2 * rows, batch - batch // rows // 2 * rows)
     weights = [query_weight, key_weight, value_weight, outgate_weight, output_weight]
     own_sums, wi, wf, ibias, fbias, slope, at, stab, norm_gain, head_gain, current, *loaded = load(
         0,
@@ -316,12 +351,13 @@
     near, far, masks, low = gather(tokens, current)
     sums = pieces(own_sums)
     memory = in_hbm(cell_memory)
-    new_memory, new_sums, new_stab = at, own_sums, stab
+    new_memory, sums_out, stabs = at, [], []
     for layer in range(blocks):
         if layer:
             near, far, masks, low = gather(current, current)
             loaded = load(layer, [], weights)
         wq, wk, wv, wg, wo = loaded
+        first = batch // rows * EARLY[layer > 0] // 10 * rows
         kept = call(
             functools.partial(state_kernel, layer, rows),
             pltpu.VMEM((first, width, depth), F32),
@@ -343,44 +379,43 @@
                 shape((batch, width), BF16),
                 shape((batch, width), BF16),
                 shape((batch, heads), F32),
-                shape(stab.shape, F32),
+                pltpu.VMEM(stab.shape[1:], F32),
                 pltpu.VMEM((width, lanes), F32),
                 pltpu.VMEM((batch, depth), F32),
             ),
-            [VM] * 11,
+            [VM] * 10,
             (VM,) * 6,
-        )(normed, wv, wg, wi, wf, ibias, fbias, slope, at, stab, new_stab)
+        )(normed, wv, wg, wi, wf, ibias, fbias, slope, at, stab)
+        stabs.append(new_stab)
         gated, new_sums, keys, rest = call(
             functools.partial(read_kernel, layer, split, rows),
             (
                 shape((batch, width), BF16),
-                shape(own_sums.shape, F32),
+                pltpu.VMEM((batch, width), F32),
                 pltpu.VMEM((batch, depth), F32),
                 pltpu.VMEM((batch - first, width, depth), F32),
             ),
-            [HBM] + [VM] * (6 + 2 * split),
+            [HBM] + [VM] * (5 + 2 * split),
             (VM,) * 4,
             [
                 pltpu.VMEM((batch, depth), F32),
                 pltpu.VMEM((split, 2, batch, width), BF16),
                 pltpu.SemaphoreType.DMA(((batch - first) // rows,)),
             ],
-        )(memory, kept, *pairs, *sums, values, outgate, factors, head_gain, new_sums)
+        )(memory, kept, *pairs, *sums, values, outgate, factors, head_gain)
+        sums_out.append(new_sums)
 
         near, far, masks, low = gather(gated, gated)
-        for part, state in enumerate((kept, rest)):
+        for part, size in enumerate(sizes):
             new_memory = call(
-                functools.partial(update_kernel, layer, part * first, rows),
+                functools.partial(update_kernel, layer, part * sizes[0], size, rows),
                 shape(cell_memory.shape, F32),
-                [VM] * 4 + [HBM],
+                [VM] * 5 + [HBM],
                 HBM,
-                [
-                    pltpu.VMEM((sizes[part], width, depth), F32),
-                    pltpu.SemaphoreType.DMA((sizes[part] // rows,)),
-                ],
-                {} if layer == part == 0 else {4: 0},
+                [pltpu.VMEM((size, width, depth), F32), pltpu.SemaphoreType.DMA((size // rows,))],
+                {} if layer == part == 0 else {5: 0},
                 limit=8,
-            )(state, columns, decays, keys, in_hbm(new_memory))
+            )(kept, rest, columns, decays, keys, in_hbm(new_memory))
 
         current = call(
             functools.partial(out_kernel, masks, low),
@@ -389,6 +424,13 @@
             VM,
             [pltpu.VMEM((count, batch, width), BF16)],
         )(near, far, current, wo)
+    new_sums, new_stab = call(
+        functools.partial(store_kernel, blocks),
+        (shape(own_sums.shape, F32), shape(stab.shape, F32)),
+        [VM] * (2 * blocks),
+        (HBM, HBM),
+        [pltpu.SemaphoreType.DMA((2 * blocks,))],
+    )(*sums_out, *stabs)
     return current, new_memory, new_sums, jnp.swapaxes(new_stab, 1, 2)
 
 

time: 76.1 us -> 75.3 us (0.989)
    pallas_call x2, Pallas kernels: 6.7 us -> 5.71 us  [body(): call(functools.partial(read_kernel, layer, split, rows), (shape((batch, w...]
    pallas_call x4 -> x5, Pallas kernels: 10.7 us -> 11.3 us  [the longest x4 10.6 us: body(): call(functools.partial(update_kernel, layer, part * sizes[0], size, rows)...]
  transfers between devices with their start and end apart: 23 -> 23, of which waited for: 15 -> 16; matrix products, arithmetic and copies ran while one was open for 0% -> 0% of each run, Pallas kernels for 29% -> 30%
where the time goes in v3:
time: 75.3 us; the launch traced here: 75.1 us
  Pallas kernels  29.7 us (39%)
  starting transfers between devices  26.5 us (35%)
  waiting for transfers between devices  17.9 us (24%)
  between operations  0.82 us (1%)
    ppermute x23, starting transfers between devices, swap(): lax.ppermute(value, 'tp', [(s, s ^ mask) for s in range(lax.axis_size('tp...  26.5 us
    ppermute x23, waiting for transfers between devices, swap(): lax.ppermute(value, 'tp', [(s, s ^ mask) for s in range(lax.axis_size('tp...  17.9 us
    pallas_call x4, Pallas kernels, body(): call(functools.partial(update_kernel, layer, part * sizes[0], size, rows)...  10.6 us
    pallas_call x2, Pallas kernels, body(): call(functools.partial(read_kernel, layer, split, rows), (shape((batch, w...  5.71 us
    pallas_call x2, Pallas kernels, body(): call(functools.partial(state_kernel, layer, rows), pltpu.VMEM((first, wid...  5.38 us
    pallas_call x2, Pallas kernels, load(): call(functools.partial(load_kernel, layer, len(whole), len(sliced)), tupl...  3.74 us
    pallas_call x2, Pallas kernels, body(): call(functools.partial(gates_kernel, layer, split), (shape((batch, width)...  1.53 us
  transfers between devices with their start and end apart: 23, of which 16 were waited for; matrix products, arithmetic and copies ran while one was open for 0% of the time, Pallas kernels for 30%

profile of v3, /device:TPU:0, one launch (start us, length us, event | category | flops | bytes accessed | tf_op | source)
XLA Modules:
  0.0 75.1 jit_solution(15391988170439369319)
XLA Ops:
  0.6 3.6 %collective-permute-start = (bf16[1,80,128]{2,1,0:T(8,128)(2,1)}, bf16[1,80,128]{2,1,0:T(8,128)(2,1)S(1)}, u32[]{:S(2)}, u32[]{:S(2)}) collective-permute-start(bf16[1,80,128]{2,1,0:T(8,128)(2,1)} %bitcast.23), channel_id=1, source_target_pairs={{0,9},{1,8},{2,11},{3,10},{4,13},{5,12},{6,15},{7,14},{8,1},{9,0},... | collective-permute-start | bytes 61448 | tf_op jit(solution)/shard_map/ppermute | solution.py:44
  4.2 2.0 %shard_map.194 = (f32[2,80,128]{2,1,0:T(8,128)S(1)}, bf16[2,8,2048]{2,1,0:T(8,128)(2,1)S(1)}, bf16[2,8,2048]{2,1,0:T(8,128)(2,1)S(1)}, f32[2,8]{1,0:T(2,128)S(1)...) custom-call(f32[2,80,128]{2,1,0:T(8,128)} %refs_0_.2, ...), custom_call_target="tpu_custom_call" | custom-call | flops 1048576 | bytes 67108864 | tf_op jit(solution)/shard_map/pallas_call | solution.py:279
  6.2 0.0 copy-start
  6.3 0.0 collective-permute-done
  6.3 2.9 %collective-permute-start.1 = (bf16[2,80,128]{2,1,0:T(8,128)(2,1)S(1)}, bf16[2,80,128]{2,1,0:T(8,128)(2,1)S(1)}, u32[]{:S(2)}, u32[]{:S(2)}) collective-permute-start(bf16[2,80,128]{2,1,0:T(8,128)(2,1)S(1)} %pad_maximum_fusion), channel_id=1, source_target_pairs={{0,7},{1,6},{2,5},{3,4},{4,3},{5,2},{6,1},{7,0},{8,15},{9,14},{10,... | collective-permute-start | bytes 122888 | tf_op jit(solution)/shard_map/ppermute | solution.py:44
  9.2 0.1 collective-permute-start.2
  9.3 0.6 collective-permute-start.3
  9.9 1.2 %collective-permute-done.1 = bf16[2,80,128]{2,1,0:T(8,128)(2,1)S(1)} collective-permute-done((bf16[2,80,128]{2,1,0:T(8,128)(2,1)S(1)}, bf16[2,80,128]{2,1,0:T(8,128)(2,1)S(1)}, u32[]{:S(2)}, u32[]{:S(2)}) %collective-permute-start.1) | collective-permute-done | bytes 40992 | tf_op jit(solution)/shard_map/ppermute | solution.py:44
  11.1 1.8 %collective-permute-done.2 = bf16[2,80,128]{2,1,0:T(8,128)(2,1)S(1)} collective-permute-done((bf16[2,80,128]{2,1,0:T(8,128)(2,1)S(1)}, bf16[2,80,128]{2,1,0:T(8,128)(2,1)S(1)}, u32[]{:S(2)}, u32[]{:S(2)}) %collective-permute-start.2) | collective-permute-done | bytes 40992 | tf_op jit(solution)/shard_map/ppermute | solution.py:44
  12.9 0.0 collective-permute-done.3
  12.9 0.4 collective-permute-start.4
  13.3 0.2 collective-permute-start.6
  13.5 0.9 %collective-permute-done.4.far = bf16[8,80,128]{2,1,0:T(8,128)(2,1)S(1)} collective-permute-done((bf16[8,80,128]{2,1,0:T(8,128)(2,1)S(1)}, bf16[8,80,128]{2,1,0:T(8,128)(2,1)S(1)}, u32[]{:S(2)}, u32[]{:S(2)}) %collective-permute-start.4) | collective-permute-done | bytes 163872 | tf_op jit(solution)/shard_map/ppermute | solution.py:44
  14.4 0.5 shard_map.195
  14.8 0.4 collective-permute-start.5
  15.2 2.9 %shard_map.193.kept = f32[48,128,256]{2,1,0:T(8,128)S(1)} custom-call(f32[2,80,128,256]{3,2,1,0:T(8,128)} %memory.7), custom_call_target="tpu_custom_call" | custom-call | flops 1048576 | bytes 67108864 | tf_op jit(solution)/shard_map/pallas_call | solution.py:361
  18.1 0.8 %shard_map.196 = (bf16[80,128]{1,0:T(8,128)(2,1)S(1)}, bf16[80,128]{1,0:T(8,128)(2,1)S(1)}, f32[80,8]{1,0:T(8,128)S(1)}, f32[8,80]{1,0:T(8,128)S(1)}, f32[128,128]{1,0:T(8,128)S(1)}, /*index=5*/f32[80,256]{1,0:T(8,128)S(1)}) custom-call(bf16[80,2048]{1,0:T(8,128)(2,1)S(1)} %get-tuple-element.57.normed, bf16[2048,128]{1,0:T(8,128)(2,1)S(1)} %get-tuple-element.58.wv, ...), custom_call_target="tpu_custom_call" | custom-call | flops 1048576 | bytes 67108864 | tf_op jit(solution)/shard_map/pallas_call | solution.py:376
  18.8 0.0 collective-permute-done.6.refs_3_
  18.8 0.0 collective-permute-done.5.refs_1_
  18.8 2.7 %shard_map.197 = (bf16[80,128]{1,0:T(8,128)(2,1)S(1)}, f32[80,128]{1,0:T(8,128)S(1)}, f32[80,256]{1,0:T(8,128)S(1)}, f32[32,128,256]{2,1,0:T(8,128)S(1)}) custom-call(f32[2,80,128,256]{3,2,1,0:T(8,128)} %memory.7, f32[48,128,256]{2,1,0:T(8,128)S(1)} %shard_map.193.kept, bf16[2,80,128]{2,1,0:T(8,128)(2,1)S(1)} %get-tuple-element.55.refs_0_, ...), custom_call_target="tpu_custom_call" | custom-call | flops 1048576 | bytes 67108864 | tf_op jit(solution)/shard_map/pallas_call | solution.py:390
  21.5 2.9 %collective-permute-start.7 = (bf16[1,80,128]{2,1,0:T(8,128)(2,1)S(1)}, bf16[1,80,128]{2,1,0:T(8,128)(2,1)S(1)}, u32[]{:S(2)}, u32[]{:S(2)}) collective-permute-start(bf16[1,80,128]{2,1,0:T(8,128)(2,1)S(1)} %bitcast.19), channel_id=1, source_target_pairs={{0,9},{1,8},{2,11},{3,10},{4,13},{5,12},{6,15},{7,14},{8,1},{9,0},... | collective-permute-start | bytes 61448 | tf_op jit(solution)/shard_map/ppermute | solution.py:44
  24.5 1.7 %collective-permute-done.7 = bf16[1,80,128]{2,1,0:T(8,128)(2,1)S(1)} collective-permute-done((bf16[1,80,128]{2,1,0:T(8,128)(2,1)S(1)}, bf16[1,80,128]{2,1,0:T(8,128)(2,1)S(1)}, u32[]{:S(2)}, u32[]{:S(2)}) %collective-permute-start.7) | collective-permute-done | bytes 20512 | tf_op jit(solution)/shard_map/ppermute | solution.py:44
  26.2 0.7 collective-permute-start.8
  26.9 1.0 %collective-permute-start.9 = (bf16[2,80,128]{2,1,0:T(8,128)(2,1)S(1)}, bf16[2,80,128]{2,1,0:T(8,128)(2,1)S(1)}, u32[]{:S(2)}, u32[]{:S(2)}) collective-permute-start(bf16[2,80,128]{2,1,0:T(8,128)(2,1)S(1)} %pad_maximum_fusion.1), channel_id=1, source_target_pairs={{0,3},{1,2},{2,1},{3,0},{4,7},{5,6},{6,5},{7,4},{8,11},{9,10},{10,... | collective-permute-start | bytes 122888 | tf_op jit(solution)/shard_map/ppermute | solution.py:44
  27.9 1.4 %collective-permute-start.10 = (bf16[2,80,128]{2,1,0:T(8,128)(2,1)S(1)}, bf16[2,80,128]{2,1,0:T(8,128)(2,1)S(1)}, u32[]{:S(2)}, u32[]{:S(2)}) collective-permute-start(bf16[2,80,128]{2,1,0:T(8,128)(2,1)S(1)} %pad_maximum_fusion.1), channel_id=1, source_target_pairs={{0,5},{1,4},{2,7},{3,6},{4,1},{5,0},{6,3},{7,2},{8,13},{9,12},{10,... | collective-permute-start | bytes 122888 | tf_op jit(solution)/shard_map/ppermute | solution.py:44
  29.2 1.4 %collective-permute-done.8 = bf16[2,80,128]{2,1,0:T(8,128)(2,1)S(1)} collective-permute-done((bf16[2,80,128]{2,1,0:T(8,128)(2,1)S(1)}, bf16[2,80,128]{2,1,0:T(8,128)(2,1)S(1)}, u32[]{:S(2)}, u32[]{:S(2)}) %collective-permute-start.8) | collective-permute-done | bytes 40992 | tf_op jit(solution)/shard_map/ppermute | solution.py:44
  30.7 0.6 collective-permute-done.9
  31.3 0.4 collective-permute-done.10
  31.7 0.2 collective-permute-start.11
  31.9 1.3 %collective-permute-done.11.far = bf16[8,80,128]{2,1,0:T(8,128)(2,1)S(1)} collective-permute-done((bf16[8,80,128]{2,1,0:T(8,128)(2,1)S(1)}, bf16[8,80,128]{2,1,0:T(8,128)(2,1)S(1)}, u32[]{:S(2)}, u32[]{:S(2)}) %collective-permute-start.11) | collective-permute-done | bytes 163872 | tf_op jit(solution)/shard_map/ppermute | solution.py:44
  33.2 0.3 shard_map.198.current
  33.5 2.3 %collective-permute-start.12 = (bf16[1,80,128]{2,1,0:T(8,128)(2,1)S(1)}, bf16[1,80,128]{2,1,0:T(8,128)(2,1)S(1)}, u32[]{:S(2)}, u32[]{:S(2)}) collective-permute-start(bf16[1,80,128]{2,1,0:T(8,128)(2,1)S(1)} %bitcast.14), channel_id=1, source_target_pairs={{0,9},{1,8},{2,11},{3,10},{4,13},{5,12},{6,15},{7,14},{8,1},{9,0},... | collective-permute-start | bytes 61448 | tf_op jit(solution)/shard_map/ppermute | solution.py:44
  35.8 1.9 %collective-permute-done.12 = bf16[1,80,128]{2,1,0:T(8,128)(2,1)S(1)} collective-permute-done((bf16[1,80,128]{2,1,0:T(8,128)(2,1)S(1)}, bf16[1,80,128]{2,1,0:T(8,128)(2,1)S(1)}, u32[]{:S(2)}, u32[]{:S(2)}) %collective-permute-start.12) | collective-permute-done | bytes 20512 | tf_op jit(solution)/shard_map/ppermute | solution.py:44
  37.6 2.0 %collective-permute-start.13 = (bf16[2,80,128]{2,1,0:T(8,128)(2,1)S(1)}, bf16[2,80,128]{2,1,0:T(8,128)(2,1)S(1)}, u32[]{:S(2)}, u32[]{:S(2)}) collective-permute-start(bf16[2,80,128]{2,1,0:T(8,128)(2,1)S(1)} %pad_maximum_fusion.2), channel_id=1, source_target_pairs={{0,7},{1,6},{2,5},{3,4},{4,3},{5,2},{6,1},{7,0},{8,15},{9,14},{10,... | collective-permute-start | bytes 122888 | tf_op jit(solution)/shard_map/ppermute | solution.py:44
  39.6 0.3 collective-permute-start.14
  40.0 0.7 collective-permute-start.15
  40.6 1.5 %collective-permute-done.13 = bf16[2,80,128]{2,1,0:T(8,128)(2,1)S(1)} collective-permute-done((bf16[2,80,128]{2,1,0:T(8,128)(2,1)S(1)}, bf16[2,80,128]{2,1,0:T(8,128)(2,1)S(1)}, u32[]{:S(2)}, u32[]{:S(2)}) %collective-permute-start.13) | collective-permute-done | bytes 40992 | tf_op jit(solution)/shard_map/ppermute | solution.py:44
  42.1 1.0 %collective-permute-done.14 = bf16[2,80,128]{2,1,0:T(8,128)(2,1)S(1)} collective-permute-done((bf16[2,80,128]{2,1,0:T(8,128)(2,1)S(1)}, bf16[2,80,128]{2,1,0:T(8,128)(2,1)S(1)}, u32[]{:S(2)}, u32[]{:S(2)}) %collective-permute-start.14) | collective-permute-done | bytes 40992 | tf_op jit(solution)/shard_map/ppermute | solution.py:44
  43.1 0.3 collective-permute-done.15
  43.4 0.3 collective-permute-start.16
  43.7 1.7 %shard_map.199 = (bf16[2048,128]{1,0:T(8,128)(2,1)S(1)}, bf16[2048,128]{1,0:T(8,128)(2,1)S(1)}, bf16[2048,128]{1,0:T(8,128)(2,1)S(1)}, bf16[2048,128]{1,0:T(8,128)(2,1)S(1)}, bf16[2048,128]{1,0:T(8,128)(2,1)S(1)}) custom-call(bf16[2,2048,128]{2,1,0:T(8,128)(2,1)} %refs_0_.3, bf16[2,2048,128]{2,1,0:T(8,128)(2,1)} %refs_1_.1, bf16[2,2048,128]{2,1,0:T(8,128)(2,1)} %refs_2_.1, ...), custom_call_target="tpu_custom_call" | custom-call | flops 1048576 | bytes 67108864 | tf_op jit(solution)/shard_map/pallas_call | solution.py:279
  45.4 0.0 collective-permute-done.16.far
  45.4 0.5 shard_map.200
  45.9 0.3 collective-permute-start.17
  46.2 2.5 %shard_map.192.kept = f32[40,128,256]{2,1,0:T(8,128)S(1)} custom-call(f32[2,80,128,256]{3,2,1,0:T(8,128)} %memory.7), custom_call_target="tpu_custom_call" | custom-call | flops 1048576 | bytes 67108864 | tf_op jit(solution)/shard_map/pallas_call | solution.py:361
  48.8 0.8 %shard_map.201 = (bf16[80,128]{1,0:T(8,128)(2,1)S(1)}, bf16[80,128]{1,0:T(8,128)(2,1)S(1)}, f32[80,8]{1,0:T(8,128)S(1)}, f32[8,80]{1,0:T(8,128)S(1)}, f32[128,128]{1,0:T(8,128)S(1)}, /*index=5*/f32[80,256]{1,0:T(8,128)S(1)}) custom-call(bf16[80,2048]{1,0:T(8,128)(2,1)S(1)} %get-tuple-element.76.normed, bf16[2048,128]{1,0:T(8,128)(2,1)S(1)} %get-tuple-element.77.wv, ...), custom_call_target="tpu_custom_call" | custom-call | flops 1048576 | bytes 67108864 | tf_op jit(solution)/shard_map/pallas_call | solution.py:376
  49.5 0.0 collective-permute-done.17.refs_1_
  49.5 3.0 %shard_map.202 = (bf16[80,128]{1,0:T(8,128)(2,1)S(1)}, f32[80,128]{1,0:T(8,128)S(1)}, f32[80,256]{1,0:T(8,128)S(1)}, f32[40,128,256]{2,1,0:T(8,128)S(1)}) custom-call(f32[2,80,128,256]{3,2,1,0:T(8,128)} %memory.7, f32[40,128,256]{2,1,0:T(8,128)S(1)} %shard_map.192.kept, bf16[2,80,128]{2,1,0:T(8,128)(2,1)S(1)} %get-tuple-element.75.refs_0_, ...), custom_call_target="tpu_custom_call" | custom-call | flops 1048576 | bytes 67108864 | tf_op jit(solution)/shard_map/pallas_call | solution.py:390
  52.6 2.7 %collective-permute-start.18 = (bf16[1,80,128]{2,1,0:T(8,128)(2,1)S(1)}, bf16[1,80,128]{2,1,0:T(8,128)(2,1)S(1)}, u32[]{:S(2)}, u32[]{:S(2)}) collective-permute-start(bf16[1,80,128]{2,1,0:T(8,128)(2,1)S(1)} %bitcast.17), channel_id=1, source_target_pairs={{0,9},{1,8},{2,11},{3,10},{4,13},{5,12},{6,15},{7,14},{8,1},{9,0},... | collective-permute-start | bytes 61448 | tf_op jit(solution)/shard_map/ppermute | solution.py:44
  55.3 1.5 %collective-permute-done.18 = bf16[1,80,128]{2,1,0:T(8,128)(2,1)S(1)} collective-permute-done((bf16[1,80,128]{2,1,0:T(8,128)(2,1)S(1)}, bf16[1,80,128]{2,1,0:T(8,128)(2,1)S(1)}, u32[]{:S(2)}, u32[]{:S(2)}) %collective-permute-start.18) | collective-permute-done | bytes 20512 | tf_op jit(solution)/shard_map/ppermute | solution.py:44
  56.8 1.1 %collective-permute-start.19 = (bf16[2,80,128]{2,1,0:T(8,128)(2,1)S(1)}, bf16[2,80,128]{2,1,0:T(8,128)(2,1)S(1)}, u32[]{:S(2)}, u32[]{:S(2)}) collective-permute-start(bf16[2,80,128]{2,1,0:T(8,128)(2,1)S(1)} %pad_maximum_fusion.3), channel_id=1, source_target_pairs={{0,7},{1,6},{2,5},{3,4},{4,3},{5,2},{6,1},{7,0},{8,15},{9,14},{10,... | collective-permute-start | bytes 122888 | tf_op jit(solution)/shard_map/ppermute | solution.py:44
  57.9 1.2 %collective-permute-start.20 = (bf16[2,80,128]{2,1,0:T(8,128)(2,1)S(1)}, bf16[2,80,128]{2,1,0:T(8,128)(2,1)S(1)}, u32[]{:S(2)}, u32[]{:S(2)}) collective-permute-start(bf16[2,80,128]{2,1,0:T(8,128)(2,1)S(1)} %pad_maximum_fusion.3), channel_id=1, source_target_pairs={{0,3},{1,2},{2,1},{3,0},{4,7},{5,6},{6,5},{7,4},{8,11},{9,10},{10,... | collective-permute-start | bytes 122888 | tf_op jit(solution)/shard_map/ppermute | solution.py:44
  59.1 1.2 %collective-permute-start.21 = (bf16[2,80,128]{2,1,0:T(8,128)(2,1)S(1)}, bf16[2,80,128]{2,1,0:T(8,128)(2,1)S(1)}, u32[]{:S(2)}, u32[]{:S(2)}) collective-permute-start(bf16[2,80,128]{2,1,0:T(8,128)(2,1)S(1)} %pad_maximum_fusion.3), channel_id=1, source_target_pairs={{0,5},{1,4},{2,7},{3,6},{4,1},{5,0},{6,3},{7,2},{8,13},{9,12},{10,... | collective-permute-start | bytes 122888 | tf_op jit(solution)/shard_map/ppermute | solution.py:44
  60.2 0.9 %collective-permute-done.19 = bf16[2,80,128]{2,1,0:T(8,128)(2,1)S(1)} collective-permute-done((bf16[2,80,128]{2,1,0:T(8,128)(2,1)S(1)}, bf16[2,80,128]{2,1,0:T(8,128)(2,1)S(1)}, u32[]{:S(2)}, u32[]{:S(2)}) %collective-permute-start.19) | collective-permute-done | bytes 40992 | tf_op jit(solution)/shard_map/ppermute | solution.py:44
  61.2 1.3 %collective-permute-done.20 = bf16[2,80,128]{2,1,0:T(8,128)(2,1)S(1)} collective-permute-done((bf16[2,80,128]{2,1,0:T(8,128)(2,1)S(1)}, bf16[2,80,128]{2,1,0:T(8,128)(2,1)S(1)}, u32[]{:S(2)}, u32[]{:S(2)}) %collective-permute-start.20) | collective-permute-done | bytes 40992 | tf_op jit(solution)/shard_map/ppermute | solution.py:44
  62.4 0.2 collective-permute-done.21
  62.7 0.2 collective-permute-start.22
  62.9 2.6 %shard_map.204._old = f32[2,80,128,256]{3,2,1,0:T(8,128)} custom-call(f32[48,128,256]{2,1,0:T(8,128)S(1)} %shard_map.193.kept, f32[32,128,256]{2,1,0:T(8,128)S(1)} %get-tuple-element.88.rest, f32[128,128]{1,0:T(8,128)S(1)} %get-tuple-element.89.columns, f32[80,256]{1,0:T(8,128)S(1)} %get-tuple-element.90.decays, f32[80,256]{1,0:T(8,128)S(1)} %get-tuple-element.91.keys, ...), custom_call_target="tpu_custom_call" | custom-call | flops 1048576 | bytes 67108864 | tf_op jit(solution)/shard_map/pallas_call | solution.py:410
  65.5 2.7 %shard_map.205._old = f32[2,80,128,256]{3,2,1,0:T(8,128)} custom-call(f32[48,128,256]{2,1,0:T(8,128)S(1)} %shard_map.193.kept, f32[32,128,256]{2,1,0:T(8,128)S(1)} %get-tuple-element.88.rest, f32[128,128]{1,0:T(8,128)S(1)} %get-tuple-element.89.columns, f32[80,256]{1,0:T(8,128)S(1)} %get-tuple-element.90.decays, ...), custom_call_target="tpu_custom_call", output_to_operand_aliasing={{}: (5, {})} | custom-call | flops 1048576 | bytes 67108864 | tf_op jit(solution)/shard_map/pallas_call | solution.py:410
  68.2 2.7 %shard_map.206._old = f32[2,80,128,256]{3,2,1,0:T(8,128)} custom-call(f32[40,128,256]{2,1,0:T(8,128)S(1)} %shard_map.192.kept, f32[40,128,256]{2,1,0:T(8,128)S(1)} %get-tuple-element.84.rest, f32[128,128]{1,0:T(8,128)S(1)} %get-tuple-element.85.columns, f32[80,256]{1,0:T(8,128)S(1)} %get-tuple-element.86.decays, ...), custom_call_target="tpu_custom_call", output_to_operand_aliasing={{}: (5, {})} | custom-call | flops 1048576 | bytes 67108864 | tf_op jit(solution)/shard_map/pallas_call | solution.py:410
  70.9 2.7 %shard_map.207 = f32[2,80,128,256]{3,2,1,0:T(8,128)} custom-call(f32[40,128,256]{2,1,0:T(8,128)S(1)} %shard_map.192.kept, f32[40,128,256]{2,1,0:T(8,128)S(1)} %get-tuple-element.84.rest, f32[128,128]{1,0:T(8,128)S(1)} %get-tuple-element.85.columns, f32[80,256]{1,0:T(8,128)S(1)} %get-tuple-element.86.decays, ...), custom_call_target="tpu_custom_call", output_to_operand_aliasing={{}: (5, {})} | custom-call | flops 1048576 | bytes 67108864 | tf_op jit(solution)/shard_map/pallas_call | solution.py:410
  73.5 0.7 shard_map.208
  74.2 0.0 collective-permute-done.22.far
  74.2 0.9 %shard_map.203 = bf16[80,128]{1,0:T(8,128)(2,1)} custom-call(bf16[8,80,128]{2,1,0:T(8,128)(2,1)S(1)} %constant_dynamic-update-slice_fusion.15.near, bf16[8,80,128]{2,1,0:T(8,128)(2,1)S(1)} %collective-permute-done.22.far, bf16[80,128]{1,0:T(8,128)(2,1)S(1)} %shard_map.198.current, bf16[2048,128]{1,0:T(8,128)(2,1)S(1)} %get-tuple-element.83.wo), custom_call_target="tpu_custom_call" | custom-call | flops 1048576 | bytes 67108864 | tf_op jit(solution)/shard_map/pallas_call | solution.py:420
  (25 shorter events, 0.2 us)
Async XLA Ops:
  0.6 5.6 %collective-permute-start = (bf16[1,80,128]{2,1,0:T(8,128)(2,1)}, bf16[1,80,128]{2,1,0:T(8,128)(2,1)S(1)}, u32[]{:S(2)}, u32[]{:S(2)}) collective-permute-start(bf16[1,80,128]{2,1,0:T(8,128)(2,1)} %bitcast.23), channel_id=1, source_target_pairs={{0,9},{1,8},{2,11},{3,10},{4,13},{5,12},{6,15},{7,14},{8,1},{9,0},... | collective-permute-start | bytes 61448 | tf_op jit(solution)/shard_map/ppermute | solution.py:44
  6.2 42.5 %copy-start = (s32[1,80]{1,0:T(1,128)}, s32[1,80]{1,0:T(1,128)S(1)}, u32[]{:S(2)}) copy-start(s32[1,80]{1,0:T(1,128)S(1)} %get-tuple-element.65.lengths._old) | copy-start | bytes 964
  6.3 4.8 %collective-permute-start.1 = (bf16[2,80,128]{2,1,0:T(8,128)(2,1)S(1)}, bf16[2,80,128]{2,1,0:T(8,128)(2,1)S(1)}, u32[]{:S(2)}, u32[]{:S(2)}) collective-permute-start(bf16[2,80,128]{2,1,0:T(8,128)(2,1)S(1)} %pad_maximum_fusion), channel_id=1, source_target_pairs={{0,7},{1,6},{2,5},{3,4},{4,3},{5,2},{6,1},{7,0},{8,15},{9,14},{10,... | collective-permute-start | bytes 122888 | tf_op jit(solution)/shard_map/ppermute | solution.py:44
  9.2 3.7 %collective-permute-start.2 = (bf16[2,80,128]{2,1,0:T(8,128)(2,1)S(1)}, bf16[2,80,128]{2,1,0:T(8,128)(2,1)S(1)}, u32[]{:S(2)}, u32[]{:S(2)}) collective-permute-start(bf16[2,80,128]{2,1,0:T(8,128)(2,1)S(1)} %pad_maximum_fusion), channel_id=1, source_target_pairs={{0,3},{1,2},{2,1},{3,0},{4,7},{5,6},{6,5},{7,4},{8,11},{9,10},{10,... | collective-permute-start | bytes 122888 | tf_op jit(solution)/shard_map/ppermute | solution.py:44
  9.3 3.6 %collective-permute-start.3 = (bf16[2,80,128]{2,1,0:T(8,128)(2,1)S(1)}, bf16[2,80,128]{2,1,0:T(8,128)(2,1)S(1)}, u32[]{:S(2)}, u32[]{:S(2)}) collective-permute-start(bf16[2,80,128]{2,1,0:T(8,128)(2,1)S(1)} %pad_maximum_fusion), channel_id=1, source_target_pairs={{0,5},{1,4},{2,7},{3,6},{4,1},{5,0},{6,3},{7,2},{8,13},{9,12},{10,... | collective-permute-start | bytes 122888 | tf_op jit(solution)/shard_map/ppermute | solution.py:44
  12.9 1.5 %collective-permute-start.4 = (bf16[8,80,128]{2,1,0:T(8,128)(2,1)S(1)}, bf16[8,80,128]{2,1,0:T(8,128)(2,1)S(1)}, u32[]{:S(2)}, u32[]{:S(2)}) collective-permute-start(bf16[8,80,128]{2,1,0:T(8,128)(2,1)S(1)} %constant_dynamic-update-slice_fusion.near), channel_id=1, source_target_pairs={{0,1},{1,0},{2,3},{3,2},{4,5},{5,4},{6,7},{7,6},{8,9},{9,8},{10,11... | collective-permute-start | bytes 491528 | tf_op jit(solution)/shard_map/ppermute | solution.py:44
  13.3 5.5 %collective-permute-start.6 = (f32[2,80,128]{2,1,0:T(8,128)S(1)}, f32[2,80,128]{2,1,0:T(8,128)S(1)}, u32[]{:S(2)}, u32[]{:S(2)}) collective-permute-start(f32[2,80,128]{2,1,0:T(8,128)S(1)} %get-tuple-element.56.refs_2_), channel_id=1, source_target_pairs={{0,1},{1,0},{2,3},{3,2},{4,5},{5,4},{6,7},{7,6},{8,9},{9,8},{10,11... | collective-permute-start | bytes 245768 | tf_op jit(solution)/shard_map/ppermute | solution.py:44
  14.8 4.0 %collective-permute-start.5 = (bf16[2,80,128]{2,1,0:T(8,128)(2,1)S(1)}, bf16[2,80,128]{2,1,0:T(8,128)(2,1)S(1)}, u32[]{:S(2)}, u32[]{:S(2)}) collective-permute-start(bf16[2,80,128]{2,1,0:T(8,128)(2,1)S(1)} %get-tuple-element.55.refs_0_), channel_id=1, source_target_pairs={{0,1},{1,0},{2,3},{3,2},{4,5},{5,4},{6,7},{7,6},{8,9},{9,8},{10,11... | collective-permute-start | bytes 122888 | tf_op jit(solution)/shard_map/ppermute | solution.py:44
  21.5 4.7 %collective-permute-start.7 = (bf16[1,80,128]{2,1,0:T(8,128)(2,1)S(1)}, bf16[1,80,128]{2,1,0:T(8,128)(2,1)S(1)}, u32[]{:S(2)}, u32[]{:S(2)}) collective-permute-start(bf16[1,80,128]{2,1,0:T(8,128)(2,1)S(1)} %bitcast.19), channel_id=1, source_target_pairs={{0,9},{1,8},{2,11},{3,10},{4,13},{5,12},{6,15},{7,14},{8,1},{9,0},... | collective-permute-start | bytes 61448 | tf_op jit(solution)/shard_map/ppermute | solution.py:44
  26.2 4.5 %collective-permute-start.8 = (bf16[2,80,128]{2,1,0:T(8,128)(2,1)S(1)}, bf16[2,80,128]{2,1,0:T(8,128)(2,1)S(1)}, u32[]{:S(2)}, u32[]{:S(2)}) collective-permute-start(bf16[2,80,128]{2,1,0:T(8,128)(2,1)S(1)} %pad_maximum_fusion.1), channel_id=1, source_target_pairs={{0,7},{1,6},{2,5},{3,4},{4,3},{5,2},{6,1},{7,0},{8,15},{9,14},{10,... | collective-permute-start | bytes 122888 | tf_op jit(solution)/shard_map/ppermute | solution.py:44
  26.9 4.4 %collective-permute-start.9 = (bf16[2,80,128]{2,1,0:T(8,128)(2,1)S(1)}, bf16[2,80,128]{2,1,0:T(8,128)(2,1)S(1)}, u32[]{:S(2)}, u32[]{:S(2)}) collective-permute-start(bf16[2,80,128]{2,1,0:T(8,128)(2,1)S(1)} %pad_maximum_fusion.1), channel_id=1, source_target_pairs={{0,3},{1,2},{2,1},{3,0},{4,7},{5,6},{6,5},{7,4},{8,11},{9,10},{10,... | collective-permute-start | bytes 122888 | tf_op jit(solution)/shard_map/ppermute | solution.py:44
  27.9 3.9 %collective-permute-start.10 = (bf16[2,80,128]{2,1,0:T(8,128)(2,1)S(1)}, bf16[2,80,128]{2,1,0:T(8,128)(2,1)S(1)}, u32[]{:S(2)}, u32[]{:S(2)}) collective-permute-start(bf16[2,80,128]{2,1,0:T(8,128)(2,1)S(1)} %pad_maximum_fusion.1), channel_id=1, source_target_pairs={{0,5},{1,4},{2,7},{3,6},{4,1},{5,0},{6,3},{7,2},{8,13},{9,12},{10,... | collective-permute-start | bytes 122888 | tf_op jit(solution)/shard_map/ppermute | solution.py:44
  31.7 1.5 %collective-permute-start.11 = (bf16[8,80,128]{2,1,0:T(8,128)(2,1)S(1)}, bf16[8,80,128]{2,1,0:T(8,128)(2,1)S(1)}, u32[]{:S(2)}, u32[]{:S(2)}) collective-permute-start(bf16[8,80,128]{2,1,0:T(8,128)(2,1)S(1)} %constant_dynamic-update-slice_fusion.5.near), channel_id=1, source_target_pairs={{0,1},{1,0},{2,3},{3,2},{4,5},{5,4},{6,7},{7,6},{8,9},{9,8},{10,11... | collective-permute-start | bytes 491528 | tf_op jit(solution)/shard_map/ppermute | solution.py:44
  33.5 4.2 %collective-permute-start.12 = (bf16[1,80,128]{2,1,0:T(8,128)(2,1)S(1)}, bf16[1,80,128]{2,1,0:T(8,128)(2,1)S(1)}, u32[]{:S(2)}, u32[]{:S(2)}) collective-permute-start(bf16[1,80,128]{2,1,0:T(8,128)(2,1)S(1)} %bitcast.14), channel_id=1, source_target_pairs={{0,9},{1,8},{2,11},{3,10},{4,13},{5,12},{6,15},{7,14},{8,1},{9,0},... | collective-permute-start | bytes 61448 | tf_op jit(solution)/shard_map/ppermute | solution.py:44
  37.6 4.4 %collective-permute-start.13 = (bf16[2,80,128]{2,1,0:T(8,128)(2,1)S(1)}, bf16[2,80,128]{2,1,0:T(8,128)(2,1)S(1)}, u32[]{:S(2)}, u32[]{:S(2)}) collective-permute-start(bf16[2,80,128]{2,1,0:T(8,128)(2,1)S(1)} %pad_maximum_fusion.2), channel_id=1, source_target_pairs={{0,7},{1,6},{2,5},{3,4},{4,3},{5,2},{6,1},{7,0},{8,15},{9,14},{10,... | collective-permute-start | bytes 122888 | tf_op jit(solution)/shard_map/ppermute | solution.py:44
  39.6 3.4 %collective-permute-start.14 = (bf16[2,80,128]{2,1,0:T(8,128)(2,1)S(1)}, bf16[2,80,128]{2,1,0:T(8,128)(2,1)S(1)}, u32[]{:S(2)}, u32[]{:S(2)}) collective-permute-start(bf16[2,80,128]{2,1,0:T(8,128)(2,1)S(1)} %pad_maximum_fusion.2), channel_id=1, source_target_pairs={{0,3},{1,2},{2,1},{3,0},{4,7},{5,6},{6,5},{7,4},{8,11},{9,10},{10,... | collective-permute-start | bytes 122888 | tf_op jit(solution)/shard_map/ppermute | solution.py:44
  40.0 3.4 %collective-permute-start.15 = (bf16[2,80,128]{2,1,0:T(8,128)(2,1)S(1)}, bf16[2,80,128]{2,1,0:T(8,128)(2,1)S(1)}, u32[]{:S(2)}, u32[]{:S(2)}) collective-permute-start(bf16[2,80,128]{2,1,0:T(8,128)(2,1)S(1)} %pad_maximum_fusion.2), channel_id=1, source_target_pairs={{0,5},{1,4},{2,7},{3,6},{4,1},{5,0},{6,3},{7,2},{8,13},{9,12},{10,... | collective-permute-start | bytes 122888 | tf_op jit(solution)/shard_map/ppermute | solution.py:44
  43.4 2.0 %collective-permute-start.16 = (bf16[8,80,128]{2,1,0:T(8,128)(2,1)S(1)}, bf16[8,80,128]{2,1,0:T(8,128)(2,1)S(1)}, u32[]{:S(2)}, u32[]{:S(2)}) collective-permute-start(bf16[8,80,128]{2,1,0:T(8,128)(2,1)S(1)} %constant_dynamic-update-slice_fusion.10.near), channel_id=1, source_target_pairs={{0,1},{1,0},{2,3},{3,2},{4,5},{5,4},{6,7},{7,6},{8,9},{9,8},{10,11... | collective-permute-start | bytes 491528 | tf_op jit(solution)/shard_map/ppermute | solution.py:44
  45.9 3.6 %collective-permute-start.17 = (bf16[2,80,128]{2,1,0:T(8,128)(2,1)S(1)}, bf16[2,80,128]{2,1,0:T(8,128)(2,1)S(1)}, u32[]{:S(2)}, u32[]{:S(2)}) collective-permute-start(bf16[2,80,128]{2,1,0:T(8,128)(2,1)S(1)} %get-tuple-element.75.refs_0_), channel_id=1, source_target_pairs={{0,1},{1,0},{2,3},{3,2},{4,5},{5,4},{6,7},{7,6},{8,9},{9,8},{10,11... | collective-permute-start | bytes 122888 | tf_op jit(solution)/shard_map/ppermute | solution.py:44
  52.6 4.2 %collective-permute-start.18 = (bf16[1,80,128]{2,1,0:T(8,128)(2,1)S(1)}, bf16[1,80,128]{2,1,0:T(8,128)(2,1)S(1)}, u32[]{:S(2)}, u32[]{:S(2)}) collective-permute-start(bf16[1,80,128]{2,1,0:T(8,128)(2,1)S(1)} %bitcast.17), channel_id=1, source_target_pairs={{0,9},{1,8},{2,11},{3,10},{4,13},{5,12},{6,15},{7,14},{8,1},{9,0},... | collective-permute-start | bytes 61448 | tf_op jit(solution)/shard_map/ppermute | solution.py:44
  56.8 4.3 %collective-permute-start.19 = (bf16[2,80,128]{2,1,0:T(8,128)(2,1)S(1)}, bf16[2,80,128]{2,1,0:T(8,128)(2,1)S(1)}, u32[]{:S(2)}, u32[]{:S(2)}) collective-permute-start(bf16[2,80,128]{2,1,0:T(8,128)(2,1)S(1)} %pad_maximum_fusion.3), channel_id=1, source_target_pairs={{0,7},{1,6},{2,5},{3,4},{4,3},{5,2},{6,1},{7,0},{8,15},{9,14},{10,... | collective-permute-start | bytes 122888 | tf_op jit(solution)/shard_map/ppermute | solution.py:44
  57.9 4.5 %collective-permute-start.20 = (bf16[2,80,128]{2,1,0:T(8,128)(2,1)S(1)}, bf16[2,80,128]{2,1,0:T(8,128)(2,1)S(1)}, u32[]{:S(2)}, u32[]{:S(2)}) collective-permute-start(bf16[2,80,128]{2,1,0:T(8,128)(2,1)S(1)} %pad_maximum_fusion.3), channel_id=1, source_target_pairs={{0,3},{1,2},{2,1},{3,0},{4,7},{5,6},{6,5},{7,4},{8,11},{9,10},{10,... | collective-permute-start | bytes 122888 | tf_op jit(solution)/shard_map/ppermute | solution.py:44
  59.1 3.6 %collective-permute-start.21 = (bf16[2,80,128]{2,1,0:T(8,128)(2,1)S(1)}, bf16[2,80,128]{2,1,0:T(8,128)(2,1)S(1)}, u32[]{:S(2)}, u32[]{:S(2)}) collective-permute-start(bf16[2,80,128]{2,1,0:T(8,128)(2,1)S(1)} %pad_maximum_fusion.3), channel_id=1, source_target_pairs={{0,5},{1,4},{2,7},{3,6},{4,1},{5,0},{6,3},{7,2},{8,13},{9,12},{10,... | collective-permute-start | bytes 122888 | tf_op jit(solution)/shard_map/ppermute | solution.py:44
  62.7 11.5 %collective-permute-start.22 = (bf16[8,80,128]{2,1,0:T(8,128)(2,1)S(1)}, bf16[8,80,128]{2,1,0:T(8,128)(2,1)S(1)}, u32[]{:S(2)}, u32[]{:S(2)}) collective-permute-start(bf16[8,80,128]{2,1,0:T(8,128)(2,1)S(1)} %constant_dynamic-update-slice_fusion.15.near), channel_id=1, source_target_pairs={{0,1},{1,0},{2,3},{3,2},{4,5},{5,4},{6,7},{7,6},{8,9},{9,8},{10,11... | collective-permute-start | bytes 491528 | tf_op jit(solution)/shard_map/ppermute | solution.py:44

commit v4 on v3

--- a/solution.py
+++ b/solution.py
@@ -201,9 +201,9 @@
     sums_new[...] = decay * sums[0][layer] + weight * pairs[0][1].astype(F32)
 
 
-def out_kernel(masks, low, near, far, current, wo, after, rows):
+def out_kernel(layer, masks, low, near, far, current, wo, after, rows):
     place(near, far, rows, masks, low)
-    total = current[...].astype(F32) + dot(joined(rows), wo[...])
+    total = current[...].astype(F32) + dot(joined(rows), wo[layer])
     after[...] = total.astype(BF16)
 
 
@@ -330,7 +330,7 @@
     rows = 8 if batch % 8 == 0 else 1
     lanes = -(-batch // LANES) * LANES
     sizes = (batch // rows // 2 * rows, batch - batch // rows // 2 * rows)
-    weights = [query_weight, key_weight, value_weight, outgate_weight, output_weight]
+    weights = [query_weight, key_weight, value_weight, outgate_weight]
     own_sums, wi, wf, ibias, fbias, slope, at, stab, norm_gain, head_gain, current, *loaded = load(
         0,
         [
@@ -350,13 +350,19 @@
     )
     near, far, masks, low = gather(tokens, current)
     sums = pieces(own_sums)
+    loaded = [loaded]
+    for layer in range(1, blocks):
+        *outs, wq, wk, wv, wg = load(layer, [output_weight] if layer == 1 else [], weights)
+        wo = outs[0] if outs else wo
+        loaded.append([wq, wk, wv, wg])
+    if blocks == 1:
+        (wo,) = load(1, [output_weight], [])
     memory = in_hbm(cell_memory)
     new_memory, sums_out, stabs = at, [], []
     for layer in range(blocks):
         if layer:
             near, far, masks, low = gather(current, current)
-            loaded = load(layer, [], weights)
-        wq, wk, wv, wg, wo = loaded
+        wq, wk, wv, wg = loaded[layer]
         first = batch // rows * EARLY[layer > 0] // 10 * rows
         kept = call(
             functools.partial(state_kernel, layer, rows),
@@ -418,7 +424,7 @@
             )(kept, rest, columns, decays, keys, in_hbm(new_memory))
 
         current = call(
-            functools.partial(out_kernel, masks, low),
+            functools.partial(out_kernel, layer, masks, low),
             shape((batch, width), BF16),
             [VM] * 4,
             VM,

time: 75.3 us -> 75.1 us (level)
  transfers between devices with their start and end apart: 23 -> 23, of which waited for: 16 -> 15; matrix products, arithmetic and copies ran while one was open for 0% -> 0% of each run, Pallas kernels for 30% -> 30%
where the time goes in v4:
time: 75.1 us; the launch traced here: 74.9 us
  Pallas kernels  29.6 us (39%)
  starting transfers between devices  26.5 us (35%)
  waiting for transfers between devices  17.7 us (24%)
  between operations  0.83 us (1%)
    ppermute x23, starting transfers between devices, swap(): lax.ppermute(value, 'tp', [(s, s ^ mask) for s in range(lax.axis_size('tp...  26.5 us
    ppermute x23, waiting for transfers between devices, swap(): lax.ppermute(value, 'tp', [(s, s ^ mask) for s in range(lax.axis_size('tp...  17.7 us
    pallas_call x4, Pallas kernels, body(): call(functools.partial(update_kernel, layer, part * sizes[0], size, rows)...  10.6 us
    pallas_call x2, Pallas kernels, body(): call(functools.partial(read_kernel, layer, split, rows), (shape((batch, w...  5.71 us
    pallas_call x2, Pallas kernels, body(): call(functools.partial(state_kernel, layer, rows), pltpu.VMEM((first, wid...  5.38 us
    pallas_call x2, Pallas kernels, load(): call(functools.partial(load_kernel, layer, len(whole), len(sliced)), tupl...  3.73 us
    pallas_call x2, Pallas kernels, body(): call(functools.partial(gates_kernel, layer, split), (shape((batch, width)...  1.51 us
  transfers between devices with their start and end apart: 23, of which 15 were waited for; matrix products, arithmetic and copies ran while one was open for 0% of the time, Pallas kernels for 30%

profile of v4, /device:TPU:0, one launch (start us, length us, event | category | flops | bytes accessed | tf_op | source)
XLA Modules:
  0.0 74.9 jit_solution(10536995418204233156)
XLA Ops:
  0.6 3.6 %collective-permute-start = (bf16[1,80,128]{2,1,0:T(8,128)(2,1)}, bf16[1,80,128]{2,1,0:T(8,128)(2,1)S(1)}, u32[]{:S(2)}, u32[]{:S(2)}) collective-permute-start(bf16[1,80,128]{2,1,0:T(8,128)(2,1)} %bitcast.23), channel_id=1, source_target_pairs={{0,9},{1,8},{2,11},{3,10},{4,13},{5,12},{6,15},{7,14},{8,1},{9,0},... | collective-permute-start | bytes 61448 | tf_op jit(solution)/shard_map/ppermute | solution.py:44
  4.2 1.9 %shard_map.194 = (f32[2,80,128]{2,1,0:T(8,128)S(1)}, bf16[2,8,2048]{2,1,0:T(8,128)(2,1)S(1)}, bf16[2,8,2048]{2,1,0:T(8,128)(2,1)S(1)}, f32[2,8]{1,0:T(2,128)S(1)...) custom-call(f32[2,80,128]{2,1,0:T(8,128)} %refs_0_.2, ...), custom_call_target="tpu_custom_call" | custom-call | flops 1048576 | bytes 67108864 | tf_op jit(solution)/shard_map/pallas_call | solution.py:279
  6.1 0.0 copy-start
  6.1 0.0 collective-permute-done
  6.1 2.9 %collective-permute-start.1 = (bf16[2,80,128]{2,1,0:T(8,128)(2,1)S(1)}, bf16[2,80,128]{2,1,0:T(8,128)(2,1)S(1)}, u32[]{:S(2)}, u32[]{:S(2)}) collective-permute-start(bf16[2,80,128]{2,1,0:T(8,128)(2,1)S(1)} %pad_maximum_fusion), channel_id=1, source_target_pairs={{0,7},{1,6},{2,5},{3,4},{4,3},{5,2},{6,1},{7,0},{8,15},{9,14},{10,... | collective-permute-start | bytes 122888 | tf_op jit(solution)/shard_map/ppermute | solution.py:44
  9.0 0.3 collective-permute-start.2
  9.3 0.4 collective-permute-start.3
  9.7 1.2 %collective-permute-done.1 = bf16[2,80,128]{2,1,0:T(8,128)(2,1)S(1)} collective-permute-done((bf16[2,80,128]{2,1,0:T(8,128)(2,1)S(1)}, bf16[2,80,128]{2,1,0:T(8,128)(2,1)S(1)}, u32[]{:S(2)}, u32[]{:S(2)}) %collective-permute-start.1) | collective-permute-done | bytes 40992 | tf_op jit(solution)/shard_map/ppermute | solution.py:44
  10.9 1.6 %collective-permute-done.2 = bf16[2,80,128]{2,1,0:T(8,128)(2,1)S(1)} collective-permute-done((bf16[2,80,128]{2,1,0:T(8,128)(2,1)S(1)}, bf16[2,80,128]{2,1,0:T(8,128)(2,1)S(1)}, u32[]{:S(2)}, u32[]{:S(2)}) %collective-permute-start.2) | collective-permute-done | bytes 40992 | tf_op jit(solution)/shard_map/ppermute | solution.py:44
  12.5 0.1 collective-permute-done.3
  12.7 0.4 collective-permute-start.4
  13.1 0.1 collective-permute-start.6
  13.3 0.9 %collective-permute-done.4.far = bf16[8,80,128]{2,1,0:T(8,128)(2,1)S(1)} collective-permute-done((bf16[8,80,128]{2,1,0:T(8,128)(2,1)S(1)}, bf16[8,80,128]{2,1,0:T(8,128)(2,1)S(1)}, u32[]{:S(2)}, u32[]{:S(2)}) %collective-permute-start.4) | collective-permute-done | bytes 163872 | tf_op jit(solution)/shard_map/ppermute | solution.py:44
  14.2 0.5 shard_map.195
  14.6 0.4 collective-permute-start.5
  15.0 2.9 %shard_map.193.kept = f32[48,128,256]{2,1,0:T(8,128)S(1)} custom-call(f32[2,80,128,256]{3,2,1,0:T(8,128)} %memory.7), custom_call_target="tpu_custom_call" | custom-call | flops 1048576 | bytes 67108864 | tf_op jit(solution)/shard_map/pallas_call | solution.py:367
  17.9 0.8 %shard_map.196 = (bf16[80,128]{1,0:T(8,128)(2,1)S(1)}, bf16[80,128]{1,0:T(8,128)(2,1)S(1)}, f32[80,8]{1,0:T(8,128)S(1)}, f32[8,80]{1,0:T(8,128)S(1)}, f32[128,128]{1,0:T(8,128)S(1)}, /*index=5*/f32[80,256]{1,0:T(8,128)S(1)}) custom-call(bf16[80,2048]{1,0:T(8,128)(2,1)S(1)} %get-tuple-element.56.normed, bf16[2048,128]{1,0:T(8,128)(2,1)S(1)} %get-tuple-element.57.wv, ...), custom_call_target="tpu_custom_call" | custom-call | flops 1048576 | bytes 67108864 | tf_op jit(solution)/shard_map/pallas_call | solution.py:382
  18.7 0.0 collective-permute-done.6.refs_3_
  18.7 0.0 collective-permute-done.5.refs_1_
  18.7 2.7 %shard_map.197 = (bf16[80,128]{1,0:T(8,128)(2,1)S(1)}, f32[80,128]{1,0:T(8,128)S(1)}, f32[80,256]{1,0:T(8,128)S(1)}, f32[32,128,256]{2,1,0:T(8,128)S(1)}) custom-call(f32[2,80,128,256]{3,2,1,0:T(8,128)} %memory.7, f32[48,128,256]{2,1,0:T(8,128)S(1)} %shard_map.193.kept, bf16[2,80,128]{2,1,0:T(8,128)(2,1)S(1)} %get-tuple-element.54.refs_0_, ...), custom_call_target="tpu_custom_call" | custom-call | flops 1048576 | bytes 67108864 | tf_op jit(solution)/shard_map/pallas_call | solution.py:396
  21.4 3.1 %collective-permute-start.7 = (bf16[1,80,128]{2,1,0:T(8,128)(2,1)S(1)}, bf16[1,80,128]{2,1,0:T(8,128)(2,1)S(1)}, u32[]{:S(2)}, u32[]{:S(2)}) collective-permute-start(bf16[1,80,128]{2,1,0:T(8,128)(2,1)S(1)} %bitcast.19), channel_id=1, source_target_pairs={{0,9},{1,8},{2,11},{3,10},{4,13},{5,12},{6,15},{7,14},{8,1},{9,0},... | collective-permute-start | bytes 61448 | tf_op jit(solution)/shard_map/ppermute | solution.py:44
  24.5 1.9 %collective-permute-done.7 = bf16[1,80,128]{2,1,0:T(8,128)(2,1)S(1)} collective-permute-done((bf16[1,80,128]{2,1,0:T(8,128)(2,1)S(1)}, bf16[1,80,128]{2,1,0:T(8,128)(2,1)S(1)}, u32[]{:S(2)}, u32[]{:S(2)}) %collective-permute-start.7) | collective-permute-done | bytes 20512 | tf_op jit(solution)/shard_map/ppermute | solution.py:44
  26.4 0.3 collective-permute-start.8
  26.8 1.1 %collective-permute-start.9 = (bf16[2,80,128]{2,1,0:T(8,128)(2,1)S(1)}, bf16[2,80,128]{2,1,0:T(8,128)(2,1)S(1)}, u32[]{:S(2)}, u32[]{:S(2)}) collective-permute-start(bf16[2,80,128]{2,1,0:T(8,128)(2,1)S(1)} %pad_maximum_fusion.1), channel_id=1, source_target_pairs={{0,3},{1,2},{2,1},{3,0},{4,7},{5,6},{6,5},{7,4},{8,11},{9,10},{10,... | collective-permute-start | bytes 122888 | tf_op jit(solution)/shard_map/ppermute | solution.py:44
  27.9 1.5 %collective-permute-start.10 = (bf16[2,80,128]{2,1,0:T(8,128)(2,1)S(1)}, bf16[2,80,128]{2,1,0:T(8,128)(2,1)S(1)}, u32[]{:S(2)}, u32[]{:S(2)}) collective-permute-start(bf16[2,80,128]{2,1,0:T(8,128)(2,1)S(1)} %pad_maximum_fusion.1), channel_id=1, source_target_pairs={{0,5},{1,4},{2,7},{3,6},{4,1},{5,0},{6,3},{7,2},{8,13},{9,12},{10,... | collective-permute-start | bytes 122888 | tf_op jit(solution)/shard_map/ppermute | solution.py:44
  29.3 1.6 %collective-permute-done.8 = bf16[2,80,128]{2,1,0:T(8,128)(2,1)S(1)} collective-permute-done((bf16[2,80,128]{2,1,0:T(8,128)(2,1)S(1)}, bf16[2,80,128]{2,1,0:T(8,128)(2,1)S(1)}, u32[]{:S(2)}, u32[]{:S(2)}) %collective-permute-start.8) | collective-permute-done | bytes 40992 | tf_op jit(solution)/shard_map/ppermute | solution.py:44
  31.0 0.0 collective-permute-done.9
  31.0 0.4 collective-permute-done.10
  31.4 0.2 collective-permute-start.11
  31.6 1.9 %shard_map.198 = (bf16[2,2048,128]{2,1,0:T(8,128)(2,1)S(1)}, bf16[2048,128]{1,0:T(8,128)(2,1)S(1)}, bf16[2048,128]{1,0:T(8,128)(2,1)S(1)}, bf16[2048,128]{1,0:T(8,128)(2,1)S(1)}, bf16[2048,128]{1,0:T(8,128)(2,1)S(1)}) custom-call(bf16[2,2048,128]{2,1,0:T(8,128)(2,1)} %refs_0_.3, bf16[2,2048,128]{2,1,0:T(8,128)(2,1)} %refs_1_.1, ...), custom_call_target="tpu_custom_call" | custom-call | flops 1048576 | bytes 67108864 | tf_op jit(solution)/shard_map/pallas_call | solution.py:279
  33.5 0.0 collective-permute-done.11.far
  33.5 0.3 shard_map.199.current
  33.8 2.8 %collective-permute-start.12 = (bf16[1,80,128]{2,1,0:T(8,128)(2,1)S(1)}, bf16[1,80,128]{2,1,0:T(8,128)(2,1)S(1)}, u32[]{:S(2)}, u32[]{:S(2)}) collective-permute-start(bf16[1,80,128]{2,1,0:T(8,128)(2,1)S(1)} %bitcast.14), channel_id=1, source_target_pairs={{0,9},{1,8},{2,11},{3,10},{4,13},{5,12},{6,15},{7,14},{8,1},{9,0},... | collective-permute-start | bytes 61448 | tf_op jit(solution)/shard_map/ppermute | solution.py:44
  36.6 1.5 %collective-permute-done.12 = bf16[1,80,128]{2,1,0:T(8,128)(2,1)S(1)} collective-permute-done((bf16[1,80,128]{2,1,0:T(8,128)(2,1)S(1)}, bf16[1,80,128]{2,1,0:T(8,128)(2,1)S(1)}, u32[]{:S(2)}, u32[]{:S(2)}) %collective-permute-start.12) | collective-permute-done | bytes 20512 | tf_op jit(solution)/shard_map/ppermute | solution.py:44
  38.1 2.2 %collective-permute-start.13 = (bf16[2,80,128]{2,1,0:T(8,128)(2,1)S(1)}, bf16[2,80,128]{2,1,0:T(8,128)(2,1)S(1)}, u32[]{:S(2)}, u32[]{:S(2)}) collective-permute-start(bf16[2,80,128]{2,1,0:T(8,128)(2,1)S(1)} %pad_maximum_fusion.2), channel_id=1, source_target_pairs={{0,7},{1,6},{2,5},{3,4},{4,3},{5,2},{6,1},{7,0},{8,15},{9,14},{10,... | collective-permute-start | bytes 122888 | tf_op jit(solution)/shard_map/ppermute | solution.py:44
  40.3 0.6 collective-permute-start.14
  40.9 0.3 collective-permute-start.15
  41.2 1.3 %collective-permute-done.13 = bf16[2,80,128]{2,1,0:T(8,128)(2,1)S(1)} collective-permute-done((bf16[2,80,128]{2,1,0:T(8,128)(2,1)S(1)}, bf16[2,80,128]{2,1,0:T(8,128)(2,1)S(1)}, u32[]{:S(2)}, u32[]{:S(2)}) %collective-permute-start.13) | collective-permute-done | bytes 40992 | tf_op jit(solution)/shard_map/ppermute | solution.py:44
  42.5 1.4 %collective-permute-done.14 = bf16[2,80,128]{2,1,0:T(8,128)(2,1)S(1)} collective-permute-done((bf16[2,80,128]{2,1,0:T(8,128)(2,1)S(1)}, bf16[2,80,128]{2,1,0:T(8,128)(2,1)S(1)}, u32[]{:S(2)}, u32[]{:S(2)}) %collective-permute-start.14) | collective-permute-done | bytes 40992 | tf_op jit(solution)/shard_map/ppermute | solution.py:44
  43.9 0.5 collective-permute-done.15
  44.3 0.4 collective-permute-start.16
  44.8 1.0 %collective-permute-done.16.far = bf16[8,80,128]{2,1,0:T(8,128)(2,1)S(1)} collective-permute-done((bf16[8,80,128]{2,1,0:T(8,128)(2,1)S(1)}, bf16[8,80,128]{2,1,0:T(8,128)(2,1)S(1)}, u32[]{:S(2)}, u32[]{:S(2)}) %collective-permute-start.16) | collective-permute-done | bytes 163872 | tf_op jit(solution)/shard_map/ppermute | solution.py:44
  45.8 0.4 shard_map.200
  46.3 0.4 collective-permute-start.17
  46.7 2.5 %shard_map.192.kept = f32[40,128,256]{2,1,0:T(8,128)S(1)} custom-call(f32[2,80,128,256]{3,2,1,0:T(8,128)} %memory.7), custom_call_target="tpu_custom_call" | custom-call | flops 1048576 | bytes 67108864 | tf_op jit(solution)/shard_map/pallas_call | solution.py:367
  49.2 0.8 %shard_map.201 = (bf16[80,128]{1,0:T(8,128)(2,1)S(1)}, bf16[80,128]{1,0:T(8,128)(2,1)S(1)}, f32[80,8]{1,0:T(8,128)S(1)}, f32[8,80]{1,0:T(8,128)S(1)}, f32[128,128]{1,0:T(8,128)S(1)}, /*index=5*/f32[80,256]{1,0:T(8,128)S(1)}) custom-call(bf16[80,2048]{1,0:T(8,128)(2,1)S(1)} %get-tuple-element.75.normed, bf16[2048,128]{1,0:T(8,128)(2,1)S(1)} %get-tuple-element.76.wv, ...), custom_call_target="tpu_custom_call" | custom-call | flops 1048576 | bytes 67108864 | tf_op jit(solution)/shard_map/pallas_call | solution.py:382
  50.0 0.0 collective-permute-done.17.refs_1_
  50.0 3.0 %shard_map.202 = (bf16[80,128]{1,0:T(8,128)(2,1)S(1)}, f32[80,128]{1,0:T(8,128)S(1)}, f32[80,256]{1,0:T(8,128)S(1)}, f32[40,128,256]{2,1,0:T(8,128)S(1)}) custom-call(f32[2,80,128,256]{3,2,1,0:T(8,128)} %memory.7, f32[40,128,256]{2,1,0:T(8,128)S(1)} %shard_map.192.kept, bf16[2,80,128]{2,1,0:T(8,128)(2,1)S(1)} %get-tuple-element.74.refs_0_, ...), custom_call_target="tpu_custom_call" | custom-call | flops 1048576 | bytes 67108864 | tf_op jit(solution)/shard_map/pallas_call | solution.py:396
  53.0 2.1 %collective-permute-start.18 = (bf16[1,80,128]{2,1,0:T(8,128)(2,1)S(1)}, bf16[1,80,128]{2,1,0:T(8,128)(2,1)S(1)}, u32[]{:S(2)}, u32[]{:S(2)}) collective-permute-start(bf16[1,80,128]{2,1,0:T(8,128)(2,1)S(1)} %bitcast.17), channel_id=1, source_target_pairs={{0,9},{1,8},{2,11},{3,10},{4,13},{5,12},{6,15},{7,14},{8,1},{9,0},... | collective-permute-start | bytes 61448 | tf_op jit(solution)/shard_map/ppermute | solution.py:44
  55.1 2.5 %collective-permute-done.18 = bf16[1,80,128]{2,1,0:T(8,128)(2,1)S(1)} collective-permute-done((bf16[1,80,128]{2,1,0:T(8,128)(2,1)S(1)}, bf16[1,80,128]{2,1,0:T(8,128)(2,1)S(1)}, u32[]{:S(2)}, u32[]{:S(2)}) %collective-permute-start.18) | collective-permute-done | bytes 20512 | tf_op jit(solution)/shard_map/ppermute | solution.py:44
  57.6 0.4 collective-permute-start.19
  58.0 0.9 %collective-permute-start.20 = (bf16[2,80,128]{2,1,0:T(8,128)(2,1)S(1)}, bf16[2,80,128]{2,1,0:T(8,128)(2,1)S(1)}, u32[]{:S(2)}, u32[]{:S(2)}) collective-permute-start(bf16[2,80,128]{2,1,0:T(8,128)(2,1)S(1)} %pad_maximum_fusion.3), channel_id=1, source_target_pairs={{0,3},{1,2},{2,1},{3,0},{4,7},{5,6},{6,5},{7,4},{8,11},{9,10},{10,... | collective-permute-start | bytes 122888 | tf_op jit(solution)/shard_map/ppermute | solution.py:44
  58.9 1.6 %collective-permute-start.21 = (bf16[2,80,128]{2,1,0:T(8,128)(2,1)S(1)}, bf16[2,80,128]{2,1,0:T(8,128)(2,1)S(1)}, u32[]{:S(2)}, u32[]{:S(2)}) collective-permute-start(bf16[2,80,128]{2,1,0:T(8,128)(2,1)S(1)} %pad_maximum_fusion.3), channel_id=1, source_target_pairs={{0,5},{1,4},{2,7},{3,6},{4,1},{5,0},{6,3},{7,2},{8,13},{9,12},{10,... | collective-permute-start | bytes 122888 | tf_op jit(solution)/shard_map/ppermute | solution.py:44
  60.6 1.6 %collective-permute-done.19 = bf16[2,80,128]{2,1,0:T(8,128)(2,1)S(1)} collective-permute-done((bf16[2,80,128]{2,1,0:T(8,128)(2,1)S(1)}, bf16[2,80,128]{2,1,0:T(8,128)(2,1)S(1)}, u32[]{:S(2)}, u32[]{:S(2)}) %collective-permute-start.19) | collective-permute-done | bytes 40992 | tf_op jit(solution)/shard_map/ppermute | solution.py:44
  62.2 0.0 collective-permute-done.20
  62.2 0.1 collective-permute-done.21
  62.3 0.4 collective-permute-start.22
  62.7 2.6 %shard_map.204._old = f32[2,80,128,256]{3,2,1,0:T(8,128)} custom-call(f32[48,128,256]{2,1,0:T(8,128)S(1)} %shard_map.193.kept, f32[32,128,256]{2,1,0:T(8,128)S(1)} %get-tuple-element.86.rest, f32[128,128]{1,0:T(8,128)S(1)} %get-tuple-element.87.columns, f32[80,256]{1,0:T(8,128)S(1)} %get-tuple-element.88.decays, f32[80,256]{1,0:T(8,128)S(1)} %get-tuple-element.89.keys, ...), custom_call_target="tpu_custom_call" | custom-call | flops 1048576 | bytes 67108864 | tf_op jit(solution)/shard_map/pallas_call | solution.py:416
  65.3 2.7 %shard_map.205._old = f32[2,80,128,256]{3,2,1,0:T(8,128)} custom-call(f32[48,128,256]{2,1,0:T(8,128)S(1)} %shard_map.193.kept, f32[32,128,256]{2,1,0:T(8,128)S(1)} %get-tuple-element.86.rest, f32[128,128]{1,0:T(8,128)S(1)} %get-tuple-element.87.columns, f32[80,256]{1,0:T(8,128)S(1)} %get-tuple-element.88.decays, ...), custom_call_target="tpu_custom_call", output_to_operand_aliasing={{}: (5, {})} | custom-call | flops 1048576 | bytes 67108864 | tf_op jit(solution)/shard_map/pallas_call | solution.py:416
  68.0 2.6 %shard_map.206._old = f32[2,80,128,256]{3,2,1,0:T(8,128)} custom-call(f32[40,128,256]{2,1,0:T(8,128)S(1)} %shard_map.192.kept, f32[40,128,256]{2,1,0:T(8,128)S(1)} %get-tuple-element.82.rest, f32[128,128]{1,0:T(8,128)S(1)} %get-tuple-element.83.columns, f32[80,256]{1,0:T(8,128)S(1)} %get-tuple-element.84.decays, ...), custom_call_target="tpu_custom_call", output_to_operand_aliasing={{}: (5, {})} | custom-call | flops 1048576 | bytes 67108864 | tf_op jit(solution)/shard_map/pallas_call | solution.py:416
  70.7 2.7 %shard_map.207 = f32[2,80,128,256]{3,2,1,0:T(8,128)} custom-call(f32[40,128,256]{2,1,0:T(8,128)S(1)} %shard_map.192.kept, f32[40,128,256]{2,1,0:T(8,128)S(1)} %get-tuple-element.82.rest, f32[128,128]{1,0:T(8,128)S(1)} %get-tuple-element.83.columns, f32[80,256]{1,0:T(8,128)S(1)} %get-tuple-element.84.decays, ...), custom_call_target="tpu_custom_call", output_to_operand_aliasing={{}: (5, {})} | custom-call | flops 1048576 | bytes 67108864 | tf_op jit(solution)/shard_map/pallas_call | solution.py:416
  73.3 0.7 shard_map.208
  74.0 0.0 collective-permute-done.22.far
  74.0 0.9 %shard_map.203 = bf16[80,128]{1,0:T(8,128)(2,1)} custom-call(bf16[8,80,128]{2,1,0:T(8,128)(2,1)S(1)} %constant_dynamic-update-slice_fusion.15.near, bf16[8,80,128]{2,1,0:T(8,128)(2,1)S(1)} %collective-permute-done.22.far, bf16[80,128]{1,0:T(8,128)(2,1)S(1)} %shard_map.199.current, bf16[2,2048,128]{2,1,0:T(8,128)(2,1)S(1)} %get-tuple-element.71.wo), custom_call_target="tpu_custom_call" | custom-call | flops 1048576 | bytes 67108864 | tf_op jit(solution)/shard_map/pallas_call | solution.py:426
  (25 shorter events, 0.2 us)
Async XLA Ops:
  0.6 5.5 %collective-permute-start = (bf16[1,80,128]{2,1,0:T(8,128)(2,1)}, bf16[1,80,128]{2,1,0:T(8,128)(2,1)S(1)}, u32[]{:S(2)}, u32[]{:S(2)}) collective-permute-start(bf16[1,80,128]{2,1,0:T(8,128)(2,1)} %bitcast.23), channel_id=1, source_target_pairs={{0,9},{1,8},{2,11},{3,10},{4,13},{5,12},{6,15},{7,14},{8,1},{9,0},... | collective-permute-start | bytes 61448 | tf_op jit(solution)/shard_map/ppermute | solution.py:44
  6.1 43.2 %copy-start = (s32[1,80]{1,0:T(1,128)}, s32[1,80]{1,0:T(1,128)S(1)}, u32[]{:S(2)}) copy-start(s32[1,80]{1,0:T(1,128)S(1)} %get-tuple-element.64.lengths._old) | copy-start | bytes 964
  6.1 4.8 %collective-permute-start.1 = (bf16[2,80,128]{2,1,0:T(8,128)(2,1)S(1)}, bf16[2,80,128]{2,1,0:T(8,128)(2,1)S(1)}, u32[]{:S(2)}, u32[]{:S(2)}) collective-permute-start(bf16[2,80,128]{2,1,0:T(8,128)(2,1)S(1)} %pad_maximum_fusion), channel_id=1, source_target_pairs={{0,7},{1,6},{2,5},{3,4},{4,3},{5,2},{6,1},{7,0},{8,15},{9,14},{10,... | collective-permute-start | bytes 122888 | tf_op jit(solution)/shard_map/ppermute | solution.py:44
  9.0 3.5 %collective-permute-start.2 = (bf16[2,80,128]{2,1,0:T(8,128)(2,1)S(1)}, bf16[2,80,128]{2,1,0:T(8,128)(2,1)S(1)}, u32[]{:S(2)}, u32[]{:S(2)}) collective-permute-start(bf16[2,80,128]{2,1,0:T(8,128)(2,1)S(1)} %pad_maximum_fusion), channel_id=1, source_target_pairs={{0,3},{1,2},{2,1},{3,0},{4,7},{5,6},{6,5},{7,4},{8,11},{9,10},{10,... | collective-permute-start | bytes 122888 | tf_op jit(solution)/shard_map/ppermute | solution.py:44
  9.3 3.4 %collective-permute-start.3 = (bf16[2,80,128]{2,1,0:T(8,128)(2,1)S(1)}, bf16[2,80,128]{2,1,0:T(8,128)(2,1)S(1)}, u32[]{:S(2)}, u32[]{:S(2)}) collective-permute-start(bf16[2,80,128]{2,1,0:T(8,128)(2,1)S(1)} %pad_maximum_fusion), channel_id=1, source_target_pairs={{0,5},{1,4},{2,7},{3,6},{4,1},{5,0},{6,3},{7,2},{8,13},{9,12},{10,... | collective-permute-start | bytes 122888 | tf_op jit(solution)/shard_map/ppermute | solution.py:44
  12.7 1.5 %collective-permute-start.4 = (bf16[8,80,128]{2,1,0:T(8,128)(2,1)S(1)}, bf16[8,80,128]{2,1,0:T(8,128)(2,1)S(1)}, u32[]{:S(2)}, u32[]{:S(2)}) collective-permute-start(bf16[8,80,128]{2,1,0:T(8,128)(2,1)S(1)} %constant_dynamic-update-slice_fusion.near), channel_id=1, source_target_pairs={{0,1},{1,0},{2,3},{3,2},{4,5},{5,4},{6,7},{7,6},{8,9},{9,8},{10,11... | collective-permute-start | bytes 491528 | tf_op jit(solution)/shard_map/ppermute | solution.py:44
  13.1 5.5 %collective-permute-start.6 = (f32[2,80,128]{2,1,0:T(8,128)S(1)}, f32[2,80,128]{2,1,0:T(8,128)S(1)}, u32[]{:S(2)}, u32[]{:S(2)}) collective-permute-start(f32[2,80,128]{2,1,0:T(8,128)S(1)} %get-tuple-element.55.refs_2_), channel_id=1, source_target_pairs={{0,1},{1,0},{2,3},{3,2},{4,5},{5,4},{6,7},{7,6},{8,9},{9,8},{10,11... | collective-permute-start | bytes 245768 | tf_op jit(solution)/shard_map/ppermute | solution.py:44
  14.6 4.1 %collective-permute-start.5 = (bf16[2,80,128]{2,1,0:T(8,128)(2,1)S(1)}, bf16[2,80,128]{2,1,0:T(8,128)(2,1)S(1)}, u32[]{:S(2)}, u32[]{:S(2)}) collective-permute-start(bf16[2,80,128]{2,1,0:T(8,128)(2,1)S(1)} %get-tuple-element.54.refs_0_), channel_id=1, source_target_pairs={{0,1},{1,0},{2,3},{3,2},{4,5},{5,4},{6,7},{7,6},{8,9},{9,8},{10,11... | collective-permute-start | bytes 122888 | tf_op jit(solution)/shard_map/ppermute | solution.py:44
  21.4 5.0 %collective-permute-start.7 = (bf16[1,80,128]{2,1,0:T(8,128)(2,1)S(1)}, bf16[1,80,128]{2,1,0:T(8,128)(2,1)S(1)}, u32[]{:S(2)}, u32[]{:S(2)}) collective-permute-start(bf16[1,80,128]{2,1,0:T(8,128)(2,1)S(1)} %bitcast.19), channel_id=1, source_target_pairs={{0,9},{1,8},{2,11},{3,10},{4,13},{5,12},{6,15},{7,14},{8,1},{9,0},... | collective-permute-start | bytes 61448 | tf_op jit(solution)/shard_map/ppermute | solution.py:44
  26.4 4.6 %collective-permute-start.8 = (bf16[2,80,128]{2,1,0:T(8,128)(2,1)S(1)}, bf16[2,80,128]{2,1,0:T(8,128)(2,1)S(1)}, u32[]{:S(2)}, u32[]{:S(2)}) collective-permute-start(bf16[2,80,128]{2,1,0:T(8,128)(2,1)S(1)} %pad_maximum_fusion.1), channel_id=1, source_target_pairs={{0,7},{1,6},{2,5},{3,4},{4,3},{5,2},{6,1},{7,0},{8,15},{9,14},{10,... | collective-permute-start | bytes 122888 | tf_op jit(solution)/shard_map/ppermute | solution.py:44
  26.8 4.2 %collective-permute-start.9 = (bf16[2,80,128]{2,1,0:T(8,128)(2,1)S(1)}, bf16[2,80,128]{2,1,0:T(8,128)(2,1)S(1)}, u32[]{:S(2)}, u32[]{:S(2)}) collective-permute-start(bf16[2,80,128]{2,1,0:T(8,128)(2,1)S(1)} %pad_maximum_fusion.1), channel_id=1, source_target_pairs={{0,3},{1,2},{2,1},{3,0},{4,7},{5,6},{6,5},{7,4},{8,11},{9,10},{10,... | collective-permute-start | bytes 122888 | tf_op jit(solution)/shard_map/ppermute | solution.py:44
  27.9 3.6 %collective-permute-start.10 = (bf16[2,80,128]{2,1,0:T(8,128)(2,1)S(1)}, bf16[2,80,128]{2,1,0:T(8,128)(2,1)S(1)}, u32[]{:S(2)}, u32[]{:S(2)}) collective-permute-start(bf16[2,80,128]{2,1,0:T(8,128)(2,1)S(1)} %pad_maximum_fusion.1), channel_id=1, source_target_pairs={{0,5},{1,4},{2,7},{3,6},{4,1},{5,0},{6,3},{7,2},{8,13},{9,12},{10,... | collective-permute-start | bytes 122888 | tf_op jit(solution)/shard_map/ppermute | solution.py:44
  31.4 2.1 %collective-permute-start.11 = (bf16[8,80,128]{2,1,0:T(8,128)(2,1)S(1)}, bf16[8,80,128]{2,1,0:T(8,128)(2,1)S(1)}, u32[]{:S(2)}, u32[]{:S(2)}) collective-permute-start(bf16[8,80,128]{2,1,0:T(8,128)(2,1)S(1)} %constant_dynamic-update-slice_fusion.5.near), channel_id=1, source_target_pairs={{0,1},{1,0},{2,3},{3,2},{4,5},{5,4},{6,7},{7,6},{8,9},{9,8},{10,11... | collective-permute-start | bytes 491528 | tf_op jit(solution)/shard_map/ppermute | solution.py:44
  33.8 4.3 %collective-permute-start.12 = (bf16[1,80,128]{2,1,0:T(8,128)(2,1)S(1)}, bf16[1,80,128]{2,1,0:T(8,128)(2,1)S(1)}, u32[]{:S(2)}, u32[]{:S(2)}) collective-permute-start(bf16[1,80,128]{2,1,0:T(8,128)(2,1)S(1)} %bitcast.14), channel_id=1, source_target_pairs={{0,9},{1,8},{2,11},{3,10},{4,13},{5,12},{6,15},{7,14},{8,1},{9,0},... | collective-permute-start | bytes 61448 | tf_op jit(solution)/shard_map/ppermute | solution.py:44
  38.1 4.4 %collective-permute-start.13 = (bf16[2,80,128]{2,1,0:T(8,128)(2,1)S(1)}, bf16[2,80,128]{2,1,0:T(8,128)(2,1)S(1)}, u32[]{:S(2)}, u32[]{:S(2)}) collective-permute-start(bf16[2,80,128]{2,1,0:T(8,128)(2,1)S(1)} %pad_maximum_fusion.2), channel_id=1, source_target_pairs={{0,7},{1,6},{2,5},{3,4},{4,3},{5,2},{6,1},{7,0},{8,15},{9,14},{10,... | collective-permute-start | bytes 122888 | tf_op jit(solution)/shard_map/ppermute | solution.py:44
  40.3 3.6 %collective-permute-start.14 = (bf16[2,80,128]{2,1,0:T(8,128)(2,1)S(1)}, bf16[2,80,128]{2,1,0:T(8,128)(2,1)S(1)}, u32[]{:S(2)}, u32[]{:S(2)}) collective-permute-start(bf16[2,80,128]{2,1,0:T(8,128)(2,1)S(1)} %pad_maximum_fusion.2), channel_id=1, source_target_pairs={{0,3},{1,2},{2,1},{3,0},{4,7},{5,6},{6,5},{7,4},{8,11},{9,10},{10,... | collective-permute-start | bytes 122888 | tf_op jit(solution)/shard_map/ppermute | solution.py:44
  40.9 3.4 %collective-permute-start.15 = (bf16[2,80,128]{2,1,0:T(8,128)(2,1)S(1)}, bf16[2,80,128]{2,1,0:T(8,128)(2,1)S(1)}, u32[]{:S(2)}, u32[]{:S(2)}) collective-permute-start(bf16[2,80,128]{2,1,0:T(8,128)(2,1)S(1)} %pad_maximum_fusion.2), channel_id=1, source_target_pairs={{0,5},{1,4},{2,7},{3,6},{4,1},{5,0},{6,3},{7,2},{8,13},{9,12},{10,... | collective-permute-start | bytes 122888 | tf_op jit(solution)/shard_map/ppermute | solution.py:44
  44.3 1.5 %collective-permute-start.16 = (bf16[8,80,128]{2,1,0:T(8,128)(2,1)S(1)}, bf16[8,80,128]{2,1,0:T(8,128)(2,1)S(1)}, u32[]{:S(2)}, u32[]{:S(2)}) collective-permute-start(bf16[8,80,128]{2,1,0:T(8,128)(2,1)S(1)} %constant_dynamic-update-slice_fusion.10.near), channel_id=1, source_target_pairs={{0,1},{1,0},{2,3},{3,2},{4,5},{5,4},{6,7},{7,6},{8,9},{9,8},{10,11... | collective-permute-start | bytes 491528 | tf_op jit(solution)/shard_map/ppermute | solution.py:44
  46.3 3.7 %collective-permute-start.17 = (bf16[2,80,128]{2,1,0:T(8,128)(2,1)S(1)}, bf16[2,80,128]{2,1,0:T(8,128)(2,1)S(1)}, u32[]{:S(2)}, u32[]{:S(2)}) collective-permute-start(bf16[2,80,128]{2,1,0:T(8,128)(2,1)S(1)} %get-tuple-element.74.refs_0_), channel_id=1, source_target_pairs={{0,1},{1,0},{2,3},{3,2},{4,5},{5,4},{6,7},{7,6},{8,9},{9,8},{10,11... | collective-permute-start | bytes 122888 | tf_op jit(solution)/shard_map/ppermute | solution.py:44
  53.0 4.6 %collective-permute-start.18 = (bf16[1,80,128]{2,1,0:T(8,128)(2,1)S(1)}, bf16[1,80,128]{2,1,0:T(8,128)(2,1)S(1)}, u32[]{:S(2)}, u32[]{:S(2)}) collective-permute-start(bf16[1,80,128]{2,1,0:T(8,128)(2,1)S(1)} %bitcast.17), channel_id=1, source_target_pairs={{0,9},{1,8},{2,11},{3,10},{4,13},{5,12},{6,15},{7,14},{8,1},{9,0},... | collective-permute-start | bytes 61448 | tf_op jit(solution)/shard_map/ppermute | solution.py:44
  57.6 4.6 %collective-permute-start.19 = (bf16[2,80,128]{2,1,0:T(8,128)(2,1)S(1)}, bf16[2,80,128]{2,1,0:T(8,128)(2,1)S(1)}, u32[]{:S(2)}, u32[]{:S(2)}) collective-permute-start(bf16[2,80,128]{2,1,0:T(8,128)(2,1)S(1)} %pad_maximum_fusion.3), channel_id=1, source_target_pairs={{0,7},{1,6},{2,5},{3,4},{4,3},{5,2},{6,1},{7,0},{8,15},{9,14},{10,... | collective-permute-start | bytes 122888 | tf_op jit(solution)/shard_map/ppermute | solution.py:44
  58.0 4.2 %collective-permute-start.20 = (bf16[2,80,128]{2,1,0:T(8,128)(2,1)S(1)}, bf16[2,80,128]{2,1,0:T(8,128)(2,1)S(1)}, u32[]{:S(2)}, u32[]{:S(2)}) collective-permute-start(bf16[2,80,128]{2,1,0:T(8,128)(2,1)S(1)} %pad_maximum_fusion.3), channel_id=1, source_target_pairs={{0,3},{1,2},{2,1},{3,0},{4,7},{5,6},{6,5},{7,4},{8,11},{9,10},{10,... | collective-permute-start | bytes 122888 | tf_op jit(solution)/shard_map/ppermute | solution.py:44
  58.9 3.4 %collective-permute-start.21 = (bf16[2,80,128]{2,1,0:T(8,128)(2,1)S(1)}, bf16[2,80,128]{2,1,0:T(8,128)(2,1)S(1)}, u32[]{:S(2)}, u32[]{:S(2)}) collective-permute-start(bf16[2,80,128]{2,1,0:T(8,128)(2,1)S(1)} %pad_maximum_fusion.3), channel_id=1, source_target_pairs={{0,5},{1,4},{2,7},{3,6},{4,1},{5,0},{6,3},{7,2},{8,13},{9,12},{10,... | collective-permute-start | bytes 122888 | tf_op jit(solution)/shard_map/ppermute | solution.py:44
  62.3 11.7 %collective-permute-start.22 = (bf16[8,80,128]{2,1,0:T(8,128)(2,1)S(1)}, bf16[8,80,128]{2,1,0:T(8,128)(2,1)S(1)}, u32[]{:S(2)}, u32[]{:S(2)}) collective-permute-start(bf16[8,80,128]{2,1,0:T(8,128)(2,1)S(1)} %constant_dynamic-update-slice_fusion.15.near), channel_id=1, source_target_pairs={{0,1},{1,0},{2,3},{3,2},{4,5},{5,4},{6,7},{7,6},{8,9},{9,8},{10,11... | collective-permute-start | bytes 491528 | tf_op jit(solution)/shard_map/ppermute | solution.py:44
